TPU v7x, 128 devices: a whole 4x4x4 slice. The times are simulated.
128 devices in a mesh: sp: 64 (over z, y, x), tp: 2 (over core).
Axes of the slice: x: 4, y: 4, z: 4, core: 2. Of those that a mesh axis runs over, the one named last changes fastest.
Arguments:
- stream_rows: bfloat16 [12288, 2048], P('sp'), may hold values from -6 to 6
- out_cotangent: bfloat16 [12288, 2048], P('sp'), may hold values from -16 to 16
- expert_ids: int32 [12288, 2], P('sp'), may hold values from 0 to 63, all different within a row; in each aligned block of 192 rows (0 to 191, 192 to 383, ...) at most 9 rows name the same one
- route_weights: float32 [12288, 2], P('sp'), may hold values from 0.05 to 1
- gate_weight: bfloat16 [64, 2048, 1536], P('sp', None, 'tp'), may hold values from -0.125 to 0.125
- up_weight: bfloat16 [64, 2048, 1536], P('sp', None, 'tp'), may hold values from -0.125 to 0.125
- down_weight: bfloat16 [64, 1536, 2048], P('sp', 'tp'), may hold values from -0.15625 to 0.15625
- proj_weight: bfloat16 [1024, 2048], P('tp'), may hold values from -0.1875 to 0.1875
- gate_input: bfloat16 [12288, 1024], P('sp', 'tp'), may hold values from -6 to 6
- scan_out: bfloat16 [12288, 1024], P('sp', 'tp'), may hold values from -6 to 6
- values: bfloat16 [12288, 1024], P('sp', 'tp'), may hold values from -6 to 6
- in_map: bfloat16 [12288, 512], P('sp', 'tp'), may hold values from -2 to 2
- out_map: bfloat16 [12288, 512], P('sp', 'tp'), may hold values from -2 to 2
- log_decay: float32 [12288, 16], P('sp', 'tp'), may hold values from -2 to 0, as said below
Outputs:
- stream_grad: bfloat16 [12288, 2048], P('sp', 'tp')
- proj_grad: float32 [2048, 1024], P('sp', 'tp')
- value_grad: bfloat16 [12288, 1024], P('sp', 'tp')
- in_map_grad: bfloat16 [12288, 512], P('sp', 'tp')
- out_map_grad: bfloat16 [12288, 512], P('sp', 'tp')
- gate_input_grad: bfloat16 [12288, 1024], P('sp', 'tp')
- gate_weight_grad: bfloat16 [64, 2048, 1536], P('sp', None, 'tp')
- up_weight_grad: bfloat16 [64, 2048, 1536], P('sp', None, 'tp')
- down_matrix_gradient: bfloat16 [64, 1536, 2048], P('sp', 'tp')
Inputs may be any that keep to these rules, and one draw needn't show every extreme that they name: `expert_ids`: the 2 experts of a token differ; among the tokens of one index of sp each expert is named at most 9 times, and exactly 9 times in some. `log_decay`: every entry is negative.
All inputs are finite; a program needn't handle non-finite values.
Results may differ from a plain program's by a relative error of at most 0.007.
Values may be sent and summed in bfloat16 or wider, within the bound.
No kernel may reach another device: no remote copies, remote signals or barrier semaphores. Data moves between devices by JAX's collectives and lax.ppermute only.
A program may use at most 192 MiB of HBM per device.

v0:
```python
import jax
import jax.numpy as jnp
from jax import lax
from jax.sharding import Mesh
from jax.sharding import PartitionSpec as P

HEADS = 16
HEAD_DIM = 64
GROUPS = 4
STATE = 128
SP = ("sp_0", "sp_1", "sp_2")


exact_mode = lax.Precision.HIGHEST


def in_one_piece(arrays, axis, split_dim, concat_dim, along):
    both = jnp.concatenate(arrays, axis=along)
    out, at, gathered = (
        lax.all_to_all(both, axis, split_axis=split_dim, concat_axis=concat_dim, tiled=True),
        0,
        [],
    )
    for a in arrays:
        gathered.append(lax.slice_in_dim(out, at, at + a.shape[along], axis=along))
        at += a.shape[along]
    return tuple(gathered)


def split_up(array, dim, length):
    shape = array.shape
    tiles = array.reshape(*shape[:dim], length, shape[dim] // length, *shape[dim + 1 :])
    return jnp.moveaxis(tiles, dim, 0)


def sent_and_summed(array, axis, dim):
    length = lax.axis_size(axis)
    tiles = lax.all_to_all(split_up(array, dim, length), axis, 0, 0, tiled=True)
    return jnp.sum(tiles.astype(jnp.float32), axis=0)


def neutral_like(array, identity):
    return jax.tree.map(
        lambda a, e: jnp.broadcast_to(jnp.asarray(e, a.dtype), a.shape), array, identity
    )


def entering(array, axes, combine, identity, reverse):
    before = start = neutral_like(array, identity)
    running = array
    for axis in reversed(axes):
        length, index = (lax.axis_size(axis), lax.axis_index(axis))
        pieces = jax.tree.map(lambda part: lax.all_gather(part, axis), running)
        inside, running = (start, start)
        for k in reversed(range(length)) if reverse else range(length):
            passed = k > index if reverse else k < index
            running = combine(running, jax.tree.map(lambda part: part[k], pieces))
            inside = jax.tree.map(lambda new, old: jnp.where(passed, new, old), running, inside)
        before = combine(inside, before)
    return before


def silu_slope(pre_act):
    squash = jax.nn.sigmoid(pre_act)
    return squash * (1.0 + pre_act * (1.0 - squash))


def chain_states(earlier, later):
    factor = later[0][:, :, None, None]
    return (earlier[0] * later[0], factor * earlier[1] + later[1], factor * earlier[2] + later[2])


def block_states(value_heads, grad_heads, in_keys, out_keys, cum_decay):
    block_total = cum_decay[-1]
    to_end = jnp.exp(block_total[None] - cum_decay)
    from_start = jnp.exp(cum_decay)
    end_x = jnp.einsum("tge,tgep,tgn->gepn", to_end, value_heads, in_keys, precision=exact_mode)
    end_g = jnp.einsum("tge,tgep,tgn->gepn", to_end, grad_heads, out_keys, precision=exact_mode)
    start_x = jnp.einsum(
        "tge,tgep,tgn->gepn", from_start, value_heads, in_keys, precision=exact_mode
    )
    start_g = jnp.einsum(
        "tge,tgep,tgn->gepn", from_start, grad_heads, out_keys, precision=exact_mode
    )
    return (jnp.exp(block_total), end_x, end_g, start_x, start_g)


def local_grads(
    value_heads, grad_heads, in_keys, out_keys, cum_decay, left_x, left_g, right_x, right_g
):
    block_total = cum_decay[-1]
    from_start = jnp.exp(cum_decay)
    to_end = jnp.exp(block_total[None] - cum_decay)
    cum_heads = jnp.transpose(cum_decay, (1, 2, 0))
    kernel = jnp.exp(-jnp.abs(cum_heads[..., :, None] - cum_heads[..., None, :]))
    intersection = jnp.einsum("tgn,sgn->gts", out_keys, in_keys, precision=exact_mode)
    weighted = kernel * intersection[:, None]
    value_grad = jnp.einsum("gets,tgep->sgep", weighted, grad_heads, precision=exact_mode)
    value_grad = value_grad + jnp.einsum(
        "sge,gepn,sgn->sgep", from_start, left_g, in_keys, precision=exact_mode
    )
    value_grad = value_grad + jnp.einsum(
        "sge,gepn,sgn->sgep", to_end, right_g, in_keys, precision=exact_mode
    )
    pair_weights = kernel * jnp.einsum(
        "tgep,sgep->gets", grad_heads, value_heads, precision=exact_mode
    )
    out_grad = jnp.einsum("gets,sgn->tgn", pair_weights, in_keys, precision=exact_mode)
    out_grad = out_grad + jnp.einsum(
        "tge,gepn,tgep->tgn", from_start, left_x, grad_heads, precision=exact_mode
    )
    out_grad = out_grad + jnp.einsum(
        "tge,gepn,tgep->tgn", to_end, right_x, grad_heads, precision=exact_mode
    )
    in_grad = jnp.einsum("gets,tgn->sgn", pair_weights, out_keys, precision=exact_mode)
    in_grad = in_grad + jnp.einsum(
        "sge,gepn,sgep->sgn", from_start, left_g, value_heads, precision=exact_mode
    )
    in_grad = in_grad + jnp.einsum(
        "sge,gepn,sgep->sgn", to_end, right_g, value_heads, precision=exact_mode
    )
    return (value_grad, in_grad, out_grad)


def fill_slots(slot_ids, flattened_rows, slot_count):
    blank_rows = jnp.zeros((slot_count, flattened_rows.shape[1]), jnp.bfloat16)
    return blank_rows.at[slot_ids].set(flattened_rows)


def on_device(
    stream_rows,
    out_cotangent,
    expert_ids,
    route_weights,
    gate_weight,
    up_weight,
    down_weight,
    proj_weight,
    gate_input,
    scan_out,
    values,
    in_map,
    out_map,
    log_decay,
):
    experts = lax.axis_size(SP)
    tok_rows = stream_rows.shape[0]
    width = stream_rows.shape[1]
    top_count = expert_ids.shape[1]
    capacity = max(2, 3 * tok_rows // experts)
    flat_ids = expert_ids.reshape(-1)
    onehot = (flat_ids[:, None] == jnp.arange(experts, dtype=jnp.int32)[None, :]).astype(jnp.int32)
    rank_in = jnp.sum((jnp.cumsum(onehot, axis=0) - 1) * onehot, axis=1)
    slot_ids = flat_ids * capacity + rank_in
    part_w = width // lax.axis_size("tp")
    offset = lax.axis_index("tp") * part_w
    routed_rows = jnp.broadcast_to(stream_rows[:, None, :], (tok_rows, top_count, width))
    scaled = (route_weights[:, :, None] * out_cotangent[:, None, :].astype(jnp.float32)).astype(
        jnp.bfloat16
    )
    send_rows = lax.dynamic_slice_in_dim(routed_rows, offset, part_w, 2).reshape(-1, part_w)
    send_cot = lax.dynamic_slice_in_dim(scaled, offset, part_w, 2).reshape(-1, part_w)
    buf_rows = fill_slots(slot_ids, send_rows, experts * capacity).reshape(
        experts, capacity, part_w
    )
    buf_cot = fill_slots(slot_ids, send_cot, experts * capacity).reshape(experts, capacity, part_w)
    got_rows, got_cot = in_one_piece((buf_rows, buf_cot), SP, 0, 0, 1)
    got_rows, got_cot = (
        lax.all_gather(got_rows, "tp", axis=2, tiled=True),
        lax.all_gather(got_cot, "tp", axis=2, tiled=True),
    )
    row_data = got_rows.reshape(-1, width)
    cotangent = got_cot.reshape(-1, width)
    gate_w = gate_weight[0]
    up_w = up_weight[0]
    down_w = down_weight[0]
    outer_dims = (((0,), (0,)), ((), ()))
    inner_dims = (((1,), (1,)), ((), ()))
    gate_pre = jnp.dot(row_data, gate_w, preferred_element_type=jnp.float32)
    up_val = jnp.dot(row_data, up_w, preferred_element_type=jnp.float32)
    active = (jax.nn.silu(gate_pre) * up_val).astype(jnp.bfloat16)
    down_grad = lax.dot_general(
        active, cotangent, outer_dims, preferred_element_type=jnp.float32
    ).astype(jnp.bfloat16)
    act_grad = lax.dot_general(cotangent, down_w, inner_dims, preferred_element_type=jnp.float32)
    up_grad = (act_grad * jax.nn.silu(gate_pre)).astype(jnp.bfloat16)
    pre_grad = (act_grad * up_val * silu_slope(gate_pre)).astype(jnp.bfloat16)
    gate_w_grad = lax.dot_general(
        row_data, pre_grad, outer_dims, preferred_element_type=jnp.float32
    ).astype(jnp.bfloat16)
    up_w_grad = lax.dot_general(
        row_data, up_grad, outer_dims, preferred_element_type=jnp.float32
    ).astype(jnp.bfloat16)
    partial_value = lax.dot_general(
        pre_grad, gate_w, inner_dims, preferred_element_type=jnp.float32
    )
    partial_value = partial_value + lax.dot_general(
        up_grad, up_w, inner_dims, preferred_element_type=jnp.float32
    )
    summed = sent_and_summed(partial_value.astype(jnp.bfloat16), "tp", 1).astype(jnp.bfloat16)
    returned_buf = lax.all_to_all(
        summed.reshape(experts, capacity, part_w), SP, split_axis=0, concat_axis=0, tiled=True
    )
    returned = returned_buf.reshape(-1, part_w)[slot_ids].reshape(tok_rows, top_count, part_w)
    own_cot = lax.dynamic_slice_in_dim(out_cotangent, offset, part_w, 1)
    stream_grad = (
        own_cot.astype(jnp.float32) + jnp.sum(returned.astype(jnp.float32), axis=1)
    ).astype(jnp.bfloat16)
    stream_full = lax.all_gather(stream_grad, "tp", axis=1, tiled=True)
    gate_vals = gate_input.astype(jnp.float32)
    scan_vals = scan_out.astype(jnp.float32)
    mixed_grad = lax.dot_general(
        stream_full, proj_weight, inner_dims, preferred_element_type=jnp.float32
    )
    gated = (scan_vals * jax.nn.silu(gate_vals)).astype(jnp.bfloat16)
    gate_grad = (mixed_grad * scan_vals * silu_slope(gate_vals)).astype(jnp.bfloat16)
    scan_grad = (mixed_grad * jax.nn.silu(gate_vals)).astype(jnp.bfloat16)
    proj_grad = sent_and_summed(
        lax.dot_general(stream_full, gated, outer_dims, preferred_element_type=jnp.float32).astype(
            jnp.bfloat16
        ),
        SP,
        0,
    )
    groups = in_map.shape[1] // STATE
    per_group = HEADS // GROUPS
    value_heads = values.astype(jnp.float32).reshape(tok_rows, groups, per_group, HEAD_DIM)
    grad_heads = scan_grad.astype(jnp.float32).reshape(tok_rows, groups, per_group, HEAD_DIM)
    in_keys = in_map.astype(jnp.float32).reshape(tok_rows, groups, STATE)
    out_keys = out_map.astype(jnp.float32).reshape(tok_rows, groups, STATE)
    cum_decay = jnp.cumsum(log_decay.reshape(tok_rows, groups, per_group), axis=0)
    decay_tot, end_x, end_g, start_x, start_g = block_states(
        value_heads, grad_heads, in_keys, out_keys, cum_decay
    )
    identity = (jnp.ones_like(decay_tot), jnp.zeros_like(end_x), jnp.zeros_like(end_g))
    left_state = entering((decay_tot, end_x, end_g), SP, chain_states, identity, False)
    right_state = entering((decay_tot, start_x, start_g), SP, chain_states, identity, True)
    value_grad, in_grad, out_grad = local_grads(
        value_heads,
        grad_heads,
        in_keys,
        out_keys,
        cum_decay,
        left_state[1],
        left_state[2],
        right_state[1],
        right_state[2],
    )
    value_grad = value_grad.reshape(tok_rows, -1).astype(jnp.bfloat16)
    in_grad = in_grad.reshape(tok_rows, -1).astype(jnp.bfloat16)
    out_grad = out_grad.reshape(tok_rows, -1).astype(jnp.bfloat16)
    return (
        stream_grad,
        proj_grad,
        value_grad,
        in_grad,
        out_grad,
        gate_grad,
        gate_w_grad[None],
        up_w_grad[None],
        down_grad[None],
    )


def solution(mesh):
    finer = Mesh(mesh.devices.reshape(4, 4, 4, mesh.shape["tp"]), ("sp_0", "sp_1", "sp_2", "tp"))
    return jax.shard_map(
        on_device,
        mesh=finer,
        in_specs=(
            P(SP, None),
            P(SP, None),
            P(SP, None),
            P(SP, None),
            P(SP, None, "tp"),
            P(SP, None, "tp"),
            P(SP, "tp", None),
            P("tp", None),
            P(SP, "tp"),
            P(SP, "tp"),
            P(SP, "tp"),
            P(SP, "tp"),
            P(SP, "tp"),
            P(SP, "tp"),
        ),
        out_specs=(
            P(SP, "tp"),
            P(SP, "tp"),
            P(SP, "tp"),
            P(SP, "tp"),
            P(SP, "tp"),
            P(SP, "tp"),
            P(SP, None, "tp"),
            P(SP, None, "tp"),
            P(SP, "tp", None),
        ),
        check_vma=False,
    )
```

profile of v0, /device:TPU:0, one launch (start us, length us, event | category | flops | bytes accessed | tf_op | source)
XLA Modules:
  0.0 528.8 jit_solution(12722006792180912339)
XLA Ops:
  42.6 52.9 %all_to_all.20 = bf16[64,18,1024]{2,1,0:T(8,128)(2,1)S(1)} all-to-all(bf16[64,18,1024]{2,1,0:T(8,128)(2,1)S(1)} %pad_maximum_fusion), channel_id=1, replica_groups=mesh['sp_0'=4,'sp_1'=4,'sp_2'=4,'tp'=2] {'sp_0','sp_1','sp_2'}, dimensions={0} | all-to-all | bytes 4718592 | tf_op jit(solution)/shard_map/all_to_all | solution.py:20
  104.2 7.1 %all-gather.21.cloned.1.call-done = bf16[64,9,2048]{2,1,0:T(8,128)(2,1)} async-done(((bf16[64,9,1024]{2,1,0:T(8,128)(2,1)}), bf16[64,9,2048]{2,1,0:T(8,128)(2,1)}) %all-gather.21.cloned.1.call-update) | async-done | bytes 2359312 | tf_op jit(solution)/shard_map/all_gather | solution.py:169
  116.0 5.1 fusion.2
  124.3 7.0 %all-gather.19.cloned.1.call-done = bf16[64,9,2048]{2,1,0:T(8,128)(2,1)} async-done(((bf16[64,9,1024]{2,1,0:T(8,128)(2,1)}), bf16[64,9,2048]{2,1,0:T(8,128)(2,1)}) %all-gather.19.cloned.1.call-update) | async-done | bytes 2359312 | tf_op jit(solution)/shard_map/all_gather | solution.py:170
  136.0 6.1 %multiply_convert_fusion.1 = (bf16[576,768]{1,0:T(8,128)(2,1)S(1)}, bf16[576,768]{1,0:T(8,128)(2,1)S(1)}) fusion(f32[576,768]{1,0:T(8,128)} %fusion.2, f32[576,768]{1,0:T(8,128)} %fusion.6, bf16[576,2048]{1,0:T(8,128)(2,1)} %reshape.301, bf16[1,768,2048]{2,1,0:T(8,128)(2,1)} %param.20), kind=kOutput, calls=%fused_computation.25 | convolution fusion | flops 1817690112 | bytes 10813440 | tf_op jit(solution)/shard_map/dot_general | solution.py:185
  146.9 5.6 %all_to_all.21 = bf16[2,576,1024]{2,1,0:T(8,128)(2,1)S(1)} all-to-all(bf16[2,576,1024]{2,1,0:T(8,128)(2,1)S(1)} %bitcast.561), channel_id=1, replica_groups=mesh['sp_0'=4,'sp_1'=4,'sp_2'=4,'tp'=2] {'tp'}, dimensions={0} | all-to-all | bytes 4718592 | tf_op jit(solution)/shard_map/all_to_all | solution.py:38
  157.7 14.9 %all-to-all-start.2 = ((bf16[64,9,1024]{2,1,0:T(8,128)(2,1)}), bf16[64,9,1024]{2,1,0:T(8,128)(2,1)S(1)}, u32[]{:S(2)}, u32[]{:S(2)}) async-start(bf16[64,9,1024]{2,1,0:T(8,128)(2,1)} %reshape.304), calls=%async_computation.2 | async-start | bytes 4194304 | tf_op jit(solution)/shard_map/all_to_all | solution.py:201
  177.1 33.4 %all-to-all-done.2 = bf16[64,9,1024]{2,1,0:T(8,128)(2,1)S(1)} async-done(((bf16[64,9,1024]{2,1,0:T(8,128)(2,1)}), bf16[64,9,1024]{2,1,0:T(8,128)(2,1)S(1)}, u32[]{:S(2)}, u32[]{:S(2)}) %all-to-all-start.2) | async-done | bytes 1179680 | tf_op jit(solution)/shard_map/all_to_all | solution.py:201
  224.9 8.0 %all_gather.90 = f32[4,2,4]{2,1,0:T(2,128)S(1)} all-gather(f32[1,2,4]{2,1,0:T(2,128)S(1)} %copy.143), channel_id=1, replica_groups=mesh['sp_0'=4,'sp_1'=4,'sp_2'=4,'tp'=2] {'sp_2'}, dimensions={0}, use_global_device_ids=true | all-gather | bytes 160 | tf_op jit(solution)/shard_map/all_gather | solution.py:53
  232.9 7.6 %all_gather.91 = f32[4,2,4]{2,1,0:T(2,128)S(1)} all-gather(f32[1,2,4]{2,1,0:T(2,128)S(1)} %get-tuple-element.87), channel_id=1, replica_groups=mesh['sp_0'=4,'sp_1'=4,'sp_2'=4,'tp'=2] {'sp_1'}, dimensions={0}, use_global_device_ids=true | all-gather | bytes 160 | tf_op jit(solution)/shard_map/all_gather | solution.py:53
  246.0 23.1 %all-gather.45.cloned.1.call-done = f32[8,4,64,128]{3,2,1,0:T(8,128)} async-done(((f32[2,4,64,128]{3,2,1,0:T(8,128)}), f32[8,4,64,128]{3,2,1,0:T(8,128)}) %all-gather.45.cloned.1.call-update) | async-done | bytes 1048592 | tf_op jit(solution)/shard_map/all_gather | solution.py:53
  269.1 26.7 %all-gather.41.cloned.1.call-done = f32[8,4,64,128]{3,2,1,0:T(8,128)} async-done(((f32[2,4,64,128]{3,2,1,0:T(8,128)}), f32[8,4,64,128]{3,2,1,0:T(8,128)}) %all-gather.41.cloned.1.call-update) | async-done | bytes 1048592 | tf_op jit(solution)/shard_map/all_gather | solution.py:53
  299.0 22.9 %all-gather.23.cloned.1.call-done = f32[4,2,4,64,128]{4,3,2,1,0:T(8,128)} async-done(((f32[1,2,4,64,128]{4,3,2,1,0:T(8,128)}), f32[4,2,4,64,128]{4,3,2,1,0:T(8,128)}) %all-gather.23.cloned.1.call-update) | async-done | bytes 1048592 | tf_op jit(solution)/shard_map/all_gather | solution.py:53
  321.9 26.1 %all-gather.31.cloned.1.call-done = f32[4,2,4,64,128]{4,3,2,1,0:T(8,128)} async-done(((f32[1,2,4,64,128]{4,3,2,1,0:T(8,128)}), f32[4,2,4,64,128]{4,3,2,1,0:T(8,128)}) %all-gather.31.cloned.1.call-update) | async-done | bytes 1048592 | tf_op jit(solution)/shard_map/all_gather | solution.py:53
  350.7 8.5 %all_gather.97 = f32[4,2,4]{2,1,0:T(2,128)S(1)} all-gather(f32[1,2,4]{2,1,0:T(2,128)S(1)} %get-tuple-element.89), channel_id=1, replica_groups=mesh['sp_0'=4,'sp_1'=4,'sp_2'=4,'tp'=2] {'sp_1'}, dimensions={0}, use_global_device_ids=true | all-gather | bytes 160 | tf_op jit(solution)/shard_map/all_gather | solution.py:53
  359.2 15.4 %all-gather.27.cloned.1.call-done = f32[4,2,4,64,128]{4,3,2,1,0:T(8,128)} async-done(((f32[1,2,4,64,128]{4,3,2,1,0:T(8,128)}), f32[4,2,4,64,128]{4,3,2,1,0:T(8,128)}) %all-gather.27.cloned.1.call-update) | async-done | bytes 1048592 | tf_op jit(solution)/shard_map/all_gather | solution.py:53
  374.6 26.5 %all-gather.35.cloned.1.call-done = f32[4,2,4,64,128]{4,3,2,1,0:T(8,128)} async-done(((f32[1,2,4,64,128]{4,3,2,1,0:T(8,128)}), f32[4,2,4,64,128]{4,3,2,1,0:T(8,128)}) %all-gather.35.cloned.1.call-update) | async-done | bytes 1048592 | tf_op jit(solution)/shard_map/all_gather | solution.py:53
  403.7 9.9 %all_gather.92 = f32[4,2,4]{2,1,0:T(2,128)S(1)} all-gather(f32[1,2,4]{2,1,0:T(2,128)S(1)} %get-tuple-element.81), channel_id=1, replica_groups=mesh['sp_0'=4,'sp_1'=4,'sp_2'=4,'tp'=2] {'sp_0'}, dimensions={0}, use_global_device_ids=true | all-gather | bytes 160 | tf_op jit(solution)/shard_map/all_gather | solution.py:53
  413.6 7.1 %all_gather.98 = f32[4,2,4]{2,1,0:T(2,128)S(1)} all-gather(f32[1,2,4]{2,1,0:T(2,128)S(1)} %get-tuple-element.99), channel_id=1, replica_groups=mesh['sp_0'=4,'sp_1'=4,'sp_2'=4,'tp'=2] {'sp_0'}, dimensions={0}, use_global_device_ids=true | all-gather | bytes 160 | tf_op jit(solution)/shard_map/all_gather | solution.py:53
  423.2 8.2 %all-to-all-start.3 = ((bf16[64,32,512]{2,1,0:T(8,128)(2,1)}), bf16[64,32,512]{2,1,0:T(8,128)(2,1)S(1)}, u32[]{:S(2)}, u32[]{:S(2)}) async-start(bf16[64,32,512]{2,1,0:T(8,128)(2,1)} %bitcast.578), calls=%async_computation.3 | async-start | bytes 4194304 | tf_op jit(solution)/shard_map/all_to_all | solution.py:38
  432.0 6.4 %fusion.10 = bf16[1,2048,768]{2,1,0:T(8,128)(2,1)} fusion(bf16[576,2048]{1,0:T(8,128)(2,1)} %reshape.302, bf16[576,768]{1,0:T(8,128)(2,1)} %copy-done.47), kind=kOutput, calls=%fused_computation.20 | convolution fusion | flops 1813512192 | bytes 6389760 | tf_op jit(solution)/shard_map/dot_general | solution.py:188
  449.3 6.4 %all-to-all-done.3 = bf16[64,32,512]{2,1,0:T(8,128)(2,1)S(1)} async-done(((bf16[64,32,512]{2,1,0:T(8,128)(2,1)}), bf16[64,32,512]{2,1,0:T(8,128)(2,1)S(1)}, u32[]{:S(2)}, u32[]{:S(2)}) %all-to-all-start.3) | async-done | bytes 2097184 | tf_op jit(solution)/shard_map/all_to_all | solution.py:38
  469.1 19.4 %all-gather.29.cloned.1.call-done = f32[4,2,4,64,128]{4,3,2,1,0:T(8,128)} async-done(((f32[1,2,4,64,128]{4,3,2,1,0:T(8,128)}), f32[4,2,4,64,128]{4,3,2,1,0:T(8,128)}) %all-gather.29.cloned.1.call-update) | async-done | bytes 1048592 | tf_op jit(solution)/shard_map/all_gather | solution.py:53
  493.3 21.4 %all-gather.25.cloned.1.call-done = f32[4,2,4,64,128]{4,3,2,1,0:T(8,128)} async-done(((f32[1,2,4,64,128]{4,3,2,1,0:T(8,128)}), f32[4,2,4,64,128]{4,3,2,1,0:T(8,128)}) %all-gather.25.cloned.1.call-update) | async-done | bytes 1048592 | tf_op jit(solution)/shard_map/all_gather | solution.py:53
  (234 shorter events, 136.3 us)
Async XLA Ops:
  8.0 108.0 %copy-start = (bf16[1,2048,768]{2,1,0:T(8,128)(2,1)S(1)}, bf16[1,2048,768]{2,1,0:T(8,128)(2,1)}, u32[]{:S(2)}) copy-start(bf16[1,2048,768]{2,1,0:T(8,128)(2,1)} %param.18) | copy-start | bytes 9437188
  8.0 103.3 %all-gather.21.cloned.1.call-start = ((), (), s32[]{:S(2)}) async-start(), calls=%async_computation.5 | async-start | bytes 6291456 | tf_op jit(solution)/shard_map/all_gather | solution.py:169
  98.8 32.5 %all-gather.19.cloned.1.call-start = ((), (), s32[]{:S(2)}) async-start(), calls=%async_computation.4 | async-start | bytes 6291456 | tf_op jit(solution)/shard_map/all_gather | solution.py:170
  102.5 70.2 %copy-start.22 = (f32[4,2,256]{2,0,1:T(4,128)}, f32[4,2,256]{2,0,1:T(4,128)S(1)}, u32[]{:S(2)}) copy-start(f32[4,2,256]{2,0,1:T(4,128)S(1)} %copy.224) | copy-start | bytes 24580
  157.7 52.8 %all-to-all-start.2 = ((bf16[64,9,1024]{2,1,0:T(8,128)(2,1)}), bf16[64,9,1024]{2,1,0:T(8,128)(2,1)S(1)}, u32[]{:S(2)}, u32[]{:S(2)}) async-start(bf16[64,9,1024]{2,1,0:T(8,128)(2,1)} %reshape.304), calls=%async_computation.2 | async-start | bytes 4194304 | tf_op jit(solution)/shard_map/all_to_all | solution.py:201
  172.6 67.9 %all-gather.43.cloned.1.call-start = ((), (), s32[]{:S(2)}) async-start(), calls=%async_computation.16 | async-start | bytes 1310720 | tf_op jit(solution)/shard_map/all_gather | solution.py:53
  175.8 66.9 %all-gather.39.cloned.1.call-start = ((), (), s32[]{:S(2)}) async-start(), calls=%async_computation.14 | async-start | bytes 1310720 | tf_op jit(solution)/shard_map/all_gather | solution.py:53
  222.4 46.8 %all-gather.45.cloned.1.call-start = ((), (), s32[]{:S(2)}) async-start(), calls=%async_computation.17 | async-start | bytes 1310720 | tf_op jit(solution)/shard_map/all_gather | solution.py:53
  223.6 72.2 %all-gather.41.cloned.1.call-start = ((), (), s32[]{:S(2)}) async-start(), calls=%async_computation.15 | async-start | bytes 1310720 | tf_op jit(solution)/shard_map/all_gather | solution.py:53
  224.8 97.2 %all-gather.23.cloned.1.call-start = ((), (), s32[]{:S(2)}) async-start(), calls=%async_computation.6 | async-start | bytes 1310720 | tf_op jit(solution)/shard_map/all_gather | solution.py:53
  240.5 216.2 %copy-start.24 = (f32[2,4]{1,0:T(2,128)}, f32[2,4]{1,0:T(2,128)S(1)}, u32[]{:S(2)}) copy-start(f32[2,4]{1,0:T(2,128)S(1)} %get-tuple-element.76) | copy-start | bytes 100
  240.5 216.2 %copy-start.35 = (f32[2,4]{1,0:T(2,128)}, f32[2,4]{1,0:T(2,128)S(1)}, u32[]{:S(2)}) copy-start(f32[2,4]{1,0:T(2,128)S(1)} %get-tuple-element.73) | copy-start | bytes 100
  245.2 102.8 %all-gather.31.cloned.1.call-start = ((), (), s32[]{:S(2)}) async-start(), calls=%async_computation.10 | async-start | bytes 1310720 | tf_op jit(solution)/shard_map/all_gather | solution.py:53
  246.0 128.6 %all-gather.27.cloned.1.call-start = ((), (), s32[]{:S(2)}) async-start(), calls=%async_computation.8 | async-start | bytes 1310720 | tf_op jit(solution)/shard_map/all_gather | solution.py:53
  298.4 102.7 %all-gather.35.cloned.1.call-start = ((), (), s32[]{:S(2)}) async-start(), calls=%async_computation.12 | async-start | bytes 1310720 | tf_op jit(solution)/shard_map/all_gather | solution.py:53
  299.0 157.7 %all-gather.33.cloned.1.call-start = ((), (), s32[]{:S(2)}) async-start(), calls=%async_computation.11 | async-start | bytes 1310720 | tf_op jit(solution)/shard_map/all_gather | solution.py:53
  299.0 157.7 %copy-start.26 = (f32[2,4]{1,0:T(2,128)}, f32[2,4]{1,0:T(2,128)S(1)}, u32[]{:S(2)}) copy-start(f32[2,4]{1,0:T(2,128)S(1)} %get-tuple-element.82) | copy-start | bytes 100
  299.0 157.7 %copy-start.28 = (f32[2,4]{1,0:T(2,128)}, f32[2,4]{1,0:T(2,128)S(1)}, u32[]{:S(2)}) copy-start(f32[2,4]{1,0:T(2,128)S(1)} %get-tuple-element.83) | copy-start | bytes 100
  299.0 157.7 %copy-start.30 = (f32[2,4]{1,0:T(2,128)}, f32[2,4]{1,0:T(2,128)S(1)}, u32[]{:S(2)}) copy-start(f32[2,4]{1,0:T(2,128)S(1)} %get-tuple-element.84) | copy-start | bytes 100
  350.6 70.2 %copy-start.18 = (bf16[192,256]{1,0:T(8,128)(2,1)S(1)}, bf16[192,256]{1,0:T(8,128)(2,1)}, u32[]{:S(2)}) copy-start(bf16[192,256]{1,0:T(8,128)(2,1)} %param.26) | copy-start | bytes 294916
  350.6 114.1 %all-gather.37.cloned.1.call-start = ((), (), s32[]{:S(2)}) async-start(), calls=%async_computation.13 | async-start | bytes 1310720 | tf_op jit(solution)/shard_map/all_gather | solution.py:53
  423.2 32.5 %all-to-all-start.3 = ((bf16[64,32,512]{2,1,0:T(8,128)(2,1)}), bf16[64,32,512]{2,1,0:T(8,128)(2,1)S(1)}, u32[]{:S(2)}, u32[]{:S(2)}) async-start(bf16[64,32,512]{2,1,0:T(8,128)(2,1)} %bitcast.578), calls=%async_computation.3 | async-start | bytes 4194304 | tf_op jit(solution)/shard_map/all_to_all | solution.py:38
  431.4 57.1 %all-gather.29.cloned.1.call-start = ((), (), s32[]{:S(2)}) async-start(), calls=%async_computation.9 | async-start | bytes 1310720 | tf_op jit(solution)/shard_map/all_gather | solution.py:53
  431.9 82.8 %all-gather.25.cloned.1.call-start = ((), (), s32[]{:S(2)}) async-start(), calls=%async_computation.7 | async-start | bytes 1310720 | tf_op jit(solution)/shard_map/all_gather | solution.py:53
  (44 other events, 625.7 us)
Sparse Core Ops, SparseCore 0:
  98.9 12.3 all-gather.20
  113.5 17.6 all-gather.18
Sparse Core Ops, SparseCore 1:
  175.9 31.1 all-gather.42
  222.5 20.1 all-gather.38
  244.8 24.3 all-gather.44
  271.4 24.3 all-gather.40
  297.5 24.4 all-gather.22
  323.6 24.4 all-gather.30
  350.2 24.4 all-gather.26
  376.7 24.4 all-gather.34
  402.6 24.6 all-gather.32
  429.0 35.7 all-gather.36
  466.3 22.1 all-gather.28
  490.2 24.5 all-gather.24
where the time goes:
time: 538 us; the launch traced here: 529 us
  waiting for transfers between devices  245 us (46%)
  blocking collectives  102 us (19%)
  matrix products  56 us (10%)
  local copies, waits for them, and re-layouts  52.4 us (10%)
  other arithmetic  33 us (6%)
  starting transfers between devices  23.7 us (4%)
  between operations  16.8 us (3%)
    all_gather x12, waiting for transfers between devices, entering(): pieces = jax.tree.map(lambda part: lax.all_gather(part, axis), running)  188 us
    all_to_all x1, blocking collectives, in_one_piece(): lax.all_to_all(both, axis, split_axis=split_dim, concat_axis=concat_dim,...  52.9 us
    all_gather x5, blocking collectives, entering(): pieces = jax.tree.map(lambda part: lax.all_gather(part, axis), running)  41.1 us
    all_to_all x1, waiting for transfers between devices, on_device(): lax.all_to_all(summed.reshape(experts, capacity, part_w), SP, split_axis=...  33.4 us
    all_to_all x1, starting transfers between devices, on_device(): lax.all_to_all(summed.reshape(experts, capacity, part_w), SP, split_axis=...  14.9 us
  transfers between devices with their start and end apart: 16, of which 14 were waited for; matrix products, arithmetic and copies ran while one was open for 14% of the time, Pallas kernels for 0%

commit v1 on v0

v1 whole, which is shorter than its diff:
```python
import jax
import jax.numpy as jnp
from jax import lax
from jax.experimental import pallas as pl
from jax.experimental.pallas import tpu as pltpu
from jax.sharding import Mesh
from jax.sharding import PartitionSpec as P

SP = ("sp_0", "sp_1", "sp_2")
TOK = 192
WIDTH = 2048
HALF = 1024
EXPERTS = 64
MAIN = 512
SLOTS = 576
FF = 768
FF_STEP = 256
CHAN = 512
KEYS = 256
HEADS = 8
BLOCKS = 64

BF = jnp.bfloat16
F32 = jnp.float32
EXACT = lax.Precision.HIGHEST


def mm(a, b, dims, precision=None):
    return lax.dot_general(a, b, (dims, ((), ())), preferred_element_type=F32, precision=precision)


NN = ((1,), (0,))
NT = ((1,), (1,))
TN = ((0,), (0,))


def iota(shape, dim):
    return lax.broadcasted_iota(jnp.int32, shape, dim)


def ones_where(mask):
    return jnp.where(mask, 1.0, 0.0).astype(BF)


def call(body, name, out_shape, flops, **kw):
    vmem = kw.pop("vmem", 40 << 20)
    return pl.pallas_call(
        body,
        out_shape=out_shape,
        name=name,
        compiler_params=pltpu.CompilerParams(vmem_limit_bytes=vmem),
        cost_estimate=pl.CostEstimate(flops=flops, bytes_accessed=1 << 20, transcendentals=0),
        **kw,
    )


def shape(dims, dtype=BF):
    return jax.ShapeDtypeStruct(dims, dtype)


def slot_choices(ids):
    lane = iota((TOK, EXPERTS), 1)
    named = [ids[:, k : k + 1] == lane for k in range(2)]
    either = ones_where(named[0] | named[1])
    earlier = ones_where(iota((TOK, TOK), 1) < iota((TOK, TOK), 0))
    count = mm(earlier, either, NN)
    picks = []
    for k in range(2):
        rank = jnp.sum(jnp.where(named[k], count, 0.0), axis=1, keepdims=True).astype(jnp.int32)
        own = ids[:, k : k + 1]
        row = jnp.where(rank < 8, own * 8 + rank, MAIN + own)
        picks.append(row == iota((TOK, SLOTS), 1))
    return picks


def fold_last(rows):
    q = iota((MAIN, MAIN), 0)
    order = ones_where(iota((MAIN, MAIN), 1) == (q & 7) * EXPERTS + (q >> 3))
    stacked = jnp.concatenate([rows[:, 128 * j : 128 * j + 128] for j in range(8)], axis=0)
    return mm(order, stacked, NN).astype(BF)


def unfold_last(folded):
    c = iota((MAIN, MAIN), 0)
    order = ones_where(iota((MAIN, MAIN), 1) == (c & 63) * 8 + (c >> 6))
    stacked = mm(order, folded, NN).astype(BF)
    return [
        jnp.concatenate(
            [stacked[64 * j : 64 * j + 64, 128 * i : 128 * i + 128] for j in range(8)], axis=1
        )
        for i in range(folded.shape[1] // 128)
    ]


def pack_body(tp, ids, weights, rows, cot, out):
    first, second = slot_choices(ids[...])
    both = ones_where(first | second)
    row_slots = mm(both, rows[...], TN).astype(BF)
    full = cot[...].astype(F32)
    cot_slots = mm(ones_where(first), (weights[:, 0:1] * full).astype(BF), TN)
    cot_slots = cot_slots + mm(ones_where(second), (weights[:, 1:2] * full).astype(BF), TN)
    cot_slots = cot_slots.astype(BF)
    out[:, 0:HALF] = row_slots[:MAIN]
    out[:, HALF : 2 * HALF] = cot_slots[:MAIN]
    out[:, 2 * HALF : 2 * HALF + 128] = fold_last(row_slots[MAIN:])
    out[:, 2 * HALF + 128 :] = fold_last(cot_slots[MAIN:])


def whole(dims):
    return pl.BlockSpec(dims, lambda *_: (0,) * len(dims))


def pack(tp, ids, weights, rows, cot):
    spec = pltpu.PrefetchScalarGridSpec(
        num_scalar_prefetch=1,
        grid=(1,),
        in_specs=[
            whole((TOK, 2)),
            whole((TOK, 2)),
            pl.BlockSpec((TOK, HALF), lambda i, t: (0, t[0])),
            pl.BlockSpec((TOK, HALF), lambda i, t: (0, t[0])),
        ],
        out_specs=whole((MAIN, 2 * HALF + 256)),
    )
    return call(
        pack_body, "pack", shape((MAIN, 2 * HALF + 256)), 1_000_000_000, grid_spec=spec
    )(tp, ids, weights, rows, cot)


def decay_body(values, in_map, log_decay, payload, start_w, end_w, cum_out, cum_t_out):
    upto = jnp.where(iota((TOK, TOK), 1) <= iota((TOK, TOK), 0), 1.0, 0.0)
    cum = mm(upto, log_decay[...], NN, EXACT)
    cum_t = mm(log_decay[...], upto, ((0,), (1,)), EXACT)
    cum_out[...] = cum
    cum_t_out[...] = cum_t
    spread = jnp.where(iota((HEADS, CHAN), 1) // 64 == iota((HEADS, CHAN), 0), 1.0, 0.0)
    from_start = mm(jnp.exp(cum), spread, NN, EXACT)
    to_end = mm(jnp.exp(cum[TOK - 1 :, :] - cum), spread, NN, EXACT)
    start_w[...] = from_start
    end_w[...] = to_end
    val = values[...].astype(F32)
    block_states(payload, (to_end * val).astype(BF), (from_start * val).astype(BF), in_map)
    total = jnp.exp(cum_t[:, TOK - 1 :])
    total = jnp.concatenate(
        [jnp.broadcast_to(total[h : h + 1], (64, 128)) for h in range(HEADS)], axis=0
    )
    high = total.astype(BF)
    rest = total - high.astype(F32)
    mid = rest.astype(BF)
    low = (rest - mid.astype(F32)).astype(BF)
    part = iota((MAIN, 128), 0) & 7
    parts = jnp.where(part == 0, high.astype(F32), 0.0)
    parts = jnp.where(part == 1, mid.astype(F32), parts)
    parts = jnp.where(part == 2, low.astype(F32), parts)
    payload[:, 256:] = parts.astype(BF)


def block_states(payload, to_end, from_start, keys):
    for g in range(2):
        chan = slice(256 * g, 256 * g + 256)
        key = keys[:, 128 * g : 128 * g + 128]
        payload[chan, 0:128] = mm(to_end[:, chan], key, TN).astype(BF)
        payload[chan, 128:256] = mm(from_start[:, chan], key, TN).astype(BF)


def decay(values, in_map, log_decay):
    return call(
        decay_body,
        "decay",
        (
            shape((MAIN, 384)),
            shape((TOK, CHAN), F32),
            shape((TOK, CHAN), F32),
            shape((TOK, HEADS), F32),
            shape((HEADS, TOK), F32),
        ),
        1_000_000_000,
    )(values, in_map, log_decay)


def silu_parts(x):
    squash = jax.nn.sigmoid(x)
    return x * squash, squash * (1.0 + x * (1.0 - squash))


def expert_body(
    tp, own, peer, gate_o, gate_p, up_o, up_p, down_o, down_p,
    rows_s, cot_s, active, pre_grad, up_grad, part_o, part_p, acc_o, acc_p,
):
    step = pl.program_id(0)

    @pl.when(step == 0)
    def _():
        for i, got in enumerate((own, peer)):
            rows_s[i, :MAIN] = got[:, 0:HALF]
            cot_s[i, :MAIN] = got[:, HALF : 2 * HALF]
            last_rows, last_cot = unfold_last(got[:, 2 * HALF :])
            rows_s[i, MAIN:] = last_rows
            cot_s[i, MAIN:] = last_cot

    gate_pre = mm(rows_s[0], gate_o[0], NN) + mm(rows_s[1], gate_p[0], NN)
    up_val = mm(rows_s[0], up_o[0], NN) + mm(rows_s[1], up_p[0], NN)
    act_grad = mm(cot_s[0], down_o[0], NT) + mm(cot_s[1], down_p[0], NT)
    act, slope = silu_parts(gate_pre)
    active[...] = (act * up_val).astype(BF)
    up_g = (act_grad * act).astype(BF)
    pre_g = (act_grad * up_val * slope).astype(BF)
    up_grad[...] = up_g
    pre_grad[...] = pre_g
    new_o = mm(pre_g, gate_o[0], NT) + mm(up_g, up_o[0], NT)
    new_p = mm(pre_g, gate_p[0], NT) + mm(up_g, up_p[0], NT)

    @pl.when(step == 0)
    def _():
        acc_o[...] = new_o
        acc_p[...] = new_p

    @pl.when(step == 1)
    def _():
        acc_o[...] += new_o
        acc_p[...] += new_p

    @pl.when(step == 2)
    def _():
        part_o[...] = (acc_o[...] + new_o).astype(BF)
        part_p[...] = (acc_p[...] + new_p).astype(BF)


def expert(tp, own, peer, gate_w, up_w, down_w):
    wide = 2 * HALF + 256
    spec = pltpu.PrefetchScalarGridSpec(
        num_scalar_prefetch=1,
        grid=(FF // FF_STEP,),
        in_specs=[
            whole((MAIN, wide)),
            whole((MAIN, wide)),
            pl.BlockSpec((1, HALF, FF_STEP), lambda i, t: (0, t[0], i)),
            pl.BlockSpec((1, HALF, FF_STEP), lambda i, t: (0, 1 - t[0], i)),
            pl.BlockSpec((1, HALF, FF_STEP), lambda i, t: (0, t[0], i)),
            pl.BlockSpec((1, HALF, FF_STEP), lambda i, t: (0, 1 - t[0], i)),
            pl.BlockSpec((1, FF_STEP, HALF), lambda i, t: (0, i, t[0])),
            pl.BlockSpec((1, FF_STEP, HALF), lambda i, t: (0, i, 1 - t[0])),
        ],
        out_specs=[
            whole((2, SLOTS, HALF)),
            whole((2, SLOTS, HALF)),
            pl.BlockSpec((SLOTS, FF_STEP), lambda i, t: (0, i)),
            pl.BlockSpec((SLOTS, FF_STEP), lambda i, t: (0, i)),
            pl.BlockSpec((SLOTS, FF_STEP), lambda i, t: (0, i)),
            whole((SLOTS, HALF)),
            whole((SLOTS, HALF)),
        ],
        scratch_shapes=[pltpu.VMEM((SLOTS, HALF), F32), pltpu.VMEM((SLOTS, HALF), F32)],
    )
    return call(
        expert_body,
        "expert",
        (
            shape((2, SLOTS, HALF)),
            shape((2, SLOTS, HALF)),
            shape((SLOTS, FF)),
            shape((SLOTS, FF)),
            shape((SLOTS, FF)),
            shape((SLOTS, HALF)),
            shape((SLOTS, HALF)),
        ),
        9_000_000_000,
        grid_spec=spec,
    )(tp, own, peer, gate_w, gate_w, up_w, up_w, down_w, down_w)


def weight_body(tp, rows, cot, active, pre_grad, up_grad, gate_g, up_g, down_g):
    gate_g[0] = mm(rows[0], pre_grad[...], TN).astype(BF)
    up_g[0] = mm(rows[0], up_grad[...], TN).astype(BF)
    down_g[0] = mm(active[...], cot[0], TN).astype(BF)


def weight_grads(tp, rows_s, cot_s, active, pre_grad, up_grad):
    quarter = HALF // 2

    def block(i, t):
        return (t[0] * (1 - i // 2) + (1 - t[0]) * (i // 2)) * 2 + i % 2

    spec = pltpu.PrefetchScalarGridSpec(
        num_scalar_prefetch=1,
        grid=(4,),
        in_specs=[
            pl.BlockSpec((1, SLOTS, quarter), lambda i, t: (i // 2, 0, i % 2)),
            pl.BlockSpec((1, SLOTS, quarter), lambda i, t: (i // 2, 0, i % 2)),
            whole((SLOTS, FF)),
            whole((SLOTS, FF)),
            whole((SLOTS, FF)),
        ],
        out_specs=[
            pl.BlockSpec((1, quarter, FF), lambda i, t: (0, block(i, t), 0)),
            pl.BlockSpec((1, quarter, FF), lambda i, t: (0, block(i, t), 0)),
            pl.BlockSpec((1, FF, quarter), lambda i, t: (0, 0, block(i, t))),
        ],
    )
    return call(
        weight_body,
        "weight_grads",
        (shape((1, WIDTH, FF)), shape((1, WIDTH, FF)), shape((1, FF, WIDTH))),
        5_400_000_000,
        grid_spec=spec,
    )(tp, rows_s, cot_s, active, pre_grad, up_grad)


def reply_body(own, peer, states, out):
    total = (own[...].astype(F32) + peer[...].astype(F32)).astype(BF)
    out[:, 0:HALF] = total[:MAIN]
    out[:, HALF : HALF + 128] = fold_last(total[MAIN:])
    out[:, HALF + 128 :] = states[...]


def reply(own, peer, states):
    return call(reply_body, "reply", shape((MAIN, HALF + 128 + 384)), 100_000_000)(
        own, peer, states
    )


def scan_states(left_in, right_in, decays, out, work):
    def factor(b):
        at = 8 * b
        return decays[at : at + 1] + decays[at + 1 : at + 2] + decays[at + 2 : at + 3]

    factors = [factor(b) for b in range(BLOCKS)]
    left = jnp.zeros((8, 128), F32)
    right = jnp.zeros((8, 128), F32)
    for b in range(BLOCKS):
        at = 8 * b
        work[at : at + 8, 0:128] = left
        left = factors[b] * left + left_in[at : at + 8]
        back = BLOCKS - 1 - b
        at = 8 * back
        work[at : at + 8, 128:256] = right
        right = factors[back] * right + right_in[at : at + 8]
    out[...] = work[...].astype(BF)


def join_body(tp, got, ids, cot, out, states, decays, work, wide):
    first, second = slot_choices(ids[...])
    both = ones_where(first | second)
    (last,) = unfold_last(got[:, HALF : HALF + 128])
    total = mm(both[:, :MAIN], got[:, :HALF], NN) + mm(both[:, MAIN:], last, NN)
    out[...] = (cot[...].astype(F32) + total).astype(BF)
    wide[...] = got[:, HALF + 128 :].astype(F32)
    decays[...] = wide[:, 256:]
    scan_states(wide[:, 0:128], wide[:, 128:256], wide[:, 256:], states, work)


def join(tp, got, ids, cot):
    spec = pltpu.PrefetchScalarGridSpec(
        num_scalar_prefetch=1,
        grid=(1,),
        in_specs=[
            whole((MAIN, HALF + 512)),
            whole((TOK, 2)),
            pl.BlockSpec((TOK, HALF), lambda i, t: (0, t[0])),
        ],
        out_specs=[whole((TOK, HALF)), whole((MAIN, 256)), whole((MAIN, 128))],
        scratch_shapes=[pltpu.VMEM((MAIN, 256), F32), pltpu.VMEM((MAIN, 384), F32)],
    )
    return call(
        join_body,
        "join",
        (shape((TOK, HALF)), shape((MAIN, 256)), shape((MAIN, 128), F32)),
        300_000_000,
        grid_spec=spec,
    )(tp, got, ids, cot)


def mix_body(
    stream, proj_w, gate_in, scan_out, start_w, end_w, out_map, x_states,
    gate_grad, scan_grad, gated, payload,
):
    mixed = mm(stream[0], proj_w[:, :HALF], NT) + mm(stream[1], proj_w[:, HALF:], NT)
    scan = scan_out[...].astype(F32)
    act, slope = silu_parts(gate_in[...].astype(F32))
    gated[...] = (scan * act).astype(BF)
    gate_grad[...] = (mixed * scan * slope).astype(BF)
    grad = (mixed * act).astype(BF)
    scan_grad[...] = grad
    wide = grad.astype(F32)
    block_states(
        payload, (end_w[...] * wide).astype(BF), (start_w[...] * wide).astype(BF), out_map
    )
    payload[:, 256:] = x_states[...]


def mix(*args):
    return call(
        mix_body,
        "mix",
        (shape((TOK, CHAN)), shape((TOK, CHAN)), shape((TOK, CHAN)), shape((MAIN, 512))),
        500_000_000,
    )(*args)


def proj_body(stream, gated, out):
    out[:HALF] = mm(stream[0], gated[...], TN).astype(BF)
    out[HALF:] = mm(stream[1], gated[...], TN).astype(BF)


def proj_part(stream, gated):
    return call(proj_body, "proj_part", shape((WIDTH, CHAN)), 400_000_000)(stream, gated)


def scan_body(got, decays, out, work, wide):
    wide[...] = got[:, 0:256].astype(F32)
    scan_states(wide[:, 0:128], wide[:, 128:256], decays[...], out, work)


def scan_grads(got, decays):
    return call(
        scan_body,
        "scan_grads",
        shape((MAIN, 256)),
        100_000_000,
        scratch_shapes=[pltpu.VMEM((MAIN, 256), F32), pltpu.VMEM((MAIN, 256), F32)],
    )(got, decays)


def near_body(
    scan_grad, values, in_map, out_map, cum, cum_t, start_w, end_w, states,
    out_grad, value_part, in_part,
):
    wide = scan_grad[...].astype(F32)
    from_start = (start_w[...] * wide).astype(BF)
    to_end = (end_w[...] * wide).astype(BF)
    for g in range(2):
        keys = slice(128 * g, 128 * g + 128)
        chan = slice(256 * g, 256 * g + 256)
        in_keys = in_map[:, keys]
        out_keys = out_map[:, keys]
        meet = mm(out_keys, in_keys, NT)
        pair_sum = jnp.zeros((TOK, TOK), F32)
        for e in range(4):
            h = 4 * g + e
            at = slice(64 * h, 64 * h + 64)
            kernel = jnp.exp(-jnp.abs(cum[:, h : h + 1] - cum_t[h : h + 1, :]))
            grad = scan_grad[:, at]
            value_part[:, at] = mm((kernel * meet).astype(BF), grad, TN)
            pair_sum = pair_sum + kernel * mm(grad, values[:, at], NT)
        pair_sum = pair_sum.astype(BF)
        out_total = mm(pair_sum, in_keys, NN)
        out_total = out_total + mm(from_start[:, chan], states[chan, 0:128], NN)
        out_total = out_total + mm(to_end[:, chan], states[chan, 128:256], NN)
        out_grad[:, keys] = out_total.astype(BF)
        in_part[:, keys] = mm(pair_sum, out_keys, TN)


def near(*args):
    return call(
        near_body,
        "near",
        (shape((TOK, KEYS)), shape((TOK, CHAN), F32), shape((TOK, KEYS), F32)),
        600_000_000,
    )(*args)


def far_body(states, values, in_map, start_w, end_w, value_part, in_part, value_grad, in_grad):
    val = values[...].astype(F32)
    from_start = (start_w[...] * val).astype(BF)
    to_end = (end_w[...] * val).astype(BF)
    for g in range(2):
        keys = slice(128 * g, 128 * g + 128)
        chan = slice(256 * g, 256 * g + 256)
        in_keys = in_map[:, keys]
        left = states[chan, 0:128]
        right = states[chan, 128:256]
        total = value_part[:, chan] + start_w[:, chan] * mm(in_keys, left, NT)
        total = total + end_w[:, chan] * mm(in_keys, right, NT)
        value_grad[:, chan] = total.astype(BF)
        total = in_part[:, keys] + mm(from_start[:, chan], left, NN)
        total = total + mm(to_end[:, chan], right, NN)
        in_grad[:, keys] = total.astype(BF)


def far(*args):
    return call(far_body, "far", (shape((TOK, CHAN)), shape((TOK, KEYS))), 200_000_000)(*args)


def swap(rows):
    lanes = rows.shape[1]
    out = lax.all_to_all(rows.reshape(BLOCKS, -1, lanes), SP, 0, 0, tiled=True)
    return out.reshape(-1, lanes)


def other_core(array):
    return lax.ppermute(array, "tp", [(0, 1), (1, 0)])


def on_device(
    stream_rows,
    out_cotangent,
    expert_ids,
    route_weights,
    gate_weight,
    up_weight,
    down_weight,
    proj_weight,
    gate_input,
    scan_out,
    values,
    in_map,
    out_map,
    log_decay,
):
    tp = lax.axis_index("tp").astype(jnp.int32).reshape(1)
    sent = pack(tp, expert_ids, route_weights, stream_rows, out_cotangent)
    own = swap(sent)
    x_payload, start_w, end_w, cum, cum_t = decay(values, in_map, log_decay)
    peer = other_core(own)
    rows_s, cot_s, active, pre_grad, up_grad, part_own, part_peer = expert(
        tp, own, peer, gate_weight, up_weight, down_weight
    )
    back = swap(reply(part_own, other_core(part_peer), x_payload))
    gate_w_grad, up_w_grad, down_grad = weight_grads(
        tp, rows_s, cot_s, active, pre_grad, up_grad
    )
    stream_grad, x_states, decays = join(tp, back, expert_ids, out_cotangent)
    stream = lax.all_gather(stream_grad, "tp")
    gate_grad, scan_grad, gated, payload = mix(
        stream, proj_weight, gate_input, scan_out, start_w, end_w, out_map, x_states
    )
    got = swap(payload)
    g_states = swap(scan_grads(got, decays))
    partial = swap(proj_part(stream, gated))
    proj_grad = jnp.sum(partial.reshape(BLOCKS, 32, CHAN).astype(F32), axis=0)
    out_grad, value_part, in_part = near(
        scan_grad, values, in_map, out_map, cum, cum_t, start_w, end_w, got[:, 256:]
    )
    value_grad, in_grad = far(g_states, values, in_map, start_w, end_w, value_part, in_part)
    return (
        stream_grad,
        proj_grad,
        value_grad,
        in_grad,
        out_grad,
        gate_grad,
        gate_w_grad,
        up_w_grad,
        down_grad,
    )


def solution(mesh):
    finer = Mesh(mesh.devices.reshape(4, 4, 4, mesh.shape["tp"]), ("sp_0", "sp_1", "sp_2", "tp"))
    return jax.shard_map(
        on_device,
        mesh=finer,
        in_specs=(
            P(SP, None),
            P(SP, None),
            P(SP, None),
            P(SP, None),
            P(SP, None, "tp"),
            P(SP, None, "tp"),
            P(SP, "tp", None),
            P("tp", None),
            P(SP, "tp"),
            P(SP, "tp"),
            P(SP, "tp"),
            P(SP, "tp"),
            P(SP, "tp"),
            P(SP, "tp"),
        ),
        out_specs=(
            P(SP, "tp"),
            P(SP, "tp"),
            P(SP, "tp"),
            P(SP, "tp"),
            P(SP, "tp"),
            P(SP, "tp"),
            P(SP, None, "tp"),
            P(SP, None, "tp"),
            P(SP, "tp", None),
        ),
        check_vma=False,
    )
```

time: 538 us -> 194 us (0.36); the launches traced: 529 us -> 193 us
  waiting for transfers between devices: 245 us -> 21.2 us
  matrix products: 56 us -> 0 us
  Pallas kernels: 0 us -> 42.3 us
  local copies, waits for them, and re-layouts: 52.4 us -> 19.5 us
  other arithmetic: 33 us -> 2.54 us
  between operations: 16.8 us -> 0.8 us
  starting transfers between devices: 23.7 us -> 10.4 us
  blocking collectives: 102 us -> 96 us
    all_gather x14 -> x0, waiting for transfers between devices: 202 us -> none  [the longest x12 188 us: entering(): pieces = jax.tree.map(lambda part: lax.all_gather(part, axis), running)]
    dot_general x25 -> x0, matrix products: 56 us -> none  [the longest x1 6.36 us: on_device(): lax.dot_general(row_data, pre_grad, outer_dims, preferred_element_type=jn...]
    pallas_call x0 -> x11, Pallas kernels: none -> 42.3 us  [the longest x1 18.6 us: expert(): call(expert_body, 'expert', (shape((2, SLOTS, HALF)), shape((2, SLOTS, HA...]
    all_gather x6 -> x1, blocking collectives: 43.4 us -> 2.57 us  [on_device(): stream = lax.all_gather(stream_grad, 'tp')]
    all_to_all x2 -> x3, blocking collectives: 58.6 us -> 93.4 us  [swap(): out = lax.all_to_all(rows.reshape(BLOCKS, -1, lanes), SP, 0, 0, tiled=True)]
    reshape x12 -> x0, local copies, waits for them, and re-layouts: 27.3 us -> none  [the longest x1 4.7 us: on_device(): cotangent = got_cot.reshape(-1, width)]
    all_to_all x2, waiting for transfers between devices: 39.8 us -> 16.6 us  [swap(): out = lax.all_to_all(rows.reshape(BLOCKS, -1, lanes), SP, 0, 0, tiled=True)]
    unnamed x108 -> x51, local copies, waits for them, and re-layouts: 4.38 us -> 19.5 us
  transfers between devices with their start and end apart: 16 -> 4, of which waited for: 14 -> 3; matrix products, arithmetic and copies ran while one was open for 14% -> 0% of each run, Pallas kernels for 0% -> 8%
where the time goes in v1:
time: 194 us; the launch traced here: 193 us
  blocking collectives  96 us (49%)
  Pallas kernels  42.3 us (22%)
  waiting for transfers between devices  21.2 us (11%)
  local copies, waits for them, and re-layouts  19.5 us (10%)
  starting transfers between devices  10.4 us (5%)
  other arithmetic  2.54 us (1%)
    all_to_all x3, blocking collectives, swap(): out = lax.all_to_all(rows.reshape(BLOCKS, -1, lanes), SP, 0, 0, tiled=True)  93.4 us
    unnamed x51, local copies, waits for them, and re-layouts  19.5 us
    pallas_call x1, Pallas kernels, expert(): call(expert_body, 'expert', (shape((2, SLOTS, HALF)), shape((2, SLOTS, HA...  18.6 us
    all_to_all x2, waiting for transfers between devices, swap(): out = lax.all_to_all(rows.reshape(BLOCKS, -1, lanes), SP, 0, 0, tiled=True)  16.6 us
    all_to_all x2, starting transfers between devices, swap(): out = lax.all_to_all(rows.reshape(BLOCKS, -1, lanes), SP, 0, 0, tiled=True)  10.3 us
    pallas_call x1, Pallas kernels, weight_grads(): call(weight_body, 'weight_grads', (shape((1, WIDTH, FF)), shape((1, WIDTH...  9.67 us
    ppermute x2, waiting for transfers between devices, other_core(): return lax.ppermute(array, 'tp', [(0, 1), (1, 0)])  4.53 us
  transfers between devices with their start and end apart: 4, of which 3 were waited for; matrix products, arithmetic and copies ran while one was open for 0% of the time, Pallas kernels for 8%

profile of v1, /device:TPU:0, one launch (start us, length us, event | category | flops | bytes accessed | tf_op | source)
XLA Modules:
  0.0 192.8 jit_solution(5248790949754603895)
XLA Ops:
  4.5 1.9 %pack.1 = bf16[512,2304]{1,0:T(8,128)(2,1)S(1)} custom-call(s32[1]{0:T(128)} %bitcast.tp, s32[192,2]{1,0:T(8,128)S(1)} %copy.23.ids, f32[192,2]{1,0:T(8,128)S(1)} %copy.24.weights, bf16[192,2048]{1,0:T(8,128)(2,1)S(1)} %copy-done.3, bf16[192,2048]{1,0:T(8,128)(2,1)S(1)} %copy-done), custom_call_target="tpu_custom_call" | custom-call | flops 1000000000 | bytes 1048576 | tf_op jit(solution)/shard_map/pack/pallas_call | solution.py:125
  6.5 44.4 %all_to_all.25 = bf16[64,8,2304]{2,1,0:T(8,128)(2,1)S(1)} all-to-all(bf16[64,8,2304]{2,1,0:T(8,128)(2,1)S(1)} %bitcast.11), channel_id=1, replica_groups=mesh['sp_0'=4,'sp_1'=4,'sp_2'=4,'tp'=2] {'sp_0','sp_1','sp_2'}, dimensions={0} | all-to-all | bytes 4718592 | tf_op jit(solution)/shard_map/all_to_all | solution.py:486
  50.9 4.5 %collective-permute-done.peer = bf16[512,2304]{1,0:T(8,128)(2,1)S(1)} collective-permute-done((bf16[512,2304]{1,0:T(8,128)(2,1)S(1)}, bf16[512,2304]{1,0:T(8,128)(2,1)S(1)}, u32[]{:S(2)}, u32[]{:S(2)}) %collective-permute-start) | collective-permute-done | bytes 2359328 | tf_op jit(solution)/shard_map/ppermute | solution.py:491
  55.4 18.6 %expert.1 = (bf16[2,576,1024]{2,1,0:T(8,128)(2,1)S(1)}, bf16[2,576,1024]{2,1,0:T(8,128)(2,1)S(1)}, bf16[576,768]{1,0:T(8,128)(2,1)S(1)}, bf16[576,768]{1,0:T(8,1...) custom-call(s32[1]{0:T(128)} %bitcast.tp, ...), custom_call_target="tpu_custom_call" | custom-call | flops 8999999488 | bytes 1048576 | tf_op jit(solution)/shard_map/expert/pallas_call | solution.py:255
  74.0 1.4 copy-done.13
  75.4 1.4 copy-done.15
  82.3 1.5 decay.1
  85.4 30.3 %all_to_all.26 = bf16[64,8,1536]{2,1,0:T(8,128)(2,1)S(1)} all-to-all(bf16[64,8,1536]{2,1,0:T(8,128)(2,1)S(1)} %bitcast.14), channel_id=1, replica_groups=mesh['sp_0'=4,'sp_1'=4,'sp_2'=4,'tp'=2] {'sp_0','sp_1','sp_2'}, dimensions={0} | all-to-all | bytes 3145728 | tf_op jit(solution)/shard_map/all_to_all | solution.py:486
  115.7 1.9 %join.1 = (bf16[192,1024]{1,0:T(8,128)(2,1)}, bf16[512,256]{1,0:T(8,128)(2,1)S(1)}, f32[512,128]{1,0:T(8,128)S(1)}) custom-call(s32[1]{0:T(128)} %bitcast.tp, bf16[512,1536]{1,0:T(8,128)(2,1)S(1)} %bitcast.15, s32[192,2]{1,0:T(8,128)S(1)} %copy.23.ids, bf16[192,2048]{1,0:T(8,128)(2,1)S(1)} %copy-done.1), custom_call_target="tpu_custom_call" | custom-call | flops 300000000 | bytes 1048576 | tf_op jit(solution)/shard_map/join/pallas_call | solution.py:364
  117.6 2.6 %all-gather = bf16[384,1024]{1,0:T(8,128)(2,1)S(1)} all-gather(bf16[192,1024]{1,0:T(8,128)(2,1)} %get-tuple-element.27), channel_id=2, replica_groups=mesh['sp_0'=4,'sp_1'=4,'sp_2'=4,'tp'=2] {'tp'}, dimensions={0}, use_global_device_ids=true | all-gather | bytes 1179648 | tf_op jit(solution)/shard_map/all_gather | solution.py:523
  120.2 1.7 mix.1
  121.9 18.8 %all_to_all.27 = bf16[64,8,512]{2,1,0:T(8,128)(2,1)S(1)} all-to-all(bf16[64,8,512]{2,1,0:T(8,128)(2,1)S(1)} %bitcast.21), channel_id=1, replica_groups=mesh['sp_0'=4,'sp_1'=4,'sp_2'=4,'tp'=2] {'sp_0','sp_1','sp_2'}, dimensions={0} | all-to-all | bytes 1048576 | tf_op jit(solution)/shard_map/all_to_all | solution.py:486
  141.5 4.7 %all-to-all-start.4 = ((bf16[64,8,256]{2,1,0:T(8,128)(2,1)}), bf16[64,8,256]{2,1,0:T(8,128)(2,1)S(1)}, u32[]{:S(2)}, u32[]{:S(2)}) async-start(bf16[64,8,256]{2,1,0:T(8,128)(2,1)} %bitcast.9), calls=%async_computation.4 | async-start | bytes 524288 | tf_op jit(solution)/shard_map/all_to_all | solution.py:486
  146.2 2.1 %proj_part.1 = bf16[2048,512]{1,0:T(8,128)(2,1)} custom-call(bf16[2,192,1024]{2,1,0:T(8,128)(2,1)S(1)} %bitcast.13, bf16[192,512]{1,0:T(8,128)(2,1)S(1)} %get-tuple-element.43.gated), custom_call_target="tpu_custom_call" | custom-call | flops 400000000 | bytes 1048576 | tf_op jit(solution)/shard_map/proj_part/pallas_call | solution.py:406
  148.3 8.5 %all-to-all-done.4 = bf16[64,8,256]{2,1,0:T(8,128)(2,1)S(1)} async-done(((bf16[64,8,256]{2,1,0:T(8,128)(2,1)}), bf16[64,8,256]{2,1,0:T(8,128)(2,1)S(1)}, u32[]{:S(2)}, u32[]{:S(2)}) %all-to-all-start.4) | async-done | bytes 262176 | tf_op jit(solution)/shard_map/all_to_all | solution.py:486
  156.9 5.6 %all-to-all-start.2 = ((bf16[64,32,512]{2,1,0:T(8,128)(2,1)}), bf16[64,32,512]{2,1,0:T(8,128)(2,1)}, u32[]{:S(2)}, u32[]{:S(2)}) async-start(bf16[64,32,512]{2,1,0:T(8,128)(2,1)} %bitcast.6), calls=%async_computation.2 | async-start | bytes 4194304 | tf_op jit(solution)/shard_map/all_to_all | solution.py:486
  162.5 1.7 copy-done.14
  164.1 1.7 copy-done.16
  165.8 1.2 copy-done.18
  166.9 1.2 copy-done.20
  169.3 9.7 %weight_grads.1 = (bf16[1,2048,768]{2,1,0:T(8,128)(2,1)}, bf16[1,2048,768]{2,1,0:T(8,128)(2,1)}, bf16[1,768,2048]{2,1,0:T(8,128)(2,1)}) custom-call(s32[1]{0:T(128)} %bitcast.tp, bf16[2,576,1024]{2,1,0:T(8,128)(2,1)S(1)} %copy-done.14, bf16[2,576,1024]{2,1,0:T(8,128)(2,1)S(1)} %copy-done.16, bf16[576,768]{1,0:T(8,128)(2,1)S(1)} %copy-done.18, ...), custom_call_target="tpu_custom_call" | custom-call | flops 5400000000 | bytes 1048576 | tf_op jit(solution)/shard_map/weight_grads/pallas_call | solution.py:300
  179.0 2.1 %near.1 = (bf16[192,256]{1,0:T(8,128)(2,1)}, f32[192,512]{1,0:T(8,128)S(1)}, f32[192,256]{1,0:T(8,128)S(1)}) custom-call(bf16[192,512]{1,0:T(8,128)(2,1)S(1)} %get-tuple-element.46.scan_grad, bf16[192,512]{1,0:T(8,128)(2,1)S(1)} %copy-done.6, bf16[192,256]{1,0:T(8,128)(2,1)S(1)} %copy-done.10, bf16[192,256]{1,0:T(8,128)(2,1)S(1)} %copy-done.8, ...), custom_call_target="tpu_custom_call" | custom-call | flops 600000000 | bytes 1048576 | tf_op jit(solution)/shard_map/near/pallas_call | solution.py:454
  182.1 8.1 %all-to-all-done.2 = bf16[64,32,512]{2,1,0:T(8,128)(2,1)} async-done(((bf16[64,32,512]{2,1,0:T(8,128)(2,1)}), bf16[64,32,512]{2,1,0:T(8,128)(2,1)}, u32[]{:S(2)}, u32[]{:S(2)}) %all-to-all-start.2) | async-done | bytes 2097184 | tf_op jit(solution)/shard_map/all_to_all | solution.py:486
  190.2 2.5 %convert_reduce_fusion = f32[32,512]{1,0:T(8,128)} fusion(bf16[64,32,512]{2,1,0:T(8,128)(2,1)} %all-to-all-done.2), kind=kLoop, calls=%fused_computation | loop fusion | flops 2080768 | bytes 2162688 | tf_op jit(solution)/shard_map/reduce_sum | solution.py:530
  (52 shorter events, 14.0 us)
Async XLA Ops:
  2.2 1.1 copy-start
  3.4 1.1 copy-start.3
  50.9 28.9 %copy-start.23 = (f32[192,8]{0,1:T(8,128)S(1)}, f32[192,8]{0,1:T(8,128)}, u32[]{:S(2)}) copy-start(f32[192,8]{0,1:T(8,128)} %param.27) | copy-start | bytes 18436
  50.9 29.7 %copy-start.6 = (bf16[192,512]{1,0:T(8,128)(2,1)S(1)}, bf16[192,512]{1,0:T(8,128)(2,1)}, u32[]{:S(2)}) copy-start(bf16[192,512]{1,0:T(8,128)(2,1)} %values.5) | copy-start | bytes 589828
  50.9 4.5 %collective-permute-start = (bf16[512,2304]{1,0:T(8,128)(2,1)S(1)}, bf16[512,2304]{1,0:T(8,128)(2,1)S(1)}, u32[]{:S(2)}, u32[]{:S(2)}) collective-permute-start(bf16[512,2304]{1,0:T(8,128)(2,1)S(1)} %bitcast.18), channel_id=1, source_target_pairs={{0,1},{1,0},{2,3},{3,2},{4,5},{5,4},{6,7},{7,6},{8,9},{9,8},{10,11... | collective-permute-start | bytes 7077896 | tf_op jit(solution)/shard_map/ppermute | solution.py:491
  74.0 1.4 copy-start.13
  75.4 1.4 copy-start.15
  76.8 1.0 copy-start.17
  78.7 0.9 copy-start.21
  79.6 4.8 %collective-permute-start.1 = (bf16[576,1024]{1,0:T(8,128)(2,1)}, bf16[576,1024]{1,0:T(8,128)(2,1)S(1)}, u32[]{:S(2)}, u32[]{:S(2)}) collective-permute-start(bf16[576,1024]{1,0:T(8,128)(2,1)} %get-tuple-element.37), channel_id=1, source_target_pairs={{0,1},{1,0},{2,3},{3,2},{4,5},{5,4},{6,7},{7,6},{8,9},{9,8},{10,11... | collective-permute-start | bytes 3538952 | tf_op jit(solution)/shard_map/ppermute | solution.py:491
  85.4 30.3 %copy-start.1 = (bf16[192,2048]{1,0:T(8,128)(2,1)S(1)}, bf16[192,2048]{1,0:T(8,128)(2,1)}, u32[]{:S(2)}) copy-start(bf16[192,2048]{1,0:T(8,128)(2,1)} %cot.3) | copy-start | bytes 2359300
  115.6 4.5 %copy-start.2 = (bf16[512,2048]{1,0:T(8,128)(2,1)S(1)}, bf16[512,2048]{1,0:T(8,128)(2,1)}, u32[]{:S(2)}) copy-start(bf16[512,2048]{1,0:T(8,128)(2,1)} %proj_w.1) | copy-start | bytes 6291460
  115.6 4.5 %copy-start.4 = (bf16[192,512]{1,0:T(8,128)(2,1)S(1)}, bf16[192,512]{1,0:T(8,128)(2,1)}, u32[]{:S(2)}) copy-start(bf16[192,512]{1,0:T(8,128)(2,1)} %gate_in.1) | copy-start | bytes 589828
  115.6 4.5 %copy-start.5 = (bf16[192,512]{1,0:T(8,128)(2,1)S(1)}, bf16[192,512]{1,0:T(8,128)(2,1)}, u32[]{:S(2)}) copy-start(bf16[192,512]{1,0:T(8,128)(2,1)} %scan_out.1) | copy-start | bytes 589828
  115.6 4.5 %copy-start.8 = (bf16[192,256]{1,0:T(8,128)(2,1)S(1)}, bf16[192,256]{1,0:T(8,128)(2,1)}, u32[]{:S(2)}) copy-start(bf16[192,256]{1,0:T(8,128)(2,1)} %out_map.3) | copy-start | bytes 294916
  141.5 15.3 %all-to-all-start.4 = ((bf16[64,8,256]{2,1,0:T(8,128)(2,1)}), bf16[64,8,256]{2,1,0:T(8,128)(2,1)S(1)}, u32[]{:S(2)}, u32[]{:S(2)}) async-start(bf16[64,8,256]{2,1,0:T(8,128)(2,1)} %bitcast.9), calls=%async_computation.4 | async-start | bytes 524288 | tf_op jit(solution)/shard_map/all_to_all | solution.py:486
  156.9 33.4 %all-to-all-start.2 = ((bf16[64,32,512]{2,1,0:T(8,128)(2,1)}), bf16[64,32,512]{2,1,0:T(8,128)(2,1)}, u32[]{:S(2)}, u32[]{:S(2)}) async-start(bf16[64,32,512]{2,1,0:T(8,128)(2,1)} %bitcast.6), calls=%async_computation.2 | async-start | bytes 4194304 | tf_op jit(solution)/shard_map/all_to_all | solution.py:486
  162.4 1.7 copy-start.14
  164.1 1.7 copy-start.16
  165.8 1.2 copy-start.18
  166.9 1.2 copy-start.20
  168.1 1.2 copy-start.22
  169.3 9.7 %copy-start.10 = (bf16[192,256]{1,0:T(8,128)(2,1)S(1)}, bf16[192,256]{1,0:T(8,128)(2,1)}, u32[]{:S(2)}) copy-start(bf16[192,256]{1,0:T(8,128)(2,1)} %in_map.5) | copy-start | bytes 294916
  169.3 9.7 %copy-start.12 = (f32[192,8]{1,0:T(8,128)S(1)}, f32[192,8]{1,0:T(8,128)}, u32[]{:S(2)}) copy-start(f32[192,8]{1,0:T(8,128)} %copy-done.11) | copy-start | bytes 18436
  (4 other events, 3.4 us)

commit v2 on v1

--- a/solution.py
+++ b/solution.py
@@ -5,6 +5,7 @@
 from jax.experimental.pallas import tpu as pltpu
 from jax.sharding import Mesh
 from jax.sharding import PartitionSpec as P
+
 
 SP = ("sp_0", "sp_1", "sp_2")
 TOK = 192
@@ -42,34 +43,43 @@
     return jnp.where(mask, 1.0, 0.0).astype(BF)
 
 
-def call(body, name, out_shape, flops, **kw):
-    vmem = kw.pop("vmem", 40 << 20)
-    return pl.pallas_call(
+def call(body, out_shape, flops, hbm_in=(), **kw):
+    vmem = kw.pop("vmem", 12 << 20)
+    kernel = pl.pallas_call(
         body,
         out_shape=out_shape,
-        name=name,
         compiler_params=pltpu.CompilerParams(vmem_limit_bytes=vmem),
         cost_estimate=pl.CostEstimate(flops=flops, bytes_accessed=1 << 20, transcendentals=0),
         **kw,
     )
 
+    def run(*args):
+        return kernel(
+            *[
+                pltpu.with_memory_space_constraint(a, pltpu.HBM) if i in hbm_in else a
+                for i, a in enumerate(args)
+            ]
+        )
+
+    return run
+
 
 def shape(dims, dtype=BF):
     return jax.ShapeDtypeStruct(dims, dtype)
 
 
 def slot_choices(ids):
-    lane = iota((TOK, EXPERTS), 1)
-    named = [ids[:, k : k + 1] == lane for k in range(2)]
+    expert = iota((EXPERTS, TOK), 0)
+    named = [ids[k : k + 1] == expert for k in range(2)]
     either = ones_where(named[0] | named[1])
-    earlier = ones_where(iota((TOK, TOK), 1) < iota((TOK, TOK), 0))
-    count = mm(earlier, either, NN)
+    earlier = ones_where(iota((TOK, TOK), 0) < iota((TOK, TOK), 1))
+    count = mm(either, earlier, NN)
     picks = []
     for k in range(2):
-        rank = jnp.sum(jnp.where(named[k], count, 0.0), axis=1, keepdims=True).astype(jnp.int32)
-        own = ids[:, k : k + 1]
+        rank = jnp.sum(jnp.where(named[k], count, 0.0), axis=0, keepdims=True).astype(jnp.int32)
+        own = ids[k : k + 1]
         row = jnp.where(rank < 8, own * 8 + rank, MAIN + own)
-        picks.append(row == iota((TOK, SLOTS), 1))
+        picks.append(row == iota((SLOTS, TOK), 0))
     return picks
 
 
@@ -92,17 +102,29 @@
     ]
 
 
-def pack_body(tp, ids, weights, rows, cot, out):
+def pack_body(tp, ids, weights, rows_hbm, cot_hbm, out, rows, cot, sems):
+    at = pl.ds(pl.multiple_of(tp[0] * HALF, HALF), HALF)
+    get_rows = pltpu.make_async_copy(rows_hbm.at[:, at], rows, sems.at[0])
+    get_cot = pltpu.make_async_copy(cot_hbm.at[:, at], cot, sems.at[1])
+    get_rows.start()
+    get_cot.start()
     first, second = slot_choices(ids[...])
     both = ones_where(first | second)
-    row_slots = mm(both, rows[...], TN).astype(BF)
+    same = iota((TOK, TOK), 0) == iota((TOK, TOK), 1)
+
+    def column(k):
+        return jnp.sum(jnp.where(same, weights[k : k + 1], 0.0), axis=1, keepdims=True)
+
+    get_rows.wait()
+    row_slots = mm(both, rows[...], NN).astype(BF)
+    out[:, 0:HALF] = row_slots[:MAIN]
+    out[:, 2 * HALF : 2 * HALF + 128] = fold_last(row_slots[MAIN:])
+    get_cot.wait()
     full = cot[...].astype(F32)
-    cot_slots = mm(ones_where(first), (weights[:, 0:1] * full).astype(BF), TN)
-    cot_slots = cot_slots + mm(ones_where(second), (weights[:, 1:2] * full).astype(BF), TN)
+    cot_slots = mm(ones_where(first), (column(0) * full).astype(BF), NN)
+    cot_slots = cot_slots + mm(ones_where(second), (column(1) * full).astype(BF), NN)
     cot_slots = cot_slots.astype(BF)
-    out[:, 0:HALF] = row_slots[:MAIN]
     out[:, HALF : 2 * HALF] = cot_slots[:MAIN]
-    out[:, 2 * HALF : 2 * HALF + 128] = fold_last(row_slots[MAIN:])
     out[:, 2 * HALF + 128 :] = fold_last(cot_slots[MAIN:])
 
 
@@ -115,22 +137,27 @@
         num_scalar_prefetch=1,
         grid=(1,),
         in_specs=[
-            whole((TOK, 2)),
-            whole((TOK, 2)),
-            pl.BlockSpec((TOK, HALF), lambda i, t: (0, t[0])),
-            pl.BlockSpec((TOK, HALF), lambda i, t: (0, t[0])),
+            whole((2, TOK)),
+            whole((2, TOK)),
+            pl.BlockSpec(memory_space=pltpu.HBM),
+            pl.BlockSpec(memory_space=pltpu.HBM),
         ],
         out_specs=whole((MAIN, 2 * HALF + 256)),
-    )
-    return call(
-        pack_body, "pack", shape((MAIN, 2 * HALF + 256)), 1_000_000_000, grid_spec=spec
+        scratch_shapes=[
+            pltpu.VMEM((TOK, HALF), BF),
+            pltpu.VMEM((TOK, HALF), BF),
+            pltpu.SemaphoreType.DMA((2,)),
+        ],
+    )
+    return call(
+        pack_body, shape((MAIN, 2 * HALF + 256)), 1_000_000_000, hbm_in=(1, 2, 3, 4), grid_spec=spec
     )(tp, ids, weights, rows, cot)
 
 
 def decay_body(values, in_map, log_decay, payload, start_w, end_w, cum_out, cum_t_out):
-    upto = jnp.where(iota((TOK, TOK), 1) <= iota((TOK, TOK), 0), 1.0, 0.0)
-    cum = mm(upto, log_decay[...], NN, EXACT)
-    cum_t = mm(log_decay[...], upto, ((0,), (1,)), EXACT)
+    upto = jnp.where(iota((TOK, TOK), 0) <= iota((TOK, TOK), 1), 1.0, 0.0)
+    cum = mm(upto, log_decay[...], ((0,), (1,)), EXACT)
+    cum_t = mm(log_decay[...], upto, NN, EXACT)
     cum_out[...] = cum
     cum_t_out[...] = cum_t
     spread = jnp.where(iota((HEADS, CHAN), 1) // 64 == iota((HEADS, CHAN), 0), 1.0, 0.0)
@@ -166,7 +193,6 @@
 def decay(values, in_map, log_decay):
     return call(
         decay_body,
-        "decay",
         (
             shape((MAIN, 384)),
             shape((TOK, CHAN), F32),
@@ -179,118 +205,157 @@
 
 
 def silu_parts(x):
-    squash = jax.nn.sigmoid(x)
+    squash = 0.5 * jnp.tanh(0.5 * x) + 0.5
     return x * squash, squash * (1.0 + x * (1.0 - squash))
 
 
-def expert_body(
-    tp, own, peer, gate_o, gate_p, up_o, up_p, down_o, down_p,
-    rows_s, cot_s, active, pre_grad, up_grad, part_o, part_p, acc_o, acc_p,
+def split_slots(got, rows, cot):
+    rows[:MAIN] = got[:, 0:HALF]
+    cot[:MAIN] = got[:, HALF : 2 * HALF]
+    last_rows, last_cot = unfold_last(got[:, 2 * HALF :])
+    rows[MAIN:] = last_rows
+    cot[MAIN:] = last_cot
+
+
+def own_body(tp, own, gate_w, up_w, down_w, rows, cot, gate_o, up_o, act_o):
+    @pl.when(pl.program_id(0) == 0)
+    def _():
+        split_slots(own, rows, cot)
+
+    gate_o[...] = mm(rows[...], gate_w[0], NN)
+    up_o[...] = mm(rows[...], up_w[0], NN)
+    act_o[...] = mm(cot[...], down_w[0], NT)
+
+
+def step_block(dims):
+    return pl.BlockSpec(dims, lambda i, t: (0, i))
+
+
+def expert_own(tp, own, gate_w, up_w, down_w):
+    spec = pltpu.PrefetchScalarGridSpec(
+        num_scalar_prefetch=1,
+        grid=(FF // FF_STEP,),
+        in_specs=[
+            whole((MAIN, 2 * HALF + 256)),
+            pl.BlockSpec((1, HALF, FF_STEP), lambda i, t: (0, t[0], i)),
+            pl.BlockSpec((1, HALF, FF_STEP), lambda i, t: (0, t[0], i)),
+            pl.BlockSpec((1, FF_STEP, HALF), lambda i, t: (0, i, t[0])),
+        ],
+        out_specs=[whole((SLOTS, HALF))] * 2 + [step_block((SLOTS, FF_STEP))] * 3,
+    )
+    return call(
+        own_body,
+        [shape((SLOTS, HALF))] * 2 + [shape((SLOTS, FF), F32)] * 3,
+        2_700_000_000,
+        hbm_in=(2, 3, 4),
+        grid_spec=spec,
+        vmem=24 << 20,
+    )(tp, own, gate_w, up_w, down_w)
+
+
+def peer_body(
+    tp, peer, gate_w, up_w, down_w, gate_o, up_o, act_o,
+    rows, cot, active, pre_grad, up_grad, part, acc,
 ):
     step = pl.program_id(0)
 
     @pl.when(step == 0)
     def _():
-        for i, got in enumerate((own, peer)):
-            rows_s[i, :MAIN] = got[:, 0:HALF]
-            cot_s[i, :MAIN] = got[:, HALF : 2 * HALF]
-            last_rows, last_cot = unfold_last(got[:, 2 * HALF :])
-            rows_s[i, MAIN:] = last_rows
-            cot_s[i, MAIN:] = last_cot
-
-    gate_pre = mm(rows_s[0], gate_o[0], NN) + mm(rows_s[1], gate_p[0], NN)
-    up_val = mm(rows_s[0], up_o[0], NN) + mm(rows_s[1], up_p[0], NN)
-    act_grad = mm(cot_s[0], down_o[0], NT) + mm(cot_s[1], down_p[0], NT)
+        split_slots(peer, rows, cot)
+
+    gate_pre = gate_o[...] + mm(rows[...], gate_w[0], NN)
+    up_val = up_o[...] + mm(rows[...], up_w[0], NN)
+    act_grad = act_o[...] + mm(cot[...], down_w[0], NT)
     act, slope = silu_parts(gate_pre)
     active[...] = (act * up_val).astype(BF)
     up_g = (act_grad * act).astype(BF)
     pre_g = (act_grad * up_val * slope).astype(BF)
     up_grad[...] = up_g
     pre_grad[...] = pre_g
-    new_o = mm(pre_g, gate_o[0], NT) + mm(up_g, up_o[0], NT)
-    new_p = mm(pre_g, gate_p[0], NT) + mm(up_g, up_p[0], NT)
+    new = mm(pre_g, gate_w[0], NT) + mm(up_g, up_w[0], NT)
 
     @pl.when(step == 0)
     def _():
-        acc_o[...] = new_o
-        acc_p[...] = new_p
+        acc[...] = new
 
     @pl.when(step == 1)
     def _():
-        acc_o[...] += new_o
-        acc_p[...] += new_p
+        acc[...] += new
 
     @pl.when(step == 2)
     def _():
-        part_o[...] = (acc_o[...] + new_o).astype(BF)
-        part_p[...] = (acc_p[...] + new_p).astype(BF)
-
-
-def expert(tp, own, peer, gate_w, up_w, down_w):
-    wide = 2 * HALF + 256
+        part[...] = (acc[...] + new).astype(BF)
+
+
+def expert_peer(tp, peer, gate_w, up_w, down_w, gate_o, up_o, act_o):
     spec = pltpu.PrefetchScalarGridSpec(
         num_scalar_prefetch=1,
         grid=(FF // FF_STEP,),
         in_specs=[
-            whole((MAIN, wide)),
-            whole((MAIN, wide)),
-            pl.BlockSpec((1, HALF, FF_STEP), lambda i, t: (0, t[0], i)),
+            whole((MAIN, 2 * HALF + 256)),
             pl.BlockSpec((1, HALF, FF_STEP), lambda i, t: (0, 1 - t[0], i)),
-            pl.BlockSpec((1, HALF, FF_STEP), lambda i, t: (0, t[0], i)),
             pl.BlockSpec((1, HALF, FF_STEP), lambda i, t: (0, 1 - t[0], i)),
-            pl.BlockSpec((1, FF_STEP, HALF), lambda i, t: (0, i, t[0])),
             pl.BlockSpec((1, FF_STEP, HALF), lambda i, t: (0, i, 1 - t[0])),
-        ],
-        out_specs=[
-            whole((2, SLOTS, HALF)),
-            whole((2, SLOTS, HALF)),
-            pl.BlockSpec((SLOTS, FF_STEP), lambda i, t: (0, i)),
-            pl.BlockSpec((SLOTS, FF_STEP), lambda i, t: (0, i)),
-            pl.BlockSpec((SLOTS, FF_STEP), lambda i, t: (0, i)),
-            whole((SLOTS, HALF)),
-            whole((SLOTS, HALF)),
-        ],
-        scratch_shapes=[pltpu.VMEM((SLOTS, HALF), F32), pltpu.VMEM((SLOTS, HALF), F32)],
-    )
-    return call(
-        expert_body,
-        "expert",
-        (
-            shape((2, SLOTS, HALF)),
-            shape((2, SLOTS, HALF)),
-            shape((SLOTS, FF)),
-            shape((SLOTS, FF)),
-            shape((SLOTS, FF)),
-            shape((SLOTS, HALF)),
-            shape((SLOTS, HALF)),
-        ),
-        9_000_000_000,
+        ]
+        + [step_block((SLOTS, FF_STEP))] * 3,
+        out_specs=[whole((SLOTS, HALF))] * 2
+        + [step_block((SLOTS, FF_STEP))] * 3
+        + [whole((SLOTS, HALF))],
+        scratch_shapes=[pltpu.VMEM((SLOTS, HALF), F32)],
+    )
+    return call(
+        peer_body,
+        [shape((SLOTS, HALF))] * 2 + [shape((SLOTS, FF))] * 3 + [shape((SLOTS, HALF))],
+        4_500_000_000,
+        hbm_in=(2, 3, 4),
         grid_spec=spec,
-    )(tp, own, peer, gate_w, gate_w, up_w, up_w, down_w, down_w)
-
-
-def weight_body(tp, rows, cot, active, pre_grad, up_grad, gate_g, up_g, down_g):
-    gate_g[0] = mm(rows[0], pre_grad[...], TN).astype(BF)
-    up_g[0] = mm(rows[0], up_grad[...], TN).astype(BF)
-    down_g[0] = mm(active[...], cot[0], TN).astype(BF)
-
-
-def weight_grads(tp, rows_s, cot_s, active, pre_grad, up_grad):
-    quarter = HALF // 2
-
-    def block(i, t):
-        return (t[0] * (1 - i // 2) + (1 - t[0]) * (i // 2)) * 2 + i % 2
-
+        vmem=28 << 20,
+    )(tp, peer, gate_w, up_w, down_w, gate_o, up_o, act_o)
+
+
+def rows_body(tp, pre_grad, up_grad, gate_w, up_w, part):
+    total = mm(pre_grad[...], gate_w[0], NT) + mm(up_grad[...], up_w[0], NT)
+    part[...] = total.astype(BF)
+
+
+def own_rows(tp, pre_grad, up_grad, gate_w, up_w):
     spec = pltpu.PrefetchScalarGridSpec(
         num_scalar_prefetch=1,
         grid=(4,),
         in_specs=[
-            pl.BlockSpec((1, SLOTS, quarter), lambda i, t: (i // 2, 0, i % 2)),
-            pl.BlockSpec((1, SLOTS, quarter), lambda i, t: (i // 2, 0, i % 2)),
             whole((SLOTS, FF)),
             whole((SLOTS, FF)),
-            whole((SLOTS, FF)),
+            pl.BlockSpec((1, HALF // 4, FF), lambda i, t: (0, 4 * t[0] + i, 0)),
+            pl.BlockSpec((1, HALF // 4, FF), lambda i, t: (0, 4 * t[0] + i, 0)),
         ],
+        out_specs=step_block((SLOTS, HALF // 4)),
+    )
+    return call(
+        rows_body, shape((SLOTS, HALF)), 1_800_000_000, grid_spec=spec, vmem=12 << 20
+    )(tp, pre_grad, up_grad, gate_w, up_w)
+
+
+def weight_body(tp, rows_o, cot_o, rows_p, cot_p, active, pre_grad, up_grad, gate_g, up_g, down_g):
+    for half, rows, cot in ((0, rows_o, cot_o), (1, rows_p, cot_p)):
+
+        @pl.when(pl.program_id(0) // 2 == half)
+        def _():
+            gate_g[0] = mm(rows[...], pre_grad[...], TN).astype(BF)
+            up_g[0] = mm(rows[...], up_grad[...], TN).astype(BF)
+            down_g[0] = mm(active[...], cot[...], TN).astype(BF)
+
+
+def weight_grads(tp, rows_o, cot_o, rows_p, cot_p, active, pre_grad, up_grad):
+    quarter = HALF // 2
+
+    def block(i, t):
+        return (t[0] * (1 - i // 2) + (1 - t[0]) * (i // 2)) * 2 + i % 2
+
+    spec = pltpu.PrefetchScalarGridSpec(
+        num_scalar_prefetch=1,
+        grid=(4,),
+        in_specs=[pl.BlockSpec((SLOTS, quarter), lambda i, t: (0, i % 2))] * 4
+        + [whole((SLOTS, FF))] * 3,
         out_specs=[
             pl.BlockSpec((1, quarter, FF), lambda i, t: (0, block(i, t), 0)),
             pl.BlockSpec((1, quarter, FF), lambda i, t: (0, block(i, t), 0)),
@@ -299,11 +364,11 @@
     )
     return call(
         weight_body,
-        "weight_grads",
         (shape((1, WIDTH, FF)), shape((1, WIDTH, FF)), shape((1, FF, WIDTH))),
         5_400_000_000,
         grid_spec=spec,
-    )(tp, rows_s, cot_s, active, pre_grad, up_grad)
+        vmem=24 << 20,
+    )(tp, rows_o, cot_o, rows_p, cot_p, active, pre_grad, up_grad)
 
 
 def reply_body(own, peer, states, out):
@@ -314,9 +379,7 @@
 
 
 def reply(own, peer, states):
-    return call(reply_body, "reply", shape((MAIN, HALF + 128 + 384)), 100_000_000)(
-        own, peer, states
-    )
+    return call(reply_body, shape((MAIN, HALF + 128 + 384)), 100_000_000)(own, peer, states)
 
 
 def scan_states(left_in, right_in, decays, out, work):
@@ -335,14 +398,14 @@
         at = 8 * back
         work[at : at + 8, 128:256] = right
         right = factors[back] * right + right_in[at : at + 8]
-    out[...] = work[...].astype(BF)
+    out[:, 0:256] = work[...].astype(BF)
 
 
 def join_body(tp, got, ids, cot, out, states, decays, work, wide):
     first, second = slot_choices(ids[...])
     both = ones_where(first | second)
     (last,) = unfold_last(got[:, HALF : HALF + 128])
-    total = mm(both[:, :MAIN], got[:, :HALF], NN) + mm(both[:, MAIN:], last, NN)
+    total = mm(both[:MAIN], got[:, :HALF], TN) + mm(both[MAIN:], last, TN)
     out[...] = (cot[...].astype(F32) + total).astype(BF)
     wide[...] = got[:, HALF + 128 :].astype(F32)
     decays[...] = wide[:, 256:]
@@ -355,7 +418,7 @@
         grid=(1,),
         in_specs=[
             whole((MAIN, HALF + 512)),
-            whole((TOK, 2)),
+            whole((2, TOK)),
             pl.BlockSpec((TOK, HALF), lambda i, t: (0, t[0])),
         ],
         out_specs=[whole((TOK, HALF)), whole((MAIN, 256)), whole((MAIN, 128))],
@@ -363,7 +426,6 @@
     )
     return call(
         join_body,
-        "join",
         (shape((TOK, HALF)), shape((MAIN, 256)), shape((MAIN, 128), F32)),
         300_000_000,
         grid_spec=spec,
@@ -391,34 +453,67 @@
 def mix(*args):
     return call(
         mix_body,
-        "mix",
         (shape((TOK, CHAN)), shape((TOK, CHAN)), shape((TOK, CHAN)), shape((MAIN, 512))),
         500_000_000,
     )(*args)
 
 
-def proj_body(stream, gated, out):
-    out[:HALF] = mm(stream[0], gated[...], TN).astype(BF)
-    out[HALF:] = mm(stream[1], gated[...], TN).astype(BF)
-
-
-def proj_part(stream, gated):
-    return call(proj_body, "proj_part", shape((WIDTH, CHAN)), 400_000_000)(stream, gated)
-
-
-def scan_body(got, decays, out, work, wide):
+PARTS = ((0, 384), (768, 384), (1536, 256))
+
+
+def proj_body(odd, stream, gated, keep, *sends):
+    for i in range(2):
+        part = mm(stream[i], gated[...], TN).reshape(32, 4, 8, CHAN)
+        flat = [part[:, q].reshape(256, CHAN) for q in range(4)]
+        rows = slice(256 * i, 256 * i + 256)
+
+        def tile(t):
+            return flat[t // 4][:, 128 * (t % 4) : 128 * (t % 4) + 128]
+
+        at = 0
+        for j, (first, width) in enumerate(PARTS):
+            for k in range(width // 128):
+                low = tile(first // 128 + k)
+                high = tile((first + width) // 128 + k)
+                upper = odd[j] == 1
+                keep[rows, at : at + 128] = jnp.where(upper, high, low).astype(BF)
+                sends[j][rows, 128 * k : 128 * k + 128] = jnp.where(upper, low, high).astype(BF)
+                at += 128
+
+
+def proj_part(odd, stream, gated):
+    out = [shape((MAIN, 1024))] + [shape((MAIN, width)) for _, width in PARTS]
+    spec = pltpu.PrefetchScalarGridSpec(
+        num_scalar_prefetch=1,
+        grid=(1,),
+        in_specs=[whole((2, TOK, HALF)), whole((TOK, CHAN))],
+        out_specs=[whole(o.shape) for o in out],
+    )
+    return call(proj_body, out, 400_000_000, grid_spec=spec)(odd, stream, gated)
+
+
+def scan_body(got, decays, keep, first, second, third, out, work, wide):
+    at = 0
+    for other in (first, second, third):
+        width = other.shape[1]
+        total = keep[:, at : at + width].astype(F32) + other[...].astype(F32)
+        out[:, 256 + at : 256 + at + width] = total.astype(BF)
+        at += width
     wide[...] = got[:, 0:256].astype(F32)
     scan_states(wide[:, 0:128], wide[:, 128:256], decays[...], out, work)
 
 
-def scan_grads(got, decays):
-    return call(
-        scan_body,
-        "scan_grads",
-        shape((MAIN, 256)),
-        100_000_000,
+def scan_grads(got, decays, keep, others):
+    spec = pl.GridSpec(
+        grid=(1,),
+        in_specs=[whole((MAIN, 512)), whole((MAIN, 128)), whole((MAIN, 1024))]
+        + [whole(o.shape) for o in others],
+        out_specs=whole((MAIN, 256 + 1024)),
         scratch_shapes=[pltpu.VMEM((MAIN, 256), F32), pltpu.VMEM((MAIN, 256), F32)],
-    )(got, decays)
+    )
+    return call(
+        scan_body, shape((MAIN, 256 + 1024)), 100_000_000, grid_spec=spec
+    )(got, decays, keep, *others)
 
 
 def near_body(
@@ -453,13 +548,41 @@
 def near(*args):
     return call(
         near_body,
-        "near",
         (shape((TOK, KEYS)), shape((TOK, CHAN), F32), shape((TOK, KEYS), F32)),
         600_000_000,
     )(*args)
 
 
-def far_body(states, values, in_map, start_w, end_w, value_part, in_part, value_grad, in_grad):
+def far_body(
+    states, values_h, in_map_h, start_h, end_h, value_part_h, in_part_h,
+    value_grad, in_grad, proj_grad,
+    values, in_map, start_w, end_w, value_part, in_part, sems,
+):
+    pairs = (
+        (values_h, values),
+        (in_map_h, in_map),
+        (start_h, start_w),
+        (end_h, end_w),
+        (value_part_h, value_part),
+        (in_part_h, in_part),
+    )
+    copies = [pltpu.make_async_copy(a, b, sems.at[i]) for i, (a, b) in enumerate(pairs)]
+    for c in copies:
+        c.start()
+    at = 256
+    for j, (first, width) in enumerate(PARTS):
+        sums = [jnp.zeros((8, width), F32), jnp.zeros((8, width), F32)]
+        for b in range(BLOCKS):
+            half = (b >> (4 - 2 * j)) & 1
+            sums[half] = sums[half] + states[8 * b : 8 * b + 8, at : at + width].astype(F32)
+        at += width
+        for half in range(2):
+            for k in range(width // 128):
+                tile = (first + half * width) // 128 + k
+                q, lane = 8 * (tile // 4), 128 * (tile % 4)
+                proj_grad[q : q + 8, lane : lane + 128] = sums[half][:, 128 * k : 128 * k + 128]
+    for c in copies:
+        c.wait()
     val = values[...].astype(F32)
     from_start = (start_w[...] * val).astype(BF)
     to_end = (end_w[...] * val).astype(BF)
@@ -478,7 +601,22 @@
 
 
 def far(*args):
-    return call(far_body, "far", (shape((TOK, CHAN)), shape((TOK, KEYS))), 200_000_000)(*args)
+    far_out = (shape((TOK, CHAN)), shape((TOK, KEYS)), shape((32, CHAN), F32))
+    spec = pl.GridSpec(
+        grid=(1,),
+        in_specs=[whole((MAIN, 256 + 1024))] + [pl.BlockSpec(memory_space=pltpu.HBM)] * 6,
+        out_specs=[whole(o.shape) for o in far_out],
+        scratch_shapes=[
+            pltpu.VMEM((TOK, CHAN), BF),
+            pltpu.VMEM((TOK, KEYS), BF),
+            pltpu.VMEM((TOK, CHAN), F32),
+            pltpu.VMEM((TOK, CHAN), F32),
+            pltpu.VMEM((TOK, CHAN), F32),
+            pltpu.VMEM((TOK, KEYS), F32),
+            pltpu.SemaphoreType.DMA((6,)),
+        ],
+    )
+    return call(far_body, far_out, 200_000_000, hbm_in=range(1, 7), grid_spec=spec)(*args)
 
 
 def swap(rows):
@@ -508,30 +646,40 @@
     log_decay,
 ):
     tp = lax.axis_index("tp").astype(jnp.int32).reshape(1)
-    sent = pack(tp, expert_ids, route_weights, stream_rows, out_cotangent)
+    ids = expert_ids.T
+    sent = pack(tp, ids, route_weights.T, stream_rows, out_cotangent)
     own = swap(sent)
-    x_payload, start_w, end_w, cum, cum_t = decay(values, in_map, log_decay)
+    x_payload, start_w, end_w, cum, cum_t = decay(values, in_map, log_decay.T)
     peer = other_core(own)
-    rows_s, cot_s, active, pre_grad, up_grad, part_own, part_peer = expert(
-        tp, own, peer, gate_weight, up_weight, down_weight
-    )
-    back = swap(reply(part_own, other_core(part_peer), x_payload))
+    rows_o, cot_o, *pre = expert_own(tp, own, gate_weight, up_weight, down_weight)
+    rows_p, cot_p, active, pre_grad, up_grad, part_peer = expert_peer(
+        tp, peer, gate_weight, up_weight, down_weight, *pre
+    )
+    part_in = other_core(part_peer)
+    part_own = own_rows(tp, pre_grad, up_grad, gate_weight, up_weight)
+    sent_back = reply(part_own, part_in, x_payload)
+    back = swap(sent_back)
     gate_w_grad, up_w_grad, down_grad = weight_grads(
-        tp, rows_s, cot_s, active, pre_grad, up_grad
-    )
-    stream_grad, x_states, decays = join(tp, back, expert_ids, out_cotangent)
+        tp, rows_o, cot_o, rows_p, cot_p, active, pre_grad, up_grad
+    )
+    stream_grad, x_states, decays = join(tp, back, ids, out_cotangent)
     stream = lax.all_gather(stream_grad, "tp")
     gate_grad, scan_grad, gated, payload = mix(
         stream, proj_weight, gate_input, scan_out, start_w, end_w, out_map, x_states
     )
     got = swap(payload)
-    g_states = swap(scan_grads(got, decays))
-    partial = swap(proj_part(stream, gated))
-    proj_grad = jnp.sum(partial.reshape(BLOCKS, 32, CHAN).astype(F32), axis=0)
+    odd = jnp.stack([lax.axis_index(name) & 1 for name in SP]).astype(jnp.int32)
+    keep, *halves = proj_part(odd, stream, gated)
+    pair = [(0, 1), (1, 0), (2, 3), (3, 2)]
+    others = [lax.ppermute(h, name, pair) for h, name in zip(halves, SP)]
+    buffer = scan_grads(got, decays, keep, others)
+    g_states = swap(buffer)
     out_grad, value_part, in_part = near(
         scan_grad, values, in_map, out_map, cum, cum_t, start_w, end_w, got[:, 256:]
     )
-    value_grad, in_grad = far(g_states, values, in_map, start_w, end_w, value_part, in_part)
+    value_grad, in_grad, proj_grad = far(
+        g_states, values, in_map, start_w, end_w, value_part, in_part
+    )
     return (
         stream_grad,
         proj_grad,

time: 194 us -> 176 us (0.907)
  blocking collectives: 96 us -> 47 us
  waiting for transfers between devices: 21.2 us -> 36 us
  starting transfers between devices: 10.4 us -> 24.6 us
  Pallas kernels: 42.3 us -> 49.8 us
  local copies, waits for them, and re-layouts: 19.5 us -> 16 us
  other arithmetic: 2.54 us -> 0.08 us
    all_to_all x3 -> x1, blocking collectives: 93.4 us -> 44.4 us  [swap(): out = lax.all_to_all(rows.reshape(BLOCKS, -1, lanes), SP, 0, 0, tiled=True)]
    ppermute x0 -> x3, waiting for transfers between devices: none -> 10.8 us  [on_device(): others = [lax.ppermute(h, name, pair) for h, name in zip(halves, SP)]]
    all_to_all x2 -> x3, starting transfers between devices: 10.3 us -> 19.5 us  [swap(): out = lax.all_to_all(rows.reshape(BLOCKS, -1, lanes), SP, 0, 0, tiled=True)]
    all_to_all x2 -> x3, waiting for transfers between devices: 16.6 us -> 25.3 us  [swap(): out = lax.all_to_all(rows.reshape(BLOCKS, -1, lanes), SP, 0, 0, tiled=True)]
    pallas_call x11 -> x13, Pallas kernels: 42.3 us -> 49.8 us  [run(): kernel(*[pltpu.with_memory_space_constraint(a, pltpu.HBM) if i in hbm_in...]
    ppermute x2, waiting for transfers between devices: 4.53 us -> 0.01 us  [other_core(): return lax.ppermute(array, 'tp', [(0, 1), (1, 0)])]
    ppermute x0 -> x3, starting transfers between devices: none -> 4.52 us  [on_device(): others = [lax.ppermute(h, name, pair) for h, name in zip(halves, SP)]]
    unnamed x51 -> x74, local copies, waits for them, and re-layouts: 19.5 us -> 15.9 us
  transfers between devices with their start and end apart: 4 -> 8, of which waited for: 3 -> 3; matrix products, arithmetic and copies ran while one was open for 0% -> 0% of each run, Pallas kernels for 8% -> 14%
where the time goes in v2:
time: 176 us; the launch traced here: 175 us
  Pallas kernels  49.8 us (28%)
  blocking collectives  47 us (27%)
  waiting for transfers between devices  36 us (20%)
  starting transfers between devices  24.6 us (14%)
  local copies, waits for them, and re-layouts  16 us (9%)
    pallas_call x13, Pallas kernels, run(): kernel(*[pltpu.with_memory_space_constraint(a, pltpu.HBM) if i in hbm_in...  49.8 us
    all_to_all x1, blocking collectives, swap(): out = lax.all_to_all(rows.reshape(BLOCKS, -1, lanes), SP, 0, 0, tiled=True)  44.4 us
    all_to_all x3, waiting for transfers between devices, swap(): out = lax.all_to_all(rows.reshape(BLOCKS, -1, lanes), SP, 0, 0, tiled=True)  25.3 us
    all_to_all x3, starting transfers between devices, swap(): out = lax.all_to_all(rows.reshape(BLOCKS, -1, lanes), SP, 0, 0, tiled=True)  19.5 us
    unnamed x74, local copies, waits for them, and re-layouts  15.9 us
    ppermute x3, waiting for transfers between devices, on_device(): others = [lax.ppermute(h, name, pair) for h, name in zip(halves, SP)]  10.8 us
    ppermute x3, starting transfers between devices, on_device(): others = [lax.ppermute(h, name, pair) for h, name in zip(halves, SP)]  4.52 us
  transfers between devices with their start and end apart: 8, of which 3 were waited for; matrix products, arithmetic and copies ran while one was open for 0% of the time, Pallas kernels for 14%

profile of v2, /device:TPU:0, one launch (start us, length us, event | category | flops | bytes accessed | tf_op | source)
XLA Modules:
  0.0 174.6 jit_solution(1690112187983606054)
XLA Ops:
  0.6 3.9 %shard_map.205 = bf16[512,2304]{1,0:T(8,128)(2,1)S(1)} custom-call(s32[1]{0:T(128)} %bitcast.tp, s32[2,192]{1,0:T(2,128)} %bitcast.25, f32[2,192]{1,0:T(2,128)} %bitcast.28, bf16[192,2048]{1,0:T(8,128)(2,1)} %rows_hbm.1, bf16[192,2048]{1,0:T(8,128)(2,1)} %cot.1), custom_call_target="tpu_custom_call" | custom-call | flops 1000000000 | bytes 1048576 | tf_op jit(solution)/shard_map/pallas_call | solution.py:57
  4.6 44.4 %all_to_all.20 = bf16[64,8,2304]{2,1,0:T(8,128)(2,1)S(1)} all-to-all(bf16[64,8,2304]{2,1,0:T(8,128)(2,1)S(1)} %bitcast.16), channel_id=1, replica_groups=mesh['sp_0'=4,'sp_1'=4,'sp_2'=4,'tp'=2] {'sp_0','sp_1','sp_2'}, dimensions={0} | all-to-all | bytes 4718592 | tf_op jit(solution)/shard_map/all_to_all | solution.py:624
  49.0 5.7 %shard_map.206 = (bf16[576,1024]{1,0:T(8,128)(2,1)S(1)}, bf16[576,1024]{1,0:T(8,128)(2,1)S(1)}, f32[576,768]{1,0:T(8,128)S(1)}, f32[576,768]{1,0:T(8,128)S(1)}, f32[576,768]{1,0:T(8,128)S(1)}) custom-call(s32[1]{0:T(128)} %bitcast.tp, bf16[512,2304]{1,0:T(8,128)(2,1)S(1)} %bitcast.18, bf16[1,2048,768]{2,1,0:T(8,128)(2,1)} %gate_w.5, ...), custom_call_target="tpu_custom_call" | custom-call | flops 2700000000 | bytes 1048576 | tf_op jit(solution)/shard_map/pallas_call | solution.py:57
  55.7 12.1 %shard_map.207 = (bf16[576,1024]{1,0:T(8,128)(2,1)S(1)}, bf16[576,1024]{1,0:T(8,128)(2,1)S(1)}, bf16[576,768]{1,0:T(8,128)(2,1)S(1)}, bf16[576,768]{1,0:T(8,128)...) custom-call(s32[1]{0:T(128)} %bitcast.tp, bf16[512,2304]{1,0:T(8,128)(2,1)S(1)} %collective-permute-done.peer, ...), custom_call_target="tpu_custom_call" | custom-call | flops 4499999744 | bytes 1048576 | tf_op jit(solution)/shard_map/pallas_call | solution.py:57
  70.3 1.6 shard_map.209
  72.7 2.7 %shard_map.208.own = bf16[576,1024]{1,0:T(8,128)(2,1)S(1)} custom-call(s32[1]{0:T(128)} %bitcast.tp, bf16[576,768]{1,0:T(8,128)(2,1)S(1)} %get-tuple-element.48.pre_grad, bf16[576,768]{1,0:T(8,128)(2,1)S(1)} %get-tuple-element.49.up_grad, bf16[1,2048,768]{2,1,0:T(8,128)(2,1)S(1)} %copy-done, bf16[1,2048,768]{2,1,0:T(8,128)(2,1)S(1)} %copy-done.1), custom_call_target="tpu_custom_call" | custom-call | flops 1800000000 | bytes 1048576 | tf_op jit(solution)/shard_map/pallas_call | solution.py:57
  75.5 1.9 %shard_map.210 = bf16[512,1536]{1,0:T(8,128)(2,1)} custom-call(bf16[576,1024]{1,0:T(8,128)(2,1)S(1)} %shard_map.208.own, bf16[576,1024]{1,0:T(8,128)(2,1)S(1)} %collective-permute-done.1.peer, bf16[512,384]{1,0:T(8,128)(2,1)S(1)} %get-tuple-element.51.states), custom_call_target="tpu_custom_call" | custom-call | flops 100000000 | bytes 1048576 | tf_op jit(solution)/shard_map/pallas_call | solution.py:57
  77.4 5.7 %all-to-all-start.1 = ((bf16[64,8,1536]{2,1,0:T(8,128)(2,1)}), bf16[64,8,1536]{2,1,0:T(8,128)(2,1)S(1)}, u32[]{:S(2)}, u32[]{:S(2)}) async-start(bf16[64,8,1536]{2,1,0:T(8,128)(2,1)} %bitcast.6), calls=%async_computation.1 | async-start | bytes 3145728 | tf_op jit(solution)/shard_map/all_to_all | solution.py:624
  83.1 25.3 %all-to-all-done.1 = bf16[64,8,1536]{2,1,0:T(8,128)(2,1)S(1)} async-done(((bf16[64,8,1536]{2,1,0:T(8,128)(2,1)}), bf16[64,8,1536]{2,1,0:T(8,128)(2,1)S(1)}, u32[]{:S(2)}, u32[]{:S(2)}) %all-to-all-start.1) | async-done | bytes 1572896 | tf_op jit(solution)/shard_map/all_to_all | solution.py:624
  108.4 1.8 %shard_map.211 = (bf16[192,1024]{1,0:T(8,128)(2,1)}, bf16[512,256]{1,0:T(8,128)(2,1)S(1)}, f32[512,128]{1,0:T(8,128)S(1)}) custom-call(s32[1]{0:T(128)} %bitcast.tp, bf16[512,1536]{1,0:T(8,128)(2,1)S(1)} %bitcast.19, s32[2,192]{1,0:T(2,128)S(1)} %bitcast.26, bf16[192,2048]{1,0:T(8,128)(2,1)S(1)} %copy-done.2), custom_call_target="tpu_custom_call" | custom-call | flops 300000000 | bytes 1048576 | tf_op jit(solution)/shard_map/pallas_call | solution.py:57
  110.2 2.6 %all-gather = bf16[384,1024]{1,0:T(8,128)(2,1)S(1)} all-gather(bf16[192,1024]{1,0:T(8,128)(2,1)} %get-tuple-element.36), channel_id=2, replica_groups=mesh['sp_0'=4,'sp_1'=4,'sp_2'=4,'tp'=2] {'tp'}, dimensions={0}, use_global_device_ids=true | all-gather | bytes 1179648 | tf_op jit(solution)/shard_map/all_gather | solution.py:666
  112.8 2.1 %shard_map.212 = (bf16[192,512]{1,0:T(8,128)(2,1)}, bf16[192,512]{1,0:T(8,128)(2,1)S(1)}, bf16[192,512]{1,0:T(8,128)(2,1)S(1)}, bf16[512,512]{1,0:T(8,128)(2,1)}) custom-call(bf16[2,192,1024]{2,1,0:T(8,128)(2,1)S(1)} %bitcast.23, bf16[512,2048]{1,0:T(8,128)(2,1)S(1)} %copy-done.3, bf16[192,512]{1,0:T(8,128)(2,1)S(1)} %copy-done.13, ...), custom_call_target="tpu_custom_call" | custom-call | flops 500000000 | bytes 1048576 | tf_op jit(solution)/shard_map/pallas_call | solution.py:57
  114.9 5.3 %all-to-all-start.2 = ((bf16[64,8,512]{2,1,0:T(8,128)(2,1)}), bf16[64,8,512]{2,1,0:T(8,128)(2,1)S(1)}, u32[]{:S(2)}, u32[]{:S(2)}) async-start(bf16[64,8,512]{2,1,0:T(8,128)(2,1)} %bitcast.9), calls=%async_computation.2 | async-start | bytes 1048576 | tf_op jit(solution)/shard_map/all_to_all | solution.py:624
  120.3 1.3 shard_map.213
  122.6 1.6 collective-permute-start.2
  124.1 1.5 collective-permute-start.3
  125.6 1.5 collective-permute-start.4
  127.1 6.2 %collective-permute-done.4.third = bf16[512,256]{1,0:T(8,128)(2,1)S(1)} collective-permute-done((bf16[512,256]{1,0:T(8,128)(2,1)S(1)}, bf16[512,256]{1,0:T(8,128)(2,1)S(1)}, u32[]{:S(2)}, u32[]{:S(2)}) %collective-permute-start.4) | collective-permute-done | bytes 262176 | tf_op jit(solution)/shard_map/ppermute | solution.py:674
  133.3 4.6 %collective-permute-done.2.first = bf16[512,384]{1,0:T(8,128)(2,1)S(1)} collective-permute-done((bf16[512,384]{1,0:T(8,128)(2,1)S(1)}, bf16[512,384]{1,0:T(8,128)(2,1)S(1)}, u32[]{:S(2)}, u32[]{:S(2)}) %collective-permute-start.2) | collective-permute-done | bytes 393248 | tf_op jit(solution)/shard_map/ppermute | solution.py:674
  139.1 1.5 shard_map.214
  140.6 8.6 %all-to-all-start.3 = ((bf16[64,8,1280]{2,1,0:T(8,128)(2,1)}), bf16[64,8,1280]{2,1,0:T(8,128)(2,1)S(1)}, u32[]{:S(2)}, u32[]{:S(2)}) async-start(bf16[64,8,1280]{2,1,0:T(8,128)(2,1)} %bitcast.14), calls=%async_computation.3 | async-start | bytes 2621440 | tf_op jit(solution)/shard_map/all_to_all | solution.py:624
  157.8 10.5 %shard_map.217 = (bf16[1,2048,768]{2,1,0:T(8,128)(2,1)}, bf16[1,2048,768]{2,1,0:T(8,128)(2,1)}, bf16[1,768,2048]{2,1,0:T(8,128)(2,1)}) custom-call(s32[1]{0:T(128)} %bitcast.tp, bf16[576,1024]{1,0:T(8,128)(2,1)S(1)} %copy-done.23, bf16[576,1024]{1,0:T(8,128)(2,1)S(1)} %copy-done.25, bf16[576,1024]{1,0:T(8,128)(2,1)S(1)} %copy-done.27, ...), custom_call_target="tpu_custom_call" | custom-call | flops 5400000000 | bytes 1048576 | tf_op jit(solution)/shard_map/pallas_call | solution.py:57
  168.4 2.1 %shard_map.215 = (bf16[192,256]{1,0:T(8,128)(2,1)}, f32[192,512]{1,0:T(8,128)S(1)}, f32[192,256]{1,0:T(8,128)S(1)}) custom-call(bf16[192,512]{1,0:T(8,128)(2,1)S(1)} %copy-done.33, bf16[192,512]{1,0:T(8,128)(2,1)S(1)} %copy-done.16, bf16[192,256]{1,0:T(8,128)(2,1)S(1)} %copy-done.18, bf16[192,256]{1,0:T(8,128)(2,1)S(1)} %copy-done.20, ...), custom_call_target="tpu_custom_call" | custom-call | flops 600000000 | bytes 1048576 | tf_op jit(solution)/shard_map/pallas_call | solution.py:57
  171.9 2.5 %shard_map.216 = (bf16[192,512]{1,0:T(8,128)(2,1)}, bf16[192,256]{1,0:T(8,128)(2,1)}, f32[32,512]{1,0:T(8,128)}) custom-call(bf16[512,1280]{1,0:T(8,128)(2,1)S(1)} %bitcast.20, bf16[192,512]{1,0:T(8,128)(2,1)} %values_h.1, bf16[192,256]{1,0:T(8,128)(2,1)} %in_map_h.1, f32[192,512]{1,0:T(8,128)} %copy-done.4, f32[192,512]{1,0:T(8,128)} %copy-done.5, ...), custom_call_target="tpu_custom_call" | custom-call | flops 200000000 | bytes 1048576 | tf_op jit(solution)/shard_map/pallas_call | solution.py:57
  (83 shorter events, 16.6 us)
Async XLA Ops:
  49.0 6.7 %collective-permute-start = (bf16[512,2304]{1,0:T(8,128)(2,1)S(1)}, bf16[512,2304]{1,0:T(8,128)(2,1)S(1)}, u32[]{:S(2)}, u32[]{:S(2)}) collective-permute-start(bf16[512,2304]{1,0:T(8,128)(2,1)S(1)} %bitcast.17), channel_id=1, source_target_pairs={{0,1},{1,0},{2,3},{3,2},{4,5},{5,4},{6,7},{7,6},{8,9},{9,8},{10,11... | collective-permute-start | bytes 7077896 | tf_op jit(solution)/shard_map/ppermute | solution.py:629
  55.7 12.2 %copy-start.22 = (bf16[576,1024]{1,0:T(8,128)(2,1)}, bf16[576,1024]{1,0:T(8,128)(2,1)S(1)}, u32[]{:S(2)}) copy-start(bf16[576,1024]{1,0:T(8,128)(2,1)S(1)} %get-tuple-element.73.rows_o) | copy-start | bytes 3538948
  55.7 14.6 %copy-start.15 = (bf16[192,512]{1,0:T(8,128)(2,1)S(1)}, bf16[192,512]{1,0:T(8,128)(2,1)}, u32[]{:S(2)}) copy-start(bf16[192,512]{1,0:T(8,128)(2,1)} %values_h.1) | copy-start | bytes 589828
  55.7 14.6 %copy-start.18 = (bf16[192,256]{1,0:T(8,128)(2,1)S(1)}, bf16[192,256]{1,0:T(8,128)(2,1)}, u32[]{:S(2)}) copy-start(bf16[192,256]{1,0:T(8,128)(2,1)} %in_map_h.1) | copy-start | bytes 294916
  55.7 14.6 %copy-start.34 = (f32[192,8]{0,1:T(8,128)S(1)}, f32[192,8]{0,1:T(8,128)}, u32[]{:S(2)}) copy-start(f32[192,8]{0,1:T(8,128)} %param.27) | copy-start | bytes 18436
  55.7 16.3 %copy-start.1 = (bf16[1,2048,768]{2,1,0:T(8,128)(2,1)S(1)}, bf16[1,2048,768]{2,1,0:T(8,128)(2,1)}, u32[]{:S(2)}) copy-start(bf16[1,2048,768]{2,1,0:T(8,128)(2,1)} %up_w.5) | copy-start | bytes 9437188
  69.8 5.7 %collective-permute-start.1 = (bf16[576,1024]{1,0:T(8,128)(2,1)S(1)}, bf16[576,1024]{1,0:T(8,128)(2,1)S(1)}, u32[]{:S(2)}, u32[]{:S(2)}) collective-permute-start(bf16[576,1024]{1,0:T(8,128)(2,1)S(1)} %get-tuple-element.50), channel_id=1, source_target_pairs={{0,1},{1,0},{2,3},{3,2},{4,5},{5,4},{6,7},{7,6},{8,9},{9,8},{10,11... | collective-permute-start | bytes 3538952 | tf_op jit(solution)/shard_map/ppermute | solution.py:629
  71.9 96.4 %copy-start.4 = (f32[192,512]{1,0:T(8,128)}, f32[192,512]{1,0:T(8,128)S(1)}, u32[]{:S(2)}) copy-start(f32[192,512]{1,0:T(8,128)S(1)} %get-tuple-element.53.start_w.start_h) | copy-start | bytes 1179652
  72.0 96.4 %copy-start.5 = (f32[192,512]{1,0:T(8,128)}, f32[192,512]{1,0:T(8,128)S(1)}, u32[]{:S(2)}) copy-start(f32[192,512]{1,0:T(8,128)S(1)} %get-tuple-element.54.end_w.end_h) | copy-start | bytes 1179652
  77.4 31.0 %copy-start.2 = (bf16[192,2048]{1,0:T(8,128)(2,1)S(1)}, bf16[192,2048]{1,0:T(8,128)(2,1)}, u32[]{:S(2)}) copy-start(bf16[192,2048]{1,0:T(8,128)(2,1)} %cot.1) | copy-start | bytes 2359300
  77.4 31.0 %copy-start.21 = (s32[192,2]{0,1:T(2,128)S(1)}, s32[192,2]{0,1:T(2,128)}, u32[]{:S(2)}) copy-start(s32[192,2]{0,1:T(2,128)} %param.16) | copy-start | bytes 4612
  77.4 31.0 %all-to-all-start.1 = ((bf16[64,8,1536]{2,1,0:T(8,128)(2,1)}), bf16[64,8,1536]{2,1,0:T(8,128)(2,1)S(1)}, u32[]{:S(2)}, u32[]{:S(2)}) async-start(bf16[64,8,1536]{2,1,0:T(8,128)(2,1)} %bitcast.6), calls=%async_computation.1 | async-start | bytes 3145728 | tf_op jit(solution)/shard_map/all_to_all | solution.py:624
  108.4 4.4 %copy-start.3 = (bf16[512,2048]{1,0:T(8,128)(2,1)S(1)}, bf16[512,2048]{1,0:T(8,128)(2,1)}, u32[]{:S(2)}) copy-start(bf16[512,2048]{1,0:T(8,128)(2,1)} %proj_w.1) | copy-start | bytes 6291460
  108.4 4.4 %copy-start.13 = (bf16[192,512]{1,0:T(8,128)(2,1)S(1)}, bf16[192,512]{1,0:T(8,128)(2,1)}, u32[]{:S(2)}) copy-start(bf16[192,512]{1,0:T(8,128)(2,1)} %gate_in.1) | copy-start | bytes 589828
  114.9 5.4 %copy-start.32 = (bf16[192,512]{1,0:T(8,128)(2,1)}, bf16[192,512]{1,0:T(8,128)(2,1)S(1)}, u32[]{:S(2)}) copy-start(bf16[192,512]{1,0:T(8,128)(2,1)S(1)} %get-tuple-element.63.scan_grad) | copy-start | bytes 589828
  114.9 23.0 %all-to-all-start.2 = ((bf16[64,8,512]{2,1,0:T(8,128)(2,1)}), bf16[64,8,512]{2,1,0:T(8,128)(2,1)S(1)}, u32[]{:S(2)}, u32[]{:S(2)}) async-start(bf16[64,8,512]{2,1,0:T(8,128)(2,1)} %bitcast.9), calls=%async_computation.2 | async-start | bytes 1048576 | tf_op jit(solution)/shard_map/all_to_all | solution.py:624
  122.6 15.3 %collective-permute-start.2 = (bf16[512,384]{1,0:T(8,128)(2,1)S(1)}, bf16[512,384]{1,0:T(8,128)(2,1)S(1)}, u32[]{:S(2)}, u32[]{:S(2)}) collective-permute-start(bf16[512,384]{1,0:T(8,128)(2,1)S(1)} %get-tuple-element.60), channel_id=1, source_target_pairs={{0,32},{32,0},{64,96},{96,64},{1,33},{33,1},{65,97},{97,65},{2,34}... | collective-permute-start | bytes 1179656 | tf_op jit(solution)/shard_map/ppermute | solution.py:674
  124.1 13.7 %collective-permute-start.3 = (bf16[512,384]{1,0:T(8,128)(2,1)S(1)}, bf16[512,384]{1,0:T(8,128)(2,1)S(1)}, u32[]{:S(2)}, u32[]{:S(2)}) collective-permute-start(bf16[512,384]{1,0:T(8,128)(2,1)S(1)} %get-tuple-element.61), channel_id=1, source_target_pairs={{0,8},{8,0},{16,24},{24,16},{1,9},{9,1},{17,25},{25,17},{2,10},{10... | collective-permute-start | bytes 1179656 | tf_op jit(solution)/shard_map/ppermute | solution.py:674
  125.6 7.7 %collective-permute-start.4 = (bf16[512,256]{1,0:T(8,128)(2,1)S(1)}, bf16[512,256]{1,0:T(8,128)(2,1)S(1)}, u32[]{:S(2)}, u32[]{:S(2)}) collective-permute-start(bf16[512,256]{1,0:T(8,128)(2,1)S(1)} %get-tuple-element.62), channel_id=1, source_target_pairs={{0,2},{2,0},{4,6},{6,4},{1,3},{3,1},{5,7},{7,5},{8,10},{10,8},{12,... | collective-permute-start | bytes 786440 | tf_op jit(solution)/shard_map/ppermute | solution.py:674
  140.6 31.3 %all-to-all-start.3 = ((bf16[64,8,1280]{2,1,0:T(8,128)(2,1)}), bf16[64,8,1280]{2,1,0:T(8,128)(2,1)S(1)}, u32[]{:S(2)}, u32[]{:S(2)}) async-start(bf16[64,8,1280]{2,1,0:T(8,128)(2,1)} %bitcast.14), calls=%async_computation.3 | async-start | bytes 2621440 | tf_op jit(solution)/shard_map/all_to_all | solution.py:624
  157.7 10.6 %copy-start.16 = (bf16[192,512]{1,0:T(8,128)(2,1)S(1)}, bf16[192,512]{1,0:T(8,128)(2,1)}, u32[]{:S(2)}) copy-start(bf16[192,512]{1,0:T(8,128)(2,1)} %values_h.1) | copy-start | bytes 589828
  157.7 10.6 %copy-start.20 = (bf16[192,256]{1,0:T(8,128)(2,1)S(1)}, bf16[192,256]{1,0:T(8,128)(2,1)}, u32[]{:S(2)}) copy-start(bf16[192,256]{1,0:T(8,128)(2,1)} %out_map.3) | copy-start | bytes 294916
  157.7 10.6 %copy-start.33 = (bf16[192,512]{1,0:T(8,128)(2,1)S(1)}, bf16[192,512]{1,0:T(8,128)(2,1)}, u32[]{:S(2)}) copy-start(bf16[192,512]{1,0:T(8,128)(2,1)} %copy-done.32) | copy-start | bytes 589828
  157.7 10.6 %copy-start.36 = (f32[192,8]{1,0:T(8,128)S(1)}, f32[192,8]{1,0:T(8,128)}, u32[]{:S(2)}) copy-start(f32[192,8]{1,0:T(8,128)} %copy-done.35) | copy-start | bytes 18436
  (21 other events, 36.4 us)

commit v3 on v2

--- a/solution.py
+++ b/solution.py
@@ -8,6 +8,7 @@
 
 
 SP = ("sp_0", "sp_1", "sp_2")
+ALL = SP + ("tp",)
 TOK = 192
 WIDTH = 2048
 HALF = 1024
@@ -102,7 +103,7 @@
     ]
 
 
-def pack_body(tp, ids, weights, rows_hbm, cot_hbm, out, rows, cot, sems):
+def pack_body(tp, ids, weights, rows_hbm, cot_hbm, out_hbm, rows, cot, out, sems):
     at = pl.ds(pl.multiple_of(tp[0] * HALF, HALF), HALF)
     get_rows = pltpu.make_async_copy(rows_hbm.at[:, at], rows, sems.at[0])
     get_cot = pltpu.make_async_copy(cot_hbm.at[:, at], cot, sems.at[1])
@@ -110,22 +111,27 @@
     get_cot.start()
     first, second = slot_choices(ids[...])
     both = ones_where(first | second)
-    same = iota((TOK, TOK), 0) == iota((TOK, TOK), 1)
-
-    def column(k):
-        return jnp.sum(jnp.where(same, weights[k : k + 1], 0.0), axis=1, keepdims=True)
-
+    scale = jnp.where(first, weights[0:1], jnp.where(second, weights[1:2], 0.0))
+    scale = jnp.sum(scale, axis=1, keepdims=True)
+
+    def leave(k, low, high):
+        lanes = slice(low, high)
+        return pltpu.make_async_copy(out.at[:, lanes], out_hbm.at[:, lanes], sems.at[k])
+
+    pieces = (leave(2, 0, HALF), leave(3, HALF, 2 * HALF), leave(4, 2 * HALF, 2 * HALF + 256))
     get_rows.wait()
     row_slots = mm(both, rows[...], NN).astype(BF)
     out[:, 0:HALF] = row_slots[:MAIN]
+    pieces[0].start()
     out[:, 2 * HALF : 2 * HALF + 128] = fold_last(row_slots[MAIN:])
     get_cot.wait()
-    full = cot[...].astype(F32)
-    cot_slots = mm(ones_where(first), (column(0) * full).astype(BF), NN)
-    cot_slots = cot_slots + mm(ones_where(second), (column(1) * full).astype(BF), NN)
-    cot_slots = cot_slots.astype(BF)
+    cot_slots = (scale * mm(both, cot[...], NN)).astype(BF)
+    out[:, 2 * HALF + 128 :] = fold_last(cot_slots[MAIN:])
+    pieces[2].start()
     out[:, HALF : 2 * HALF] = cot_slots[:MAIN]
-    out[:, 2 * HALF + 128 :] = fold_last(cot_slots[MAIN:])
+    pieces[1].start()
+    for piece in pieces:
+        piece.wait()
 
 
 def whole(dims):
@@ -142,15 +148,16 @@
             pl.BlockSpec(memory_space=pltpu.HBM),
             pl.BlockSpec(memory_space=pltpu.HBM),
         ],
-        out_specs=whole((MAIN, 2 * HALF + 256)),
+        out_specs=pl.BlockSpec(memory_space=pltpu.HBM),
         scratch_shapes=[
             pltpu.VMEM((TOK, HALF), BF),
             pltpu.VMEM((TOK, HALF), BF),
-            pltpu.SemaphoreType.DMA((2,)),
+            pltpu.VMEM((MAIN, 2 * HALF + 256), BF),
+            pltpu.SemaphoreType.DMA((5,)),
         ],
     )
     return call(
-        pack_body, shape((MAIN, 2 * HALF + 256)), 1_000_000_000, hbm_in=(1, 2, 3, 4), grid_spec=spec
+        pack_body, pltpu.HBM((MAIN, 2 * HALF + 256), BF), 1_000_000_000, hbm_in=(1, 2, 3, 4), grid_spec=spec
     )(tp, ids, weights, rows, cot)
 
 
@@ -217,35 +224,93 @@
     cot[MAIN:] = last_cot
 
 
-def own_body(tp, own, gate_w, up_w, down_w, rows, cot, gate_o, up_o, act_o):
-    @pl.when(pl.program_id(0) == 0)
+def fetch(half, gate_h, up_h, down_h, gate_w, up_w, down_w, sems):
+    wide = pl.ds(pl.multiple_of(half * HALF, HALF), HALF)
+    steps = []
+    for j in range(FF // FF_STEP):
+        part = pl.ds(j * FF_STEP, FF_STEP)
+        steps.append(
+            (
+                pltpu.make_async_copy(gate_h.at[0, wide, part], gate_w.at[j], sems.at[j, 0]),
+                pltpu.make_async_copy(up_h.at[0, wide, part], up_w.at[j], sems.at[j, 1]),
+                pltpu.make_async_copy(down_h.at[0, part, wide], down_w.at[j], sems.at[j, 2]),
+            )
+        )
+    return steps
+
+
+def open_step(half, got, weights_h, rows_h, cot_h, rows, cot, weights, sems, out_sems):
+    step = pl.program_id(0)
+    copies = fetch(half, *weights_h, *weights, sems)
+    keep = (
+        pltpu.make_async_copy(rows, rows_h, out_sems.at[0]),
+        pltpu.make_async_copy(cot, cot_h, out_sems.at[1]),
+    )
+
+    @pl.when(step == 0)
     def _():
-        split_slots(own, rows, cot)
-
-    gate_o[...] = mm(rows[...], gate_w[0], NN)
-    up_o[...] = mm(rows[...], up_w[0], NN)
-    act_o[...] = mm(cot[...], down_w[0], NT)
+        for group in copies:
+            for c in group:
+                c.start()
+        split_slots(got, rows, cot)
+        for c in keep:
+            c.start()
+
+    for j, group in enumerate(copies):
+
+        @pl.when(step == j)
+        def _():
+            for c in group:
+                c.wait()
+
+    return step, keep
+
+
+def own_body(
+    tp, own, gate_h, up_h, down_h, rows_h, cot_h, gate_o, up_o, act_o,
+    rows, cot, gate_w, up_w, down_w, sems, out_sems,
+):
+    step, keep = open_step(
+        tp[0], own, (gate_h, up_h, down_h), rows_h, cot_h, rows, cot, (gate_w, up_w, down_w),
+        sems, out_sems,
+    )
+    gate_o[...] = mm(rows[...], gate_w[step], NN)
+    up_o[...] = mm(rows[...], up_w[step], NN)
+    act_o[...] = mm(cot[...], down_w[step], NT)
+
+    @pl.when(step == 2)
+    def _():
+        for c in keep:
+            c.wait()
 
 
 def step_block(dims):
     return pl.BlockSpec(dims, lambda i, t: (0, i))
+
+
+HBM = pl.BlockSpec(memory_space=pltpu.HBM)
+EXPERT_SCRATCH = [
+    pltpu.VMEM((SLOTS, HALF), BF),
+    pltpu.VMEM((SLOTS, HALF), BF),
+    pltpu.VMEM((3, HALF, FF_STEP), BF),
+    pltpu.VMEM((3, HALF, FF_STEP), BF),
+    pltpu.VMEM((3, FF_STEP, HALF), BF),
+    pltpu.SemaphoreType.DMA((3, 3)),
+    pltpu.SemaphoreType.DMA((2,)),
+]
 
 
 def expert_own(tp, own, gate_w, up_w, down_w):
     spec = pltpu.PrefetchScalarGridSpec(
         num_scalar_prefetch=1,
         grid=(FF // FF_STEP,),
-        in_specs=[
-            whole((MAIN, 2 * HALF + 256)),
-            pl.BlockSpec((1, HALF, FF_STEP), lambda i, t: (0, t[0], i)),
-            pl.BlockSpec((1, HALF, FF_STEP), lambda i, t: (0, t[0], i)),
-            pl.BlockSpec((1, FF_STEP, HALF), lambda i, t: (0, i, t[0])),
-        ],
-        out_specs=[whole((SLOTS, HALF))] * 2 + [step_block((SLOTS, FF_STEP))] * 3,
+        in_specs=[whole((MAIN, 2 * HALF + 256)), HBM, HBM, HBM],
+        out_specs=[HBM, HBM] + [step_block((SLOTS, FF_STEP))] * 3,
+        scratch_shapes=EXPERT_SCRATCH,
     )
     return call(
         own_body,
-        [shape((SLOTS, HALF))] * 2 + [shape((SLOTS, FF), F32)] * 3,
+        [pltpu.HBM((SLOTS, HALF), BF)] * 2 + [shape((SLOTS, FF), F32)] * 3,
         2_700_000_000,
         hbm_in=(2, 3, 4),
         grid_spec=spec,
@@ -254,58 +319,49 @@
 
 
 def peer_body(
-    tp, peer, gate_w, up_w, down_w, gate_o, up_o, act_o,
-    rows, cot, active, pre_grad, up_grad, part, acc,
+    tp, peer, gate_h, up_h, down_h, gate_o, up_o, act_o,
+    rows_h, cot_h, active, pre_grad, up_grad, part,
+    rows, cot, gate_w, up_w, down_w, sems, out_sems, acc,
 ):
-    step = pl.program_id(0)
-
-    @pl.when(step == 0)
-    def _():
-        split_slots(peer, rows, cot)
-
-    gate_pre = gate_o[...] + mm(rows[...], gate_w[0], NN)
-    up_val = up_o[...] + mm(rows[...], up_w[0], NN)
-    act_grad = act_o[...] + mm(cot[...], down_w[0], NT)
-    act, slope = silu_parts(gate_pre)
-    active[...] = (act * up_val).astype(BF)
-    up_g = (act_grad * act).astype(BF)
-    pre_g = (act_grad * up_val * slope).astype(BF)
-    up_grad[...] = up_g
-    pre_grad[...] = pre_g
-    new = mm(pre_g, gate_w[0], NT) + mm(up_g, up_w[0], NT)
-
-    @pl.when(step == 0)
-    def _():
-        acc[...] = new
-
-    @pl.when(step == 1)
-    def _():
-        acc[...] += new
+    step, keep = open_step(
+        1 - tp[0], peer, (gate_h, up_h, down_h), rows_h, cot_h, rows, cot, (gate_w, up_w, down_w),
+        sems, out_sems,
+    )
+    for first in range(0, SLOTS, SLOTS // 2):
+        at = slice(first, first + SLOTS // 2)
+        gate_pre = gate_o[at] + mm(rows[at], gate_w[step], NN)
+        up_val = up_o[at] + mm(rows[at], up_w[step], NN)
+        act_grad = act_o[at] + mm(cot[at], down_w[step], NT)
+        act, slope = silu_parts(gate_pre)
+        active[at] = (act * up_val).astype(BF)
+        up_grad[at] = (act_grad * act).astype(BF)
+        pre_grad[at] = (act_grad * up_val * slope).astype(BF)
+    for first in range(0, SLOTS, SLOTS // 2):
+        at = slice(first, first + SLOTS // 2)
+        before = jnp.where(step == 0, 0.0, acc[at])
+        acc[at] = before + mm(pre_grad[at], gate_w[step], NT) + mm(up_grad[at], up_w[step], NT)
 
     @pl.when(step == 2)
     def _():
-        part[...] = (acc[...] + new).astype(BF)
+        part[...] = acc[...].astype(BF)
+        for c in keep:
+            c.wait()
 
 
 def expert_peer(tp, peer, gate_w, up_w, down_w, gate_o, up_o, act_o):
     spec = pltpu.PrefetchScalarGridSpec(
         num_scalar_prefetch=1,
         grid=(FF // FF_STEP,),
-        in_specs=[
-            whole((MAIN, 2 * HALF + 256)),
-            pl.BlockSpec((1, HALF, FF_STEP), lambda i, t: (0, 1 - t[0], i)),
-            pl.BlockSpec((1, HALF, FF_STEP), lambda i, t: (0, 1 - t[0], i)),
-            pl.BlockSpec((1, FF_STEP, HALF), lambda i, t: (0, i, 1 - t[0])),
-        ]
+        in_specs=[whole((MAIN, 2 * HALF + 256)), HBM, HBM, HBM]
         + [step_block((SLOTS, FF_STEP))] * 3,
-        out_specs=[whole((SLOTS, HALF))] * 2
-        + [step_block((SLOTS, FF_STEP))] * 3
-        + [whole((SLOTS, HALF))],
-        scratch_shapes=[pltpu.VMEM((SLOTS, HALF), F32)],
+        out_specs=[HBM, HBM] + [step_block((SLOTS, FF_STEP))] * 3 + [whole((SLOTS, HALF))],
+        scratch_shapes=EXPERT_SCRATCH + [pltpu.VMEM((SLOTS, HALF), F32)],
     )
     return call(
         peer_body,
-        [shape((SLOTS, HALF))] * 2 + [shape((SLOTS, FF))] * 3 + [shape((SLOTS, HALF))],
+        [pltpu.HBM((SLOTS, HALF), BF)] * 2
+        + [shape((SLOTS, FF))] * 3
+        + [shape((SLOTS, HALF))],
         4_500_000_000,
         hbm_in=(2, 3, 4),
         grid_spec=spec,
@@ -366,6 +422,7 @@
         weight_body,
         (shape((1, WIDTH, FF)), shape((1, WIDTH, FF)), shape((1, FF, WIDTH))),
         5_400_000_000,
+        hbm_in=(1, 2, 3, 4),
         grid_spec=spec,
         vmem=24 << 20,
     )(tp, rows_o, cot_o, rows_p, cot_p, active, pre_grad, up_grad)
@@ -458,7 +515,7 @@
     )(*args)
 
 
-PARTS = ((0, 384), (768, 384), (1536, 256))
+PARTS = ((0, 640), (1280, 384))
 
 
 def proj_body(odd, stream, gated, keep, *sends):
@@ -482,7 +539,7 @@
 
 
 def proj_part(odd, stream, gated):
-    out = [shape((MAIN, 1024))] + [shape((MAIN, width)) for _, width in PARTS]
+    out = [pltpu.HBM((MAIN, 1024), BF)] + [shape((MAIN, width)) for _, width in PARTS]
     spec = pltpu.PrefetchScalarGridSpec(
         num_scalar_prefetch=1,
         grid=(1,),
@@ -492,27 +549,34 @@
     return call(proj_body, out, 400_000_000, grid_spec=spec)(odd, stream, gated)
 
 
-def scan_body(got, decays, keep, first, second, third, out, work, wide):
+def scan_body(got, decays, keep_h, first, second, out, work, wide, keep, sem):
+    fetch_keep = pltpu.make_async_copy(keep_h, keep, sem.at[0])
+    fetch_keep.start()
+    wide[...] = got[:, 0:256].astype(F32)
+    scan_states(wide[:, 0:128], wide[:, 128:256], decays[...], out, work)
+    fetch_keep.wait()
     at = 0
-    for other in (first, second, third):
+    for other in (first, second):
         width = other.shape[1]
         total = keep[:, at : at + width].astype(F32) + other[...].astype(F32)
         out[:, 256 + at : 256 + at + width] = total.astype(BF)
         at += width
-    wide[...] = got[:, 0:256].astype(F32)
-    scan_states(wide[:, 0:128], wide[:, 128:256], decays[...], out, work)
 
 
 def scan_grads(got, decays, keep, others):
     spec = pl.GridSpec(
         grid=(1,),
-        in_specs=[whole((MAIN, 512)), whole((MAIN, 128)), whole((MAIN, 1024))]
-        + [whole(o.shape) for o in others],
+        in_specs=[whole((MAIN, 512)), whole((MAIN, 128)), HBM] + [whole(o.shape) for o in others],
         out_specs=whole((MAIN, 256 + 1024)),
-        scratch_shapes=[pltpu.VMEM((MAIN, 256), F32), pltpu.VMEM((MAIN, 256), F32)],
-    )
-    return call(
-        scan_body, shape((MAIN, 256 + 1024)), 100_000_000, grid_spec=spec
+        scratch_shapes=[
+            pltpu.VMEM((MAIN, 256), F32),
+            pltpu.VMEM((MAIN, 256), F32),
+            pltpu.VMEM((MAIN, 1024), BF),
+            pltpu.SemaphoreType.DMA((1,)),
+        ],
+    )
+    return call(
+        scan_body, shape((MAIN, 256 + 1024)), 100_000_000, hbm_in=(2,), grid_spec=spec
     )(got, decays, keep, *others)
 
 
@@ -554,7 +618,7 @@
 
 
 def far_body(
-    states, values_h, in_map_h, start_h, end_h, value_part_h, in_part_h,
+    tp, states, values_h, in_map_h, start_h, end_h, value_part_h, in_part_h,
     value_grad, in_grad, proj_grad,
     values, in_map, start_w, end_w, value_part, in_part, sems,
 ):
@@ -571,16 +635,21 @@
         c.start()
     at = 256
     for j, (first, width) in enumerate(PARTS):
-        sums = [jnp.zeros((8, width), F32), jnp.zeros((8, width), F32)]
+        sums = [[jnp.zeros((8, width), F32) for _ in range(2)] for _ in range(2)]
         for b in range(BLOCKS):
-            half = (b >> (4 - 2 * j)) & 1
-            sums[half] = sums[half] + states[8 * b : 8 * b + 8, at : at + width].astype(F32)
+            chunk = states[8 * b : 8 * b + 8, at : at + width].astype(F32)
+            here = sums[(b >> 4) & 1] if j == 0 else sums[b & 1]
+            other = (b >> 2) & 1
+            here[other] = here[other] + chunk
         at += width
         for half in range(2):
+            total = sums[half][0] + sums[half][1]
+            if j == 0:
+                total = jnp.where(tp[0] == 0, total, sums[0][half] + sums[1][half])
             for k in range(width // 128):
                 tile = (first + half * width) // 128 + k
                 q, lane = 8 * (tile // 4), 128 * (tile % 4)
-                proj_grad[q : q + 8, lane : lane + 128] = sums[half][:, 128 * k : 128 * k + 128]
+                proj_grad[q : q + 8, lane : lane + 128] = total[:, 128 * k : 128 * k + 128]
     for c in copies:
         c.wait()
     val = values[...].astype(F32)
@@ -602,7 +671,8 @@
 
 def far(*args):
     far_out = (shape((TOK, CHAN)), shape((TOK, KEYS)), shape((32, CHAN), F32))
-    spec = pl.GridSpec(
+    spec = pltpu.PrefetchScalarGridSpec(
+        num_scalar_prefetch=1,
         grid=(1,),
         in_specs=[whole((MAIN, 256 + 1024))] + [pl.BlockSpec(memory_space=pltpu.HBM)] * 6,
         out_specs=[whole(o.shape) for o in far_out],
@@ -616,13 +686,21 @@
             pltpu.SemaphoreType.DMA((6,)),
         ],
     )
-    return call(far_body, far_out, 200_000_000, hbm_in=range(1, 7), grid_spec=spec)(*args)
+    return call(far_body, far_out, 200_000_000, hbm_in=range(2, 8), grid_spec=spec)(*args)
 
 
 def swap(rows):
     lanes = rows.shape[1]
     out = lax.all_to_all(rows.reshape(BLOCKS, -1, lanes), SP, 0, 0, tiled=True)
     return out.reshape(-1, lanes)
+
+
+def pairs_of(piece):
+    out = []
+    for source in range(128):
+        step = 2 if piece else 32 if source % 2 == 0 else 8
+        out.append((source, source ^ step))
+    return out
 
 
 def other_core(array):
@@ -668,17 +746,17 @@
         stream, proj_weight, gate_input, scan_out, start_w, end_w, out_map, x_states
     )
     got = swap(payload)
-    odd = jnp.stack([lax.axis_index(name) & 1 for name in SP]).astype(jnp.int32)
+    place = [lax.axis_index(name).astype(jnp.int32) & 1 for name in SP]
+    odd = jnp.stack([jnp.where(tp[0] == 0, place[0], place[1]), place[2]])
     keep, *halves = proj_part(odd, stream, gated)
-    pair = [(0, 1), (1, 0), (2, 3), (3, 2)]
-    others = [lax.ppermute(h, name, pair) for h, name in zip(halves, SP)]
+    others = [lax.ppermute(h, ALL, pairs_of(i)) for i, h in enumerate(halves)]
     buffer = scan_grads(got, decays, keep, others)
     g_states = swap(buffer)
     out_grad, value_part, in_part = near(
         scan_grad, values, in_map, out_map, cum, cum_t, start_w, end_w, got[:, 256:]
     )
     value_grad, in_grad, proj_grad = far(
-        g_states, values, in_map, start_w, end_w, value_part, in_part
+        tp, g_states, values, in_map, start_w, end_w, value_part, in_part
     )
     return (
         stream_grad,

time: 176 us -> 171 us (0.972)
  local copies, waits for them, and re-layouts: 16 us -> 6.31 us
  waiting for transfers between devices: 36 us -> 40.5 us
    unnamed x74 -> x56, local copies, waits for them, and re-layouts: 15.9 us -> 6.29 us
    ppermute x3 -> x2, waiting for transfers between devices: 10.8 us -> 13.8 us  [on_device(): others = [lax.ppermute(h, ALL, pairs_of(i)) for i, h in enumerate(halves)]]
    ppermute x3 -> x2, starting transfers between devices: 4.52 us -> 2.09 us  [on_device(): others = [lax.ppermute(h, ALL, pairs_of(i)) for i, h in enumerate(halves)]]
  transfers between devices with their start and end apart: 8 -> 7, of which waited for: 3 -> 3; matrix products, arithmetic and copies ran while one was open for 0% -> 0% of each run, Pallas kernels for 14% -> 14%
where the time goes in v3:
time: 171 us; the launch traced here: 170 us
  Pallas kernels  50.6 us (30%)
  blocking collectives  47.4 us (28%)
  waiting for transfers between devices  40.5 us (24%)
  starting transfers between devices  23.9 us (14%)
  local copies, waits for them, and re-layouts  6.31 us (4%)
    pallas_call x13, Pallas kernels, run(): kernel(*[pltpu.with_memory_space_constraint(a, pltpu.HBM) if i in hbm_in...  50.6 us
    all_to_all x1, blocking collectives, swap(): out = lax.all_to_all(rows.reshape(BLOCKS, -1, lanes), SP, 0, 0, tiled=True)  44.6 us
    all_to_all x3, waiting for transfers between devices, swap(): out = lax.all_to_all(rows.reshape(BLOCKS, -1, lanes), SP, 0, 0, tiled=True)  26.7 us
    all_to_all x3, starting transfers between devices, swap(): out = lax.all_to_all(rows.reshape(BLOCKS, -1, lanes), SP, 0, 0, tiled=True)  21.2 us
    ppermute x2, waiting for transfers between devices, on_device(): others = [lax.ppermute(h, ALL, pairs_of(i)) for i, h in enumerate(halves)]  13.8 us
    unnamed x56, local copies, waits for them, and re-layouts  6.29 us
  transfers between devices with their start and end apart: 7, of which 3 were waited for; matrix products, arithmetic and copies ran while one was open for 0% of the time, Pallas kernels for 14%

profile of v3, /device:TPU:0, one launch (start us, length us, event | category | flops | bytes accessed | tf_op | source)
XLA Modules:
  0.0 169.8 jit_solution(11049056989505765252)
XLA Ops:
  0.6 4.5 %shard_map.205 = bf16[512,2304]{1,0:T(8,128)(2,1)} custom-call(s32[1]{0:T(128)} %bitcast.tp, s32[2,192]{1,0:T(2,128)} %bitcast.23, f32[2,192]{1,0:T(2,128)} %bitcast.27, bf16[192,2048]{1,0:T(8,128)(2,1)} %rows_hbm.1, bf16[192,2048]{1,0:T(8,128)(2,1)} %cot.1), custom_call_target="tpu_custom_call" | custom-call | flops 1000000000 | bytes 1048576 | tf_op jit(solution)/shard_map/pallas_call | solution.py:58
  5.2 44.6 %all_to_all.20 = bf16[64,8,2304]{2,1,0:T(8,128)(2,1)S(1)} all-to-all(bf16[64,8,2304]{2,1,0:T(8,128)(2,1)} %bitcast.26), channel_id=1, replica_groups=mesh['sp_0'=4,'sp_1'=4,'sp_2'=4,'tp'=2] {'sp_0','sp_1','sp_2'}, dimensions={0} | all-to-all | bytes 4718592 | tf_op jit(solution)/shard_map/all_to_all | solution.py:694
  49.8 5.5 %shard_map.206 = (bf16[576,1024]{1,0:T(8,128)(2,1)}, bf16[576,1024]{1,0:T(8,128)(2,1)}, f32[576,768]{1,0:T(8,128)S(1)}, f32[576,768]{1,0:T(8,128)S(1)}, f32[576,768]{1,0:T(8,128)S(1)}) custom-call(s32[1]{0:T(128)} %bitcast.tp, bf16[512,2304]{1,0:T(8,128)(2,1)S(1)} %bitcast.16, bf16[1,2048,768]{2,1,0:T(8,128)(2,1)} %gate_w.1, bf16[1,2048,768]{2,1,0:T(8,128)(2,1)} %up_w.1, ...), custom_call_target="tpu_custom_call" | custom-call | flops 2700000000 | bytes 1048576 | tf_op jit(solution)/shard_map/pallas_call | solution.py:58
  55.4 9.0 %shard_map.207 = (bf16[576,1024]{1,0:T(8,128)(2,1)}, bf16[576,1024]{1,0:T(8,128)(2,1)}, bf16[576,768]{1,0:T(8,128)(2,1)S(1)}, bf16[576,768]{1,0:T(8,128)(2,1)S(1...) custom-call(s32[1]{0:T(128)} %bitcast.tp, bf16[512,2304]{1,0:T(8,128)(2,1)S(1)} %collective-permute-done.peer, ...), custom_call_target="tpu_custom_call" | custom-call | flops 4499999744 | bytes 1048576 | tf_op jit(solution)/shard_map/pallas_call | solution.py:58
  65.0 1.6 shard_map.209
  67.2 2.7 %shard_map.208.own = bf16[576,1024]{1,0:T(8,128)(2,1)S(1)} custom-call(s32[1]{0:T(128)} %bitcast.tp, bf16[576,768]{1,0:T(8,128)(2,1)S(1)} %get-tuple-element.47.pre_grad, bf16[576,768]{1,0:T(8,128)(2,1)S(1)} %get-tuple-element.48.up_grad, bf16[1,2048,768]{2,1,0:T(8,128)(2,1)S(1)} %copy-done, bf16[1,2048,768]{2,1,0:T(8,128)(2,1)S(1)} %copy-done.1), custom_call_target="tpu_custom_call" | custom-call | flops 1800000000 | bytes 1048576 | tf_op jit(solution)/shard_map/pallas_call | solution.py:58
  70.0 1.9 %shard_map.210 = bf16[512,1536]{1,0:T(8,128)(2,1)} custom-call(bf16[576,1024]{1,0:T(8,128)(2,1)S(1)} %shard_map.208.own, bf16[576,1024]{1,0:T(8,128)(2,1)S(1)} %collective-permute-done.1.peer, bf16[512,384]{1,0:T(8,128)(2,1)S(1)} %get-tuple-element.50.states), custom_call_target="tpu_custom_call" | custom-call | flops 100000000 | bytes 1048576 | tf_op jit(solution)/shard_map/pallas_call | solution.py:58
  71.9 5.5 %all-to-all-start.1 = ((bf16[64,8,1536]{2,1,0:T(8,128)(2,1)}), bf16[64,8,1536]{2,1,0:T(8,128)(2,1)S(1)}, u32[]{:S(2)}, u32[]{:S(2)}) async-start(bf16[64,8,1536]{2,1,0:T(8,128)(2,1)} %bitcast.6), calls=%async_computation.1 | async-start | bytes 3145728 | tf_op jit(solution)/shard_map/all_to_all | solution.py:694
  77.5 25.3 %all-to-all-done.1 = bf16[64,8,1536]{2,1,0:T(8,128)(2,1)S(1)} async-done(((bf16[64,8,1536]{2,1,0:T(8,128)(2,1)}), bf16[64,8,1536]{2,1,0:T(8,128)(2,1)S(1)}, u32[]{:S(2)}, u32[]{:S(2)}) %all-to-all-start.1) | async-done | bytes 1572896 | tf_op jit(solution)/shard_map/all_to_all | solution.py:694
  102.8 1.8 %shard_map.211 = (bf16[192,1024]{1,0:T(8,128)(2,1)}, bf16[512,256]{1,0:T(8,128)(2,1)S(1)}, f32[512,128]{1,0:T(8,128)S(1)}) custom-call(s32[1]{0:T(128)} %bitcast.tp, bf16[512,1536]{1,0:T(8,128)(2,1)S(1)} %bitcast.17, s32[2,192]{1,0:T(2,128)S(1)} %bitcast.24, bf16[192,2048]{1,0:T(8,128)(2,1)S(1)} %copy-done.2), custom_call_target="tpu_custom_call" | custom-call | flops 300000000 | bytes 1048576 | tf_op jit(solution)/shard_map/pallas_call | solution.py:58
  104.6 2.7 %all-gather = bf16[384,1024]{1,0:T(8,128)(2,1)S(1)} all-gather(bf16[192,1024]{1,0:T(8,128)(2,1)} %get-tuple-element.35), channel_id=2, replica_groups=mesh['sp_0'=4,'sp_1'=4,'sp_2'=4,'tp'=2] {'tp'}, dimensions={0}, use_global_device_ids=true | all-gather | bytes 1179648 | tf_op jit(solution)/shard_map/all_gather | solution.py:744
  107.4 2.1 %shard_map.212 = (bf16[192,512]{1,0:T(8,128)(2,1)}, bf16[192,512]{1,0:T(8,128)(2,1)S(1)}, bf16[192,512]{1,0:T(8,128)(2,1)S(1)}, bf16[512,512]{1,0:T(8,128)(2,1)}) custom-call(bf16[2,192,1024]{2,1,0:T(8,128)(2,1)S(1)} %bitcast.21, bf16[512,2048]{1,0:T(8,128)(2,1)S(1)} %copy-done.3, bf16[192,512]{1,0:T(8,128)(2,1)S(1)} %copy-done.11, ...), custom_call_target="tpu_custom_call" | custom-call | flops 500000000 | bytes 1048576 | tf_op jit(solution)/shard_map/pallas_call | solution.py:58
  109.5 2.3 %shard_map.213 = (bf16[512,1024]{1,0:T(8,128)(2,1)}, bf16[512,640]{1,0:T(8,128)(2,1)S(1)}, bf16[512,384]{1,0:T(8,128)(2,1)S(1)}) custom-call(s32[2]{0:T(128)S(1)} %pad_add_fusion.odd, bf16[2,192,1024]{2,1,0:T(8,128)(2,1)S(1)} %bitcast.22, bf16[192,512]{1,0:T(8,128)(2,1)S(1)} %get-tuple-element.57.gated), custom_call_target="tpu_custom_call" | custom-call | flops 400000000 | bytes 1048576 | tf_op jit(solution)/shard_map/pallas_call | solution.py:58
  113.0 5.7 %all-to-all-start.2 = ((bf16[64,8,512]{2,1,0:T(8,128)(2,1)}), bf16[64,8,512]{2,1,0:T(8,128)(2,1)S(1)}, u32[]{:S(2)}, u32[]{:S(2)}) async-start(bf16[64,8,512]{2,1,0:T(8,128)(2,1)} %bitcast.9), calls=%async_computation.2 | async-start | bytes 1048576 | tf_op jit(solution)/shard_map/all_to_all | solution.py:694
  118.7 1.6 collective-permute-start.3
  120.4 13.8 %collective-permute-done.3.second = bf16[512,384]{1,0:T(8,128)(2,1)S(1)} collective-permute-done((bf16[512,384]{1,0:T(8,128)(2,1)}, bf16[512,384]{1,0:T(8,128)(2,1)S(1)}, u32[]{:S(2)}, u32[]{:S(2)}) %collective-permute-start.3) | collective-permute-done | bytes 393248 | tf_op jit(solution)/shard_map/ppermute | solution.py:752
  134.2 2.6 %shard_map.214 = bf16[512,1280]{1,0:T(8,128)(2,1)} custom-call(bf16[512,512]{1,0:T(8,128)(2,1)S(1)} %bitcast.19, f32[512,128]{1,0:T(8,128)S(1)} %get-tuple-element.56.decays, bf16[512,1024]{1,0:T(8,128)(2,1)} %get-tuple-element.58.keep_h, bf16[512,640]{1,0:T(8,128)(2,1)S(1)} %collective-permute-done.2.first, bf16[512,384]{1,0:T(8,128)(2,1)S(1)} %collective-permute-done.3.second), custom_call_target="tpu_custom_call" | custom-call | flops 100000000 | bytes 1048576 | tf_op jit(solution)/shard_map/pallas_call | solution.py:58
  136.8 10.0 %all-to-all-start.3 = ((bf16[64,8,1280]{2,1,0:T(8,128)(2,1)}), bf16[64,8,1280]{2,1,0:T(8,128)(2,1)S(1)}, u32[]{:S(2)}, u32[]{:S(2)}) async-start(bf16[64,8,1280]{2,1,0:T(8,128)(2,1)} %bitcast.13), calls=%async_computation.3 | async-start | bytes 2621440 | tf_op jit(solution)/shard_map/all_to_all | solution.py:694
  147.9 1.2 copy-done.9
  149.1 1.2 copy-done.21
  150.2 11.8 %shard_map.217 = (bf16[1,2048,768]{2,1,0:T(8,128)(2,1)}, bf16[1,2048,768]{2,1,0:T(8,128)(2,1)}, bf16[1,768,2048]{2,1,0:T(8,128)(2,1)}) custom-call(s32[1]{0:T(128)} %bitcast.tp, bf16[576,1024]{1,0:T(8,128)(2,1)} %get-tuple-element.71.rows_o, bf16[576,1024]{1,0:T(8,128)(2,1)} %get-tuple-element.72.cot_o, bf16[576,1024]{1,0:T(8,128)(2,1)} %get-tuple-element.73.rows_p, ...), custom_call_target="tpu_custom_call" | custom-call | flops 5400000000 | bytes 1048576 | tf_op jit(solution)/shard_map/pallas_call | solution.py:58
  162.2 2.1 %shard_map.215 = (bf16[192,256]{1,0:T(8,128)(2,1)}, f32[192,512]{1,0:T(8,128)S(1)}, f32[192,256]{1,0:T(8,128)S(1)}) custom-call(bf16[192,512]{1,0:T(8,128)(2,1)S(1)} %copy-done.24, bf16[192,512]{1,0:T(8,128)(2,1)S(1)} %copy-done.14, bf16[192,256]{1,0:T(8,128)(2,1)S(1)} %copy-done.16, bf16[192,256]{1,0:T(8,128)(2,1)S(1)} %copy-done.18, ...), custom_call_target="tpu_custom_call" | custom-call | flops 600000000 | bytes 1048576 | tf_op jit(solution)/shard_map/pallas_call | solution.py:58
  165.7 1.4 all-to-all-done.3
  167.1 2.5 %shard_map.216 = (bf16[192,512]{1,0:T(8,128)(2,1)}, bf16[192,256]{1,0:T(8,128)(2,1)}, f32[32,512]{1,0:T(8,128)}) custom-call(s32[1]{0:T(128)} %bitcast.tp, bf16[512,1280]{1,0:T(8,128)(2,1)S(1)} %bitcast.18, bf16[192,512]{1,0:T(8,128)(2,1)} %values_h.1, bf16[192,256]{1,0:T(8,128)(2,1)} %in_map_h.1, f32[192,512]{1,0:T(8,128)} %copy-done.4, ...), custom_call_target="tpu_custom_call" | custom-call | flops 200000000 | bytes 1048576 | tf_op jit(solution)/shard_map/pallas_call | solution.py:58
  (63 shorter events, 5.1 us)
Async XLA Ops:
  49.8 5.6 %collective-permute-start = (bf16[512,2304]{1,0:T(8,128)(2,1)S(1)}, bf16[512,2304]{1,0:T(8,128)(2,1)S(1)}, u32[]{:S(2)}, u32[]{:S(2)}) collective-permute-start(bf16[512,2304]{1,0:T(8,128)(2,1)S(1)} %bitcast.15), channel_id=1, source_target_pairs={{0,1},{1,0},{2,3},{3,2},{4,5},{5,4},{6,7},{7,6},{8,9},{9,8},{10,11... | collective-permute-start | bytes 7077896 | tf_op jit(solution)/shard_map/ppermute | solution.py:707
  55.3 9.7 %copy-start.13 = (bf16[192,512]{1,0:T(8,128)(2,1)S(1)}, bf16[192,512]{1,0:T(8,128)(2,1)}, u32[]{:S(2)}) copy-start(bf16[192,512]{1,0:T(8,128)(2,1)} %values_h.1) | copy-start | bytes 589828
  55.3 9.7 %copy-start.16 = (bf16[192,256]{1,0:T(8,128)(2,1)S(1)}, bf16[192,256]{1,0:T(8,128)(2,1)}, u32[]{:S(2)}) copy-start(bf16[192,256]{1,0:T(8,128)(2,1)} %in_map_h.1) | copy-start | bytes 294916
  55.3 9.7 %copy-start.25 = (f32[192,8]{0,1:T(8,128)S(1)}, f32[192,8]{0,1:T(8,128)}, u32[]{:S(2)}) copy-start(f32[192,8]{0,1:T(8,128)} %param.27) | copy-start | bytes 18436
  55.4 11.3 %copy-start.1 = (bf16[1,2048,768]{2,1,0:T(8,128)(2,1)S(1)}, bf16[1,2048,768]{2,1,0:T(8,128)(2,1)}, u32[]{:S(2)}) copy-start(bf16[1,2048,768]{2,1,0:T(8,128)(2,1)} %up_w.1) | copy-start | bytes 9437188
  64.4 5.5 %collective-permute-start.1 = (bf16[576,1024]{1,0:T(8,128)(2,1)S(1)}, bf16[576,1024]{1,0:T(8,128)(2,1)S(1)}, u32[]{:S(2)}, u32[]{:S(2)}) collective-permute-start(bf16[576,1024]{1,0:T(8,128)(2,1)S(1)} %get-tuple-element.49), channel_id=1, source_target_pairs={{0,1},{1,0},{2,3},{3,2},{4,5},{5,4},{6,7},{7,6},{8,9},{9,8},{10,11... | collective-permute-start | bytes 3538952 | tf_op jit(solution)/shard_map/ppermute | solution.py:707
  66.7 95.5 %copy-start.4 = (f32[192,512]{1,0:T(8,128)}, f32[192,512]{1,0:T(8,128)S(1)}, u32[]{:S(2)}) copy-start(f32[192,512]{1,0:T(8,128)S(1)} %get-tuple-element.52.start_w.start_h) | copy-start | bytes 1179652
  66.7 95.5 %copy-start.5 = (f32[192,512]{1,0:T(8,128)}, f32[192,512]{1,0:T(8,128)S(1)}, u32[]{:S(2)}) copy-start(f32[192,512]{1,0:T(8,128)S(1)} %get-tuple-element.53.end_w.end_h) | copy-start | bytes 1179652
  71.9 30.9 %copy-start.2 = (bf16[192,2048]{1,0:T(8,128)(2,1)S(1)}, bf16[192,2048]{1,0:T(8,128)(2,1)}, u32[]{:S(2)}) copy-start(bf16[192,2048]{1,0:T(8,128)(2,1)} %cot.1) | copy-start | bytes 2359300
  71.9 30.9 %copy-start.19 = (s32[192,2]{0,1:T(2,128)S(1)}, s32[192,2]{0,1:T(2,128)}, u32[]{:S(2)}) copy-start(s32[192,2]{0,1:T(2,128)} %param.16) | copy-start | bytes 4612
  71.9 30.9 %all-to-all-start.1 = ((bf16[64,8,1536]{2,1,0:T(8,128)(2,1)}), bf16[64,8,1536]{2,1,0:T(8,128)(2,1)S(1)}, u32[]{:S(2)}, u32[]{:S(2)}) async-start(bf16[64,8,1536]{2,1,0:T(8,128)(2,1)} %bitcast.6), calls=%async_computation.1 | async-start | bytes 3145728 | tf_op jit(solution)/shard_map/all_to_all | solution.py:694
  102.8 4.6 %copy-start.3 = (bf16[512,2048]{1,0:T(8,128)(2,1)S(1)}, bf16[512,2048]{1,0:T(8,128)(2,1)}, u32[]{:S(2)}) copy-start(bf16[512,2048]{1,0:T(8,128)(2,1)} %proj_w.1) | copy-start | bytes 6291460
  102.8 4.6 %copy-start.11 = (bf16[192,512]{1,0:T(8,128)(2,1)S(1)}, bf16[192,512]{1,0:T(8,128)(2,1)}, u32[]{:S(2)}) copy-start(bf16[192,512]{1,0:T(8,128)(2,1)} %gate_in.1) | copy-start | bytes 589828
  102.8 4.6 %copy-start.12 = (bf16[192,512]{1,0:T(8,128)(2,1)S(1)}, bf16[192,512]{1,0:T(8,128)(2,1)}, u32[]{:S(2)}) copy-start(bf16[192,512]{1,0:T(8,128)(2,1)} %scan_out.1) | copy-start | bytes 589828
  102.8 4.6 %copy-start.17 = (bf16[192,256]{1,0:T(8,128)(2,1)S(1)}, bf16[192,256]{1,0:T(8,128)(2,1)}, u32[]{:S(2)}) copy-start(bf16[192,256]{1,0:T(8,128)(2,1)} %out_map.3) | copy-start | bytes 294916
  109.5 3.5 %copy-start.23 = (bf16[192,512]{1,0:T(8,128)(2,1)}, bf16[192,512]{1,0:T(8,128)(2,1)S(1)}, u32[]{:S(2)}) copy-start(bf16[192,512]{1,0:T(8,128)(2,1)S(1)} %get-tuple-element.61.scan_grad) | copy-start | bytes 589828
  112.5 21.6 %collective-permute-start.2 = (bf16[512,640]{1,0:T(8,128)(2,1)S(1)}, bf16[512,640]{1,0:T(8,128)(2,1)S(1)}, u32[]{:S(2)}, u32[]{:S(2)}) collective-permute-start(bf16[512,640]{1,0:T(8,128)(2,1)S(1)} %get-tuple-element.59), channel_id=1, source_target_pairs={{0,32},{1,9},{2,34},{3,11},{4,36},{5,13},{6,38},{7,15},{8,40},{9,1... | collective-permute-start | bytes 1966088 | tf_op jit(solution)/shard_map/ppermute | solution.py:752
  113.0 21.2 %all-to-all-start.2 = ((bf16[64,8,512]{2,1,0:T(8,128)(2,1)}), bf16[64,8,512]{2,1,0:T(8,128)(2,1)S(1)}, u32[]{:S(2)}, u32[]{:S(2)}) async-start(bf16[64,8,512]{2,1,0:T(8,128)(2,1)} %bitcast.9), calls=%async_computation.2 | async-start | bytes 1048576 | tf_op jit(solution)/shard_map/all_to_all | solution.py:694
  118.7 15.4 %collective-permute-start.3 = (bf16[512,384]{1,0:T(8,128)(2,1)}, bf16[512,384]{1,0:T(8,128)(2,1)S(1)}, u32[]{:S(2)}, u32[]{:S(2)}) collective-permute-start(bf16[512,384]{1,0:T(8,128)(2,1)} %copy-done.22), channel_id=1, source_target_pairs={{0,2},{1,3},{2,0},{3,1},{4,6},{5,7},{6,4},{7,5},{8,10},{9,11},{10,... | collective-permute-start | bytes 1179656 | tf_op jit(solution)/shard_map/ppermute | solution.py:752
  136.8 30.3 %all-to-all-start.3 = ((bf16[64,8,1280]{2,1,0:T(8,128)(2,1)}), bf16[64,8,1280]{2,1,0:T(8,128)(2,1)S(1)}, u32[]{:S(2)}, u32[]{:S(2)}) async-start(bf16[64,8,1280]{2,1,0:T(8,128)(2,1)} %bitcast.13), calls=%async_computation.3 | async-start | bytes 2621440 | tf_op jit(solution)/shard_map/all_to_all | solution.py:694
  150.2 11.9 %copy-start.14 = (bf16[192,512]{1,0:T(8,128)(2,1)S(1)}, bf16[192,512]{1,0:T(8,128)(2,1)}, u32[]{:S(2)}) copy-start(bf16[192,512]{1,0:T(8,128)(2,1)} %values_h.1) | copy-start | bytes 589828
  150.2 11.9 %copy-start.18 = (bf16[192,256]{1,0:T(8,128)(2,1)S(1)}, bf16[192,256]{1,0:T(8,128)(2,1)}, u32[]{:S(2)}) copy-start(bf16[192,256]{1,0:T(8,128)(2,1)} %out_map.3) | copy-start | bytes 294916
  150.2 11.9 %copy-start.24 = (bf16[192,512]{1,0:T(8,128)(2,1)S(1)}, bf16[192,512]{1,0:T(8,128)(2,1)}, u32[]{:S(2)}) copy-start(bf16[192,512]{1,0:T(8,128)(2,1)} %copy-done.23) | copy-start | bytes 589828
  150.2 11.9 %copy-start.27 = (f32[192,8]{1,0:T(8,128)S(1)}, f32[192,8]{1,0:T(8,128)}, u32[]{:S(2)}) copy-start(f32[192,8]{1,0:T(8,128)} %copy-done.26) | copy-start | bytes 18436
  (11 other events, 18.0 us)

commit v4 on v3

--- a/solution.py
+++ b/solution.py
@@ -247,14 +247,14 @@
         pltpu.make_async_copy(cot, cot_h, out_sems.at[1]),
     )
 
+    def start(group):
+        for c in group:
+            c.start()
+
     @pl.when(step == 0)
     def _():
-        for group in copies:
-            for c in group:
-                c.start()
+        start(copies[0])
         split_slots(got, rows, cot)
-        for c in keep:
-            c.start()
 
     for j, group in enumerate(copies):
 
@@ -262,6 +262,12 @@
         def _():
             for c in group:
                 c.wait()
+            if j == 0:
+                start(copies[1])
+            if j == 1:
+                start(keep)
+            if j < 1:
+                start(copies[2])
 
     return step, keep
 

time: 171 us -> 170 us (level)
  no operation moved by 1% of the time
where the time goes in v4:
time: 170 us; the launch traced here: 169 us
  Pallas kernels  49.8 us (29%)
  blocking collectives  47.4 us (28%)
  waiting for transfers between devices  40.5 us (24%)
  starting transfers between devices  23.9 us (14%)
  local copies, waits for them, and re-layouts  6.32 us (4%)
    pallas_call x13, Pallas kernels, run(): kernel(*[pltpu.with_memory_space_constraint(a, pltpu.HBM) if i in hbm_in...  49.8 us
    all_to_all x1, blocking collectives, swap(): out = lax.all_to_all(rows.reshape(BLOCKS, -1, lanes), SP, 0, 0, tiled=True)  44.6 us
    all_to_all x3, waiting for transfers between devices, swap(): out = lax.all_to_all(rows.reshape(BLOCKS, -1, lanes), SP, 0, 0, tiled=True)  26.7 us
    all_to_all x3, starting transfers between devices, swap(): out = lax.all_to_all(rows.reshape(BLOCKS, -1, lanes), SP, 0, 0, tiled=True)  21.2 us
    ppermute x2, waiting for transfers between devices, on_device(): others = [lax.ppermute(h, ALL, pairs_of(i)) for i, h in enumerate(halves)]  13.8 us
    unnamed x56, local copies, waits for them, and re-layouts  6.3 us
  transfers between devices with their start and end apart: 7, of which 3 were waited for; matrix products, arithmetic and copies ran while one was open for 0% of the time, Pallas kernels for 14%

profile of v4, /device:TPU:0, one launch (start us, length us, event | category | flops | bytes accessed | tf_op | source)
XLA Modules:
  0.0 169.0 jit_solution(10519126986029239709)
XLA Ops:
  0.6 4.5 %shard_map.205 = bf16[512,2304]{1,0:T(8,128)(2,1)} custom-call(s32[1]{0:T(128)} %bitcast.tp, s32[2,192]{1,0:T(2,128)} %bitcast.23, f32[2,192]{1,0:T(2,128)} %bitcast.27, bf16[192,2048]{1,0:T(8,128)(2,1)} %rows_hbm.1, bf16[192,2048]{1,0:T(8,128)(2,1)} %cot.1), custom_call_target="tpu_custom_call" | custom-call | flops 1000000000 | bytes 1048576 | tf_op jit(solution)/shard_map/pallas_call | solution.py:58
  5.2 44.6 %all_to_all.20 = bf16[64,8,2304]{2,1,0:T(8,128)(2,1)S(1)} all-to-all(bf16[64,8,2304]{2,1,0:T(8,128)(2,1)} %bitcast.26), channel_id=1, replica_groups=mesh['sp_0'=4,'sp_1'=4,'sp_2'=4,'tp'=2] {'sp_0','sp_1','sp_2'}, dimensions={0} | all-to-all | bytes 4718592 | tf_op jit(solution)/shard_map/all_to_all | solution.py:700
  49.8 5.4 %shard_map.206 = (bf16[576,1024]{1,0:T(8,128)(2,1)}, bf16[576,1024]{1,0:T(8,128)(2,1)}, f32[576,768]{1,0:T(8,128)S(1)}, f32[576,768]{1,0:T(8,128)S(1)}, f32[576,768]{1,0:T(8,128)S(1)}) custom-call(s32[1]{0:T(128)} %bitcast.tp, bf16[512,2304]{1,0:T(8,128)(2,1)S(1)} %bitcast.16, bf16[1,2048,768]{2,1,0:T(8,128)(2,1)} %gate_w.1, bf16[1,2048,768]{2,1,0:T(8,128)(2,1)} %up_w.1, ...), custom_call_target="tpu_custom_call" | custom-call | flops 2700000000 | bytes 1048576 | tf_op jit(solution)/shard_map/pallas_call | solution.py:58
  55.3 8.4 %shard_map.207 = (bf16[576,1024]{1,0:T(8,128)(2,1)}, bf16[576,1024]{1,0:T(8,128)(2,1)}, bf16[576,768]{1,0:T(8,128)(2,1)S(1)}, bf16[576,768]{1,0:T(8,128)(2,1)S(1...) custom-call(s32[1]{0:T(128)} %bitcast.tp, bf16[512,2304]{1,0:T(8,128)(2,1)S(1)} %collective-permute-done.peer, ...), custom_call_target="tpu_custom_call" | custom-call | flops 4499999744 | bytes 1048576 | tf_op jit(solution)/shard_map/pallas_call | solution.py:58
  64.3 1.6 shard_map.209
  66.4 2.7 %shard_map.208.own = bf16[576,1024]{1,0:T(8,128)(2,1)S(1)} custom-call(s32[1]{0:T(128)} %bitcast.tp, bf16[576,768]{1,0:T(8,128)(2,1)S(1)} %get-tuple-element.47.pre_grad, bf16[576,768]{1,0:T(8,128)(2,1)S(1)} %get-tuple-element.48.up_grad, bf16[1,2048,768]{2,1,0:T(8,128)(2,1)S(1)} %copy-done, bf16[1,2048,768]{2,1,0:T(8,128)(2,1)S(1)} %copy-done.1), custom_call_target="tpu_custom_call" | custom-call | flops 1800000000 | bytes 1048576 | tf_op jit(solution)/shard_map/pallas_call | solution.py:58
  69.2 1.9 %shard_map.210 = bf16[512,1536]{1,0:T(8,128)(2,1)} custom-call(bf16[576,1024]{1,0:T(8,128)(2,1)S(1)} %shard_map.208.own, bf16[576,1024]{1,0:T(8,128)(2,1)S(1)} %collective-permute-done.1.peer, bf16[512,384]{1,0:T(8,128)(2,1)S(1)} %get-tuple-element.50.states), custom_call_target="tpu_custom_call" | custom-call | flops 100000000 | bytes 1048576 | tf_op jit(solution)/shard_map/pallas_call | solution.py:58
  71.1 5.5 %all-to-all-start.1 = ((bf16[64,8,1536]{2,1,0:T(8,128)(2,1)}), bf16[64,8,1536]{2,1,0:T(8,128)(2,1)S(1)}, u32[]{:S(2)}, u32[]{:S(2)}) async-start(bf16[64,8,1536]{2,1,0:T(8,128)(2,1)} %bitcast.6), calls=%async_computation.1 | async-start | bytes 3145728 | tf_op jit(solution)/shard_map/all_to_all | solution.py:700
  76.7 25.3 %all-to-all-done.1 = bf16[64,8,1536]{2,1,0:T(8,128)(2,1)S(1)} async-done(((bf16[64,8,1536]{2,1,0:T(8,128)(2,1)}), bf16[64,8,1536]{2,1,0:T(8,128)(2,1)S(1)}, u32[]{:S(2)}, u32[]{:S(2)}) %all-to-all-start.1) | async-done | bytes 1572896 | tf_op jit(solution)/shard_map/all_to_all | solution.py:700
  102.1 1.8 %shard_map.211 = (bf16[192,1024]{1,0:T(8,128)(2,1)}, bf16[512,256]{1,0:T(8,128)(2,1)S(1)}, f32[512,128]{1,0:T(8,128)S(1)}) custom-call(s32[1]{0:T(128)} %bitcast.tp, bf16[512,1536]{1,0:T(8,128)(2,1)S(1)} %bitcast.17, s32[2,192]{1,0:T(2,128)S(1)} %bitcast.24, bf16[192,2048]{1,0:T(8,128)(2,1)S(1)} %copy-done.2), custom_call_target="tpu_custom_call" | custom-call | flops 300000000 | bytes 1048576 | tf_op jit(solution)/shard_map/pallas_call | solution.py:58
  103.9 2.7 %all-gather = bf16[384,1024]{1,0:T(8,128)(2,1)S(1)} all-gather(bf16[192,1024]{1,0:T(8,128)(2,1)} %get-tuple-element.35), channel_id=2, replica_groups=mesh['sp_0'=4,'sp_1'=4,'sp_2'=4,'tp'=2] {'tp'}, dimensions={0}, use_global_device_ids=true | all-gather | bytes 1179648 | tf_op jit(solution)/shard_map/all_gather | solution.py:750
  106.6 2.1 %shard_map.212 = (bf16[192,512]{1,0:T(8,128)(2,1)}, bf16[192,512]{1,0:T(8,128)(2,1)S(1)}, bf16[192,512]{1,0:T(8,128)(2,1)S(1)}, bf16[512,512]{1,0:T(8,128)(2,1)}) custom-call(bf16[2,192,1024]{2,1,0:T(8,128)(2,1)S(1)} %bitcast.21, bf16[512,2048]{1,0:T(8,128)(2,1)S(1)} %copy-done.3, bf16[192,512]{1,0:T(8,128)(2,1)S(1)} %copy-done.11, ...), custom_call_target="tpu_custom_call" | custom-call | flops 500000000 | bytes 1048576 | tf_op jit(solution)/shard_map/pallas_call | solution.py:58
  108.8 2.3 %shard_map.213 = (bf16[512,1024]{1,0:T(8,128)(2,1)}, bf16[512,640]{1,0:T(8,128)(2,1)S(1)}, bf16[512,384]{1,0:T(8,128)(2,1)S(1)}) custom-call(s32[2]{0:T(128)S(1)} %pad_add_fusion.odd, bf16[2,192,1024]{2,1,0:T(8,128)(2,1)S(1)} %bitcast.22, bf16[192,512]{1,0:T(8,128)(2,1)S(1)} %get-tuple-element.57.gated), custom_call_target="tpu_custom_call" | custom-call | flops 400000000 | bytes 1048576 | tf_op jit(solution)/shard_map/pallas_call | solution.py:58
  112.2 5.8 %all-to-all-start.2 = ((bf16[64,8,512]{2,1,0:T(8,128)(2,1)}), bf16[64,8,512]{2,1,0:T(8,128)(2,1)S(1)}, u32[]{:S(2)}, u32[]{:S(2)}) async-start(bf16[64,8,512]{2,1,0:T(8,128)(2,1)} %bitcast.9), calls=%async_computation.2 | async-start | bytes 1048576 | tf_op jit(solution)/shard_map/all_to_all | solution.py:700
  118.0 1.6 collective-permute-start.3
  119.6 13.8 %collective-permute-done.3.second = bf16[512,384]{1,0:T(8,128)(2,1)S(1)} collective-permute-done((bf16[512,384]{1,0:T(8,128)(2,1)}, bf16[512,384]{1,0:T(8,128)(2,1)S(1)}, u32[]{:S(2)}, u32[]{:S(2)}) %collective-permute-start.3) | collective-permute-done | bytes 393248 | tf_op jit(solution)/shard_map/ppermute | solution.py:758
  133.4 2.6 %shard_map.214 = bf16[512,1280]{1,0:T(8,128)(2,1)} custom-call(bf16[512,512]{1,0:T(8,128)(2,1)S(1)} %bitcast.19, f32[512,128]{1,0:T(8,128)S(1)} %get-tuple-element.56.decays, bf16[512,1024]{1,0:T(8,128)(2,1)} %get-tuple-element.58.keep_h, bf16[512,640]{1,0:T(8,128)(2,1)S(1)} %collective-permute-done.2.first, bf16[512,384]{1,0:T(8,128)(2,1)S(1)} %collective-permute-done.3.second), custom_call_target="tpu_custom_call" | custom-call | flops 100000000 | bytes 1048576 | tf_op jit(solution)/shard_map/pallas_call | solution.py:58
  136.0 10.0 %all-to-all-start.3 = ((bf16[64,8,1280]{2,1,0:T(8,128)(2,1)}), bf16[64,8,1280]{2,1,0:T(8,128)(2,1)S(1)}, u32[]{:S(2)}, u32[]{:S(2)}) async-start(bf16[64,8,1280]{2,1,0:T(8,128)(2,1)} %bitcast.13), calls=%async_computation.3 | async-start | bytes 2621440 | tf_op jit(solution)/shard_map/all_to_all | solution.py:700
  147.1 1.2 copy-done.9
  148.3 1.2 copy-done.21
  149.5 11.8 %shard_map.217 = (bf16[1,2048,768]{2,1,0:T(8,128)(2,1)}, bf16[1,2048,768]{2,1,0:T(8,128)(2,1)}, bf16[1,768,2048]{2,1,0:T(8,128)(2,1)}) custom-call(s32[1]{0:T(128)} %bitcast.tp, bf16[576,1024]{1,0:T(8,128)(2,1)} %get-tuple-element.71.rows_o, bf16[576,1024]{1,0:T(8,128)(2,1)} %get-tuple-element.72.cot_o, bf16[576,1024]{1,0:T(8,128)(2,1)} %get-tuple-element.73.rows_p, ...), custom_call_target="tpu_custom_call" | custom-call | flops 5400000000 | bytes 1048576 | tf_op jit(solution)/shard_map/pallas_call | solution.py:58
  161.4 2.1 %shard_map.215 = (bf16[192,256]{1,0:T(8,128)(2,1)}, f32[192,512]{1,0:T(8,128)S(1)}, f32[192,256]{1,0:T(8,128)S(1)}) custom-call(bf16[192,512]{1,0:T(8,128)(2,1)S(1)} %copy-done.24, bf16[192,512]{1,0:T(8,128)(2,1)S(1)} %copy-done.14, bf16[192,256]{1,0:T(8,128)(2,1)S(1)} %copy-done.16, bf16[192,256]{1,0:T(8,128)(2,1)S(1)} %copy-done.18, ...), custom_call_target="tpu_custom_call" | custom-call | flops 600000000 | bytes 1048576 | tf_op jit(solution)/shard_map/pallas_call | solution.py:58
  165.0 1.4 all-to-all-done.3
  166.3 2.5 %shard_map.216 = (bf16[192,512]{1,0:T(8,128)(2,1)}, bf16[192,256]{1,0:T(8,128)(2,1)}, f32[32,512]{1,0:T(8,128)}) custom-call(s32[1]{0:T(128)} %bitcast.tp, bf16[512,1280]{1,0:T(8,128)(2,1)S(1)} %bitcast.18, bf16[192,512]{1,0:T(8,128)(2,1)} %values_h.1, bf16[192,256]{1,0:T(8,128)(2,1)} %in_map_h.1, f32[192,512]{1,0:T(8,128)} %copy-done.4, ...), custom_call_target="tpu_custom_call" | custom-call | flops 200000000 | bytes 1048576 | tf_op jit(solution)/shard_map/pallas_call | solution.py:58
  (63 shorter events, 5.1 us)
Async XLA Ops:
  49.8 5.4 %collective-permute-start = (bf16[512,2304]{1,0:T(8,128)(2,1)S(1)}, bf16[512,2304]{1,0:T(8,128)(2,1)S(1)}, u32[]{:S(2)}, u32[]{:S(2)}) collective-permute-start(bf16[512,2304]{1,0:T(8,128)(2,1)S(1)} %bitcast.15), channel_id=1, source_target_pairs={{0,1},{1,0},{2,3},{3,2},{4,5},{5,4},{6,7},{7,6},{8,9},{9,8},{10,11... | collective-permute-start | bytes 7077896 | tf_op jit(solution)/shard_map/ppermute | solution.py:713
  55.2 9.0 %copy-start.13 = (bf16[192,512]{1,0:T(8,128)(2,1)S(1)}, bf16[192,512]{1,0:T(8,128)(2,1)}, u32[]{:S(2)}) copy-start(bf16[192,512]{1,0:T(8,128)(2,1)} %values_h.1) | copy-start | bytes 589828
  55.2 9.0 %copy-start.16 = (bf16[192,256]{1,0:T(8,128)(2,1)S(1)}, bf16[192,256]{1,0:T(8,128)(2,1)}, u32[]{:S(2)}) copy-start(bf16[192,256]{1,0:T(8,128)(2,1)} %in_map_h.1) | copy-start | bytes 294916
  55.2 9.0 %copy-start.25 = (f32[192,8]{0,1:T(8,128)S(1)}, f32[192,8]{0,1:T(8,128)}, u32[]{:S(2)}) copy-start(f32[192,8]{0,1:T(8,128)} %param.27) | copy-start | bytes 18436
  55.2 10.7 %copy-start.1 = (bf16[1,2048,768]{2,1,0:T(8,128)(2,1)S(1)}, bf16[1,2048,768]{2,1,0:T(8,128)(2,1)}, u32[]{:S(2)}) copy-start(bf16[1,2048,768]{2,1,0:T(8,128)(2,1)} %up_w.1) | copy-start | bytes 9437188
  63.7 5.5 %collective-permute-start.1 = (bf16[576,1024]{1,0:T(8,128)(2,1)S(1)}, bf16[576,1024]{1,0:T(8,128)(2,1)S(1)}, u32[]{:S(2)}, u32[]{:S(2)}) collective-permute-start(bf16[576,1024]{1,0:T(8,128)(2,1)S(1)} %get-tuple-element.49), channel_id=1, source_target_pairs={{0,1},{1,0},{2,3},{3,2},{4,5},{5,4},{6,7},{7,6},{8,9},{9,8},{10,11... | collective-permute-start | bytes 3538952 | tf_op jit(solution)/shard_map/ppermute | solution.py:713
  65.9 95.5 %copy-start.4 = (f32[192,512]{1,0:T(8,128)}, f32[192,512]{1,0:T(8,128)S(1)}, u32[]{:S(2)}) copy-start(f32[192,512]{1,0:T(8,128)S(1)} %get-tuple-element.52.start_w.start_h) | copy-start | bytes 1179652
  65.9 95.5 %copy-start.5 = (f32[192,512]{1,0:T(8,128)}, f32[192,512]{1,0:T(8,128)S(1)}, u32[]{:S(2)}) copy-start(f32[192,512]{1,0:T(8,128)S(1)} %get-tuple-element.53.end_w.end_h) | copy-start | bytes 1179652
  71.1 30.9 %copy-start.2 = (bf16[192,2048]{1,0:T(8,128)(2,1)S(1)}, bf16[192,2048]{1,0:T(8,128)(2,1)}, u32[]{:S(2)}) copy-start(bf16[192,2048]{1,0:T(8,128)(2,1)} %cot.1) | copy-start | bytes 2359300
  71.1 30.9 %copy-start.19 = (s32[192,2]{0,1:T(2,128)S(1)}, s32[192,2]{0,1:T(2,128)}, u32[]{:S(2)}) copy-start(s32[192,2]{0,1:T(2,128)} %param.16) | copy-start | bytes 4612
  71.1 30.9 %all-to-all-start.1 = ((bf16[64,8,1536]{2,1,0:T(8,128)(2,1)}), bf16[64,8,1536]{2,1,0:T(8,128)(2,1)S(1)}, u32[]{:S(2)}, u32[]{:S(2)}) async-start(bf16[64,8,1536]{2,1,0:T(8,128)(2,1)} %bitcast.6), calls=%async_computation.1 | async-start | bytes 3145728 | tf_op jit(solution)/shard_map/all_to_all | solution.py:700
  102.0 4.6 %copy-start.3 = (bf16[512,2048]{1,0:T(8,128)(2,1)S(1)}, bf16[512,2048]{1,0:T(8,128)(2,1)}, u32[]{:S(2)}) copy-start(bf16[512,2048]{1,0:T(8,128)(2,1)} %proj_w.1) | copy-start | bytes 6291460
  102.0 4.6 %copy-start.11 = (bf16[192,512]{1,0:T(8,128)(2,1)S(1)}, bf16[192,512]{1,0:T(8,128)(2,1)}, u32[]{:S(2)}) copy-start(bf16[192,512]{1,0:T(8,128)(2,1)} %gate_in.1) | copy-start | bytes 589828
  102.0 4.6 %copy-start.12 = (bf16[192,512]{1,0:T(8,128)(2,1)S(1)}, bf16[192,512]{1,0:T(8,128)(2,1)}, u32[]{:S(2)}) copy-start(bf16[192,512]{1,0:T(8,128)(2,1)} %scan_out.1) | copy-start | bytes 589828
  102.1 4.6 %copy-start.17 = (bf16[192,256]{1,0:T(8,128)(2,1)S(1)}, bf16[192,256]{1,0:T(8,128)(2,1)}, u32[]{:S(2)}) copy-start(bf16[192,256]{1,0:T(8,128)(2,1)} %out_map.3) | copy-start | bytes 294916
  108.8 3.4 %copy-start.23 = (bf16[192,512]{1,0:T(8,128)(2,1)}, bf16[192,512]{1,0:T(8,128)(2,1)S(1)}, u32[]{:S(2)}) copy-start(bf16[192,512]{1,0:T(8,128)(2,1)S(1)} %get-tuple-element.61.scan_grad) | copy-start | bytes 589828
  111.8 21.6 %collective-permute-start.2 = (bf16[512,640]{1,0:T(8,128)(2,1)S(1)}, bf16[512,640]{1,0:T(8,128)(2,1)S(1)}, u32[]{:S(2)}, u32[]{:S(2)}) collective-permute-start(bf16[512,640]{1,0:T(8,128)(2,1)S(1)} %get-tuple-element.59), channel_id=1, source_target_pairs={{0,32},{1,9},{2,34},{3,11},{4,36},{5,13},{6,38},{7,15},{8,40},{9,1... | collective-permute-start | bytes 1966088 | tf_op jit(solution)/shard_map/ppermute | solution.py:758
  112.2 21.2 %all-to-all-start.2 = ((bf16[64,8,512]{2,1,0:T(8,128)(2,1)}), bf16[64,8,512]{2,1,0:T(8,128)(2,1)S(1)}, u32[]{:S(2)}, u32[]{:S(2)}) async-start(bf16[64,8,512]{2,1,0:T(8,128)(2,1)} %bitcast.9), calls=%async_computation.2 | async-start | bytes 1048576 | tf_op jit(solution)/shard_map/all_to_all | solution.py:700
  118.0 15.4 %collective-permute-start.3 = (bf16[512,384]{1,0:T(8,128)(2,1)}, bf16[512,384]{1,0:T(8,128)(2,1)S(1)}, u32[]{:S(2)}, u32[]{:S(2)}) collective-permute-start(bf16[512,384]{1,0:T(8,128)(2,1)} %copy-done.22), channel_id=1, source_target_pairs={{0,2},{1,3},{2,0},{3,1},{4,6},{5,7},{6,4},{7,5},{8,10},{9,11},{10,... | collective-permute-start | bytes 1179656 | tf_op jit(solution)/shard_map/ppermute | solution.py:758
  136.0 30.3 %all-to-all-start.3 = ((bf16[64,8,1280]{2,1,0:T(8,128)(2,1)}), bf16[64,8,1280]{2,1,0:T(8,128)(2,1)S(1)}, u32[]{:S(2)}, u32[]{:S(2)}) async-start(bf16[64,8,1280]{2,1,0:T(8,128)(2,1)} %bitcast.13), calls=%async_computation.3 | async-start | bytes 2621440 | tf_op jit(solution)/shard_map/all_to_all | solution.py:700
  149.5 11.9 %copy-start.14 = (bf16[192,512]{1,0:T(8,128)(2,1)S(1)}, bf16[192,512]{1,0:T(8,128)(2,1)}, u32[]{:S(2)}) copy-start(bf16[192,512]{1,0:T(8,128)(2,1)} %values_h.1) | copy-start | bytes 589828
  149.5 11.9 %copy-start.18 = (bf16[192,256]{1,0:T(8,128)(2,1)S(1)}, bf16[192,256]{1,0:T(8,128)(2,1)}, u32[]{:S(2)}) copy-start(bf16[192,256]{1,0:T(8,128)(2,1)} %out_map.3) | copy-start | bytes 294916
  149.5 11.9 %copy-start.24 = (bf16[192,512]{1,0:T(8,128)(2,1)S(1)}, bf16[192,512]{1,0:T(8,128)(2,1)}, u32[]{:S(2)}) copy-start(bf16[192,512]{1,0:T(8,128)(2,1)} %copy-done.23) | copy-start | bytes 589828
  149.5 11.9 %copy-start.27 = (f32[192,8]{1,0:T(8,128)S(1)}, f32[192,8]{1,0:T(8,128)}, u32[]{:S(2)}) copy-start(f32[192,8]{1,0:T(8,128)} %copy-done.26) | copy-start | bytes 18436
  (11 other events, 18.0 us)

commit v5 on v4

--- a/solution.py
+++ b/solution.py
@@ -280,9 +280,11 @@
         tp[0], own, (gate_h, up_h, down_h), rows_h, cot_h, rows, cot, (gate_w, up_w, down_w),
         sems, out_sems,
     )
-    gate_o[...] = mm(rows[...], gate_w[step], NN)
-    up_o[...] = mm(rows[...], up_w[step], NN)
-    act_o[...] = mm(cot[...], down_w[step], NT)
+    for first in range(0, SLOTS, SLOTS // 2):
+        at = slice(first, first + SLOTS // 2)
+        gate_o[at] = mm(rows[at], gate_w[step], NN)
+        up_o[at] = mm(rows[at], up_w[step], NN)
+        act_o[at] = mm(cot[at], down_w[step], NT)
 
     @pl.when(step == 2)
     def _():

time: 170 us -> 170 us (level)
  no operation moved by 1% of the time
where the time goes in v5:
time: 170 us; the launch traced here: 169 us
  Pallas kernels  49.8 us (29%)
  blocking collectives  47.4 us (28%)
  waiting for transfers between devices  40.5 us (24%)
  starting transfers between devices  23.9 us (14%)
  local copies, waits for them, and re-layouts  6.3 us (4%)
    pallas_call x13, Pallas kernels, run(): kernel(*[pltpu.with_memory_space_constraint(a, pltpu.HBM) if i in hbm_in...  49.8 us
    all_to_all x1, blocking collectives, swap(): out = lax.all_to_all(rows.reshape(BLOCKS, -1, lanes), SP, 0, 0, tiled=True)  44.6 us
    all_to_all x3, waiting for transfers between devices, swap(): out = lax.all_to_all(rows.reshape(BLOCKS, -1, lanes), SP, 0, 0, tiled=True)  26.7 us
    all_to_all x3, starting transfers between devices, swap(): out = lax.all_to_all(rows.reshape(BLOCKS, -1, lanes), SP, 0, 0, tiled=True)  21.2 us
    ppermute x2, waiting for transfers between devices, on_device(): others = [lax.ppermute(h, ALL, pairs_of(i)) for i, h in enumerate(halves)]  13.8 us
    unnamed x56, local copies, waits for them, and re-layouts  6.28 us
  transfers between devices with their start and end apart: 7, of which 3 were waited for; matrix products, arithmetic and copies ran while one was open for 0% of the time, Pallas kernels for 14%

profile of v5, /device:TPU:0, one launch (start us, length us, event | category | flops | bytes accessed | tf_op | source)
XLA Modules:
  0.0 169.0 jit_solution(14307861078077896395)
XLA Ops:
  0.6 4.5 %shard_map.205 = bf16[512,2304]{1,0:T(8,128)(2,1)} custom-call(s32[1]{0:T(128)} %bitcast.tp, s32[2,192]{1,0:T(2,128)} %bitcast.23, f32[2,192]{1,0:T(2,128)} %bitcast.27, bf16[192,2048]{1,0:T(8,128)(2,1)} %rows_hbm.1, bf16[192,2048]{1,0:T(8,128)(2,1)} %cot.1), custom_call_target="tpu_custom_call" | custom-call | flops 1000000000 | bytes 1048576 | tf_op jit(solution)/shard_map/pallas_call | solution.py:58
  5.2 44.6 %all_to_all.20 = bf16[64,8,2304]{2,1,0:T(8,128)(2,1)S(1)} all-to-all(bf16[64,8,2304]{2,1,0:T(8,128)(2,1)} %bitcast.26), channel_id=1, replica_groups=mesh['sp_0'=4,'sp_1'=4,'sp_2'=4,'tp'=2] {'sp_0','sp_1','sp_2'}, dimensions={0} | all-to-all | bytes 4718592 | tf_op jit(solution)/shard_map/all_to_all | solution.py:702
  49.8 5.4 %shard_map.206 = (bf16[576,1024]{1,0:T(8,128)(2,1)}, bf16[576,1024]{1,0:T(8,128)(2,1)}, f32[576,768]{1,0:T(8,128)S(1)}, f32[576,768]{1,0:T(8,128)S(1)}, f32[576,768]{1,0:T(8,128)S(1)}) custom-call(s32[1]{0:T(128)} %bitcast.tp, bf16[512,2304]{1,0:T(8,128)(2,1)S(1)} %bitcast.16, bf16[1,2048,768]{2,1,0:T(8,128)(2,1)} %gate_w.1, bf16[1,2048,768]{2,1,0:T(8,128)(2,1)} %up_w.1, ...), custom_call_target="tpu_custom_call" | custom-call | flops 2700000000 | bytes 1048576 | tf_op jit(solution)/shard_map/pallas_call | solution.py:58
  55.3 8.4 %shard_map.207 = (bf16[576,1024]{1,0:T(8,128)(2,1)}, bf16[576,1024]{1,0:T(8,128)(2,1)}, bf16[576,768]{1,0:T(8,128)(2,1)S(1)}, bf16[576,768]{1,0:T(8,128)(2,1)S(1...) custom-call(s32[1]{0:T(128)} %bitcast.tp, bf16[512,2304]{1,0:T(8,128)(2,1)S(1)} %collective-permute-done.peer, ...), custom_call_target="tpu_custom_call" | custom-call | flops 4499999744 | bytes 1048576 | tf_op jit(solution)/shard_map/pallas_call | solution.py:58
  64.3 1.6 shard_map.209
  66.4 2.7 %shard_map.208.own = bf16[576,1024]{1,0:T(8,128)(2,1)S(1)} custom-call(s32[1]{0:T(128)} %bitcast.tp, bf16[576,768]{1,0:T(8,128)(2,1)S(1)} %get-tuple-element.47.pre_grad, bf16[576,768]{1,0:T(8,128)(2,1)S(1)} %get-tuple-element.48.up_grad, bf16[1,2048,768]{2,1,0:T(8,128)(2,1)S(1)} %copy-done, bf16[1,2048,768]{2,1,0:T(8,128)(2,1)S(1)} %copy-done.1), custom_call_target="tpu_custom_call" | custom-call | flops 1800000000 | bytes 1048576 | tf_op jit(solution)/shard_map/pallas_call | solution.py:58
  69.2 1.9 %shard_map.210 = bf16[512,1536]{1,0:T(8,128)(2,1)} custom-call(bf16[576,1024]{1,0:T(8,128)(2,1)S(1)} %shard_map.208.own, bf16[576,1024]{1,0:T(8,128)(2,1)S(1)} %collective-permute-done.1.peer, bf16[512,384]{1,0:T(8,128)(2,1)S(1)} %get-tuple-element.50.states), custom_call_target="tpu_custom_call" | custom-call | flops 100000000 | bytes 1048576 | tf_op jit(solution)/shard_map/pallas_call | solution.py:58
  71.1 5.5 %all-to-all-start.1 = ((bf16[64,8,1536]{2,1,0:T(8,128)(2,1)}), bf16[64,8,1536]{2,1,0:T(8,128)(2,1)S(1)}, u32[]{:S(2)}, u32[]{:S(2)}) async-start(bf16[64,8,1536]{2,1,0:T(8,128)(2,1)} %bitcast.6), calls=%async_computation.1 | async-start | bytes 3145728 | tf_op jit(solution)/shard_map/all_to_all | solution.py:702
  76.7 25.3 %all-to-all-done.1 = bf16[64,8,1536]{2,1,0:T(8,128)(2,1)S(1)} async-done(((bf16[64,8,1536]{2,1,0:T(8,128)(2,1)}), bf16[64,8,1536]{2,1,0:T(8,128)(2,1)S(1)}, u32[]{:S(2)}, u32[]{:S(2)}) %all-to-all-start.1) | async-done | bytes 1572896 | tf_op jit(solution)/shard_map/all_to_all | solution.py:702
  102.1 1.8 %shard_map.211 = (bf16[192,1024]{1,0:T(8,128)(2,1)}, bf16[512,256]{1,0:T(8,128)(2,1)S(1)}, f32[512,128]{1,0:T(8,128)S(1)}) custom-call(s32[1]{0:T(128)} %bitcast.tp, bf16[512,1536]{1,0:T(8,128)(2,1)S(1)} %bitcast.17, s32[2,192]{1,0:T(2,128)S(1)} %bitcast.24, bf16[192,2048]{1,0:T(8,128)(2,1)S(1)} %copy-done.2), custom_call_target="tpu_custom_call" | custom-call | flops 300000000 | bytes 1048576 | tf_op jit(solution)/shard_map/pallas_call | solution.py:58
  103.9 2.7 %all-gather = bf16[384,1024]{1,0:T(8,128)(2,1)S(1)} all-gather(bf16[192,1024]{1,0:T(8,128)(2,1)} %get-tuple-element.35), channel_id=2, replica_groups=mesh['sp_0'=4,'sp_1'=4,'sp_2'=4,'tp'=2] {'tp'}, dimensions={0}, use_global_device_ids=true | all-gather | bytes 1179648 | tf_op jit(solution)/shard_map/all_gather | solution.py:752
  106.6 2.1 %shard_map.212 = (bf16[192,512]{1,0:T(8,128)(2,1)}, bf16[192,512]{1,0:T(8,128)(2,1)S(1)}, bf16[192,512]{1,0:T(8,128)(2,1)S(1)}, bf16[512,512]{1,0:T(8,128)(2,1)}) custom-call(bf16[2,192,1024]{2,1,0:T(8,128)(2,1)S(1)} %bitcast.21, bf16[512,2048]{1,0:T(8,128)(2,1)S(1)} %copy-done.3, bf16[192,512]{1,0:T(8,128)(2,1)S(1)} %copy-done.11, ...), custom_call_target="tpu_custom_call" | custom-call | flops 500000000 | bytes 1048576 | tf_op jit(solution)/shard_map/pallas_call | solution.py:58
  108.8 2.3 %shard_map.213 = (bf16[512,1024]{1,0:T(8,128)(2,1)}, bf16[512,640]{1,0:T(8,128)(2,1)S(1)}, bf16[512,384]{1,0:T(8,128)(2,1)S(1)}) custom-call(s32[2]{0:T(128)S(1)} %pad_add_fusion.odd, bf16[2,192,1024]{2,1,0:T(8,128)(2,1)S(1)} %bitcast.22, bf16[192,512]{1,0:T(8,128)(2,1)S(1)} %get-tuple-element.57.gated), custom_call_target="tpu_custom_call" | custom-call | flops 400000000 | bytes 1048576 | tf_op jit(solution)/shard_map/pallas_call | solution.py:58
  112.2 5.8 %all-to-all-start.2 = ((bf16[64,8,512]{2,1,0:T(8,128)(2,1)}), bf16[64,8,512]{2,1,0:T(8,128)(2,1)S(1)}, u32[]{:S(2)}, u32[]{:S(2)}) async-start(bf16[64,8,512]{2,1,0:T(8,128)(2,1)} %bitcast.9), calls=%async_computation.2 | async-start | bytes 1048576 | tf_op jit(solution)/shard_map/all_to_all | solution.py:702
  118.0 1.6 collective-permute-start.3
  119.6 13.8 %collective-permute-done.3.second = bf16[512,384]{1,0:T(8,128)(2,1)S(1)} collective-permute-done((bf16[512,384]{1,0:T(8,128)(2,1)}, bf16[512,384]{1,0:T(8,128)(2,1)S(1)}, u32[]{:S(2)}, u32[]{:S(2)}) %collective-permute-start.3) | collective-permute-done | bytes 393248 | tf_op jit(solution)/shard_map/ppermute | solution.py:760
  133.4 2.6 %shard_map.214 = bf16[512,1280]{1,0:T(8,128)(2,1)} custom-call(bf16[512,512]{1,0:T(8,128)(2,1)S(1)} %bitcast.19, f32[512,128]{1,0:T(8,128)S(1)} %get-tuple-element.56.decays, bf16[512,1024]{1,0:T(8,128)(2,1)} %get-tuple-element.58.keep_h, bf16[512,640]{1,0:T(8,128)(2,1)S(1)} %collective-permute-done.2.first, bf16[512,384]{1,0:T(8,128)(2,1)S(1)} %collective-permute-done.3.second), custom_call_target="tpu_custom_call" | custom-call | flops 100000000 | bytes 1048576 | tf_op jit(solution)/shard_map/pallas_call | solution.py:58
  136.0 10.0 %all-to-all-start.3 = ((bf16[64,8,1280]{2,1,0:T(8,128)(2,1)}), bf16[64,8,1280]{2,1,0:T(8,128)(2,1)S(1)}, u32[]{:S(2)}, u32[]{:S(2)}) async-start(bf16[64,8,1280]{2,1,0:T(8,128)(2,1)} %bitcast.13), calls=%async_computation.3 | async-start | bytes 2621440 | tf_op jit(solution)/shard_map/all_to_all | solution.py:702
  147.1 1.2 copy-done.9
  148.3 1.2 copy-done.21
  149.5 11.8 %shard_map.217 = (bf16[1,2048,768]{2,1,0:T(8,128)(2,1)}, bf16[1,2048,768]{2,1,0:T(8,128)(2,1)}, bf16[1,768,2048]{2,1,0:T(8,128)(2,1)}) custom-call(s32[1]{0:T(128)} %bitcast.tp, bf16[576,1024]{1,0:T(8,128)(2,1)} %get-tuple-element.71.rows_o, bf16[576,1024]{1,0:T(8,128)(2,1)} %get-tuple-element.72.cot_o, bf16[576,1024]{1,0:T(8,128)(2,1)} %get-tuple-element.73.rows_p, ...), custom_call_target="tpu_custom_call" | custom-call | flops 5400000000 | bytes 1048576 | tf_op jit(solution)/shard_map/pallas_call | solution.py:58
  161.4 2.1 %shard_map.215 = (bf16[192,256]{1,0:T(8,128)(2,1)}, f32[192,512]{1,0:T(8,128)S(1)}, f32[192,256]{1,0:T(8,128)S(1)}) custom-call(bf16[192,512]{1,0:T(8,128)(2,1)S(1)} %copy-done.24, bf16[192,512]{1,0:T(8,128)(2,1)S(1)} %copy-done.14, bf16[192,256]{1,0:T(8,128)(2,1)S(1)} %copy-done.16, bf16[192,256]{1,0:T(8,128)(2,1)S(1)} %copy-done.18, ...), custom_call_target="tpu_custom_call" | custom-call | flops 600000000 | bytes 1048576 | tf_op jit(solution)/shard_map/pallas_call | solution.py:58
  165.0 1.4 all-to-all-done.3
  166.3 2.5 %shard_map.216 = (bf16[192,512]{1,0:T(8,128)(2,1)}, bf16[192,256]{1,0:T(8,128)(2,1)}, f32[32,512]{1,0:T(8,128)}) custom-call(s32[1]{0:T(128)} %bitcast.tp, bf16[512,1280]{1,0:T(8,128)(2,1)S(1)} %bitcast.18, bf16[192,512]{1,0:T(8,128)(2,1)} %values_h.1, bf16[192,256]{1,0:T(8,128)(2,1)} %in_map_h.1, f32[192,512]{1,0:T(8,128)} %copy-done.4, ...), custom_call_target="tpu_custom_call" | custom-call | flops 200000000 | bytes 1048576 | tf_op jit(solution)/shard_map/pallas_call | solution.py:58
  (63 shorter events, 5.1 us)
Async XLA Ops:
  49.8 5.5 %collective-permute-start = (bf16[512,2304]{1,0:T(8,128)(2,1)S(1)}, bf16[512,2304]{1,0:T(8,128)(2,1)S(1)}, u32[]{:S(2)}, u32[]{:S(2)}) collective-permute-start(bf16[512,2304]{1,0:T(8,128)(2,1)S(1)} %bitcast.15), channel_id=1, source_target_pairs={{0,1},{1,0},{2,3},{3,2},{4,5},{5,4},{6,7},{7,6},{8,9},{9,8},{10,11... | collective-permute-start | bytes 7077896 | tf_op jit(solution)/shard_map/ppermute | solution.py:715
  55.2 9.0 %copy-start.13 = (bf16[192,512]{1,0:T(8,128)(2,1)S(1)}, bf16[192,512]{1,0:T(8,128)(2,1)}, u32[]{:S(2)}) copy-start(bf16[192,512]{1,0:T(8,128)(2,1)} %values_h.1) | copy-start | bytes 589828
  55.2 9.0 %copy-start.16 = (bf16[192,256]{1,0:T(8,128)(2,1)S(1)}, bf16[192,256]{1,0:T(8,128)(2,1)}, u32[]{:S(2)}) copy-start(bf16[192,256]{1,0:T(8,128)(2,1)} %in_map_h.1) | copy-start | bytes 294916
  55.2 9.0 %copy-start.25 = (f32[192,8]{0,1:T(8,128)S(1)}, f32[192,8]{0,1:T(8,128)}, u32[]{:S(2)}) copy-start(f32[192,8]{0,1:T(8,128)} %param.27) | copy-start | bytes 18436
  55.3 10.7 %copy-start.1 = (bf16[1,2048,768]{2,1,0:T(8,128)(2,1)S(1)}, bf16[1,2048,768]{2,1,0:T(8,128)(2,1)}, u32[]{:S(2)}) copy-start(bf16[1,2048,768]{2,1,0:T(8,128)(2,1)} %up_w.1) | copy-start | bytes 9437188
  63.7 5.5 %collective-permute-start.1 = (bf16[576,1024]{1,0:T(8,128)(2,1)S(1)}, bf16[576,1024]{1,0:T(8,128)(2,1)S(1)}, u32[]{:S(2)}, u32[]{:S(2)}) collective-permute-start(bf16[576,1024]{1,0:T(8,128)(2,1)S(1)} %get-tuple-element.49), channel_id=1, source_target_pairs={{0,1},{1,0},{2,3},{3,2},{4,5},{5,4},{6,7},{7,6},{8,9},{9,8},{10,11... | collective-permute-start | bytes 3538952 | tf_op jit(solution)/shard_map/ppermute | solution.py:715
  65.9 95.4 %copy-start.4 = (f32[192,512]{1,0:T(8,128)}, f32[192,512]{1,0:T(8,128)S(1)}, u32[]{:S(2)}) copy-start(f32[192,512]{1,0:T(8,128)S(1)} %get-tuple-element.52.start_w.start_h) | copy-start | bytes 1179652
  65.9 95.4 %copy-start.5 = (f32[192,512]{1,0:T(8,128)}, f32[192,512]{1,0:T(8,128)S(1)}, u32[]{:S(2)}) copy-start(f32[192,512]{1,0:T(8,128)S(1)} %get-tuple-element.53.end_w.end_h) | copy-start | bytes 1179652
  71.1 30.9 %copy-start.2 = (bf16[192,2048]{1,0:T(8,128)(2,1)S(1)}, bf16[192,2048]{1,0:T(8,128)(2,1)}, u32[]{:S(2)}) copy-start(bf16[192,2048]{1,0:T(8,128)(2,1)} %cot.1) | copy-start | bytes 2359300
  71.1 30.9 %copy-start.19 = (s32[192,2]{0,1:T(2,128)S(1)}, s32[192,2]{0,1:T(2,128)}, u32[]{:S(2)}) copy-start(s32[192,2]{0,1:T(2,128)} %param.16) | copy-start | bytes 4612
  71.1 30.9 %all-to-all-start.1 = ((bf16[64,8,1536]{2,1,0:T(8,128)(2,1)}), bf16[64,8,1536]{2,1,0:T(8,128)(2,1)S(1)}, u32[]{:S(2)}, u32[]{:S(2)}) async-start(bf16[64,8,1536]{2,1,0:T(8,128)(2,1)} %bitcast.6), calls=%async_computation.1 | async-start | bytes 3145728 | tf_op jit(solution)/shard_map/all_to_all | solution.py:702
  102.0 4.6 %copy-start.3 = (bf16[512,2048]{1,0:T(8,128)(2,1)S(1)}, bf16[512,2048]{1,0:T(8,128)(2,1)}, u32[]{:S(2)}) copy-start(bf16[512,2048]{1,0:T(8,128)(2,1)} %proj_w.1) | copy-start | bytes 6291460
  102.0 4.6 %copy-start.11 = (bf16[192,512]{1,0:T(8,128)(2,1)S(1)}, bf16[192,512]{1,0:T(8,128)(2,1)}, u32[]{:S(2)}) copy-start(bf16[192,512]{1,0:T(8,128)(2,1)} %gate_in.1) | copy-start | bytes 589828
  102.0 4.6 %copy-start.12 = (bf16[192,512]{1,0:T(8,128)(2,1)S(1)}, bf16[192,512]{1,0:T(8,128)(2,1)}, u32[]{:S(2)}) copy-start(bf16[192,512]{1,0:T(8,128)(2,1)} %scan_out.1) | copy-start | bytes 589828
  102.1 4.6 %copy-start.17 = (bf16[192,256]{1,0:T(8,128)(2,1)S(1)}, bf16[192,256]{1,0:T(8,128)(2,1)}, u32[]{:S(2)}) copy-start(bf16[192,256]{1,0:T(8,128)(2,1)} %out_map.3) | copy-start | bytes 294916
  108.8 3.4 %copy-start.23 = (bf16[192,512]{1,0:T(8,128)(2,1)}, bf16[192,512]{1,0:T(8,128)(2,1)S(1)}, u32[]{:S(2)}) copy-start(bf16[192,512]{1,0:T(8,128)(2,1)S(1)} %get-tuple-element.61.scan_grad) | copy-start | bytes 589828
  111.8 21.6 %collective-permute-start.2 = (bf16[512,640]{1,0:T(8,128)(2,1)S(1)}, bf16[512,640]{1,0:T(8,128)(2,1)S(1)}, u32[]{:S(2)}, u32[]{:S(2)}) collective-permute-start(bf16[512,640]{1,0:T(8,128)(2,1)S(1)} %get-tuple-element.59), channel_id=1, source_target_pairs={{0,32},{1,9},{2,34},{3,11},{4,36},{5,13},{6,38},{7,15},{8,40},{9,1... | collective-permute-start | bytes 1966088 | tf_op jit(solution)/shard_map/ppermute | solution.py:760
  112.2 21.2 %all-to-all-start.2 = ((bf16[64,8,512]{2,1,0:T(8,128)(2,1)}), bf16[64,8,512]{2,1,0:T(8,128)(2,1)S(1)}, u32[]{:S(2)}, u32[]{:S(2)}) async-start(bf16[64,8,512]{2,1,0:T(8,128)(2,1)} %bitcast.9), calls=%async_computation.2 | async-start | bytes 1048576 | tf_op jit(solution)/shard_map/all_to_all | solution.py:702
  118.0 15.4 %collective-permute-start.3 = (bf16[512,384]{1,0:T(8,128)(2,1)}, bf16[512,384]{1,0:T(8,128)(2,1)S(1)}, u32[]{:S(2)}, u32[]{:S(2)}) collective-permute-start(bf16[512,384]{1,0:T(8,128)(2,1)} %copy-done.22), channel_id=1, source_target_pairs={{0,2},{1,3},{2,0},{3,1},{4,6},{5,7},{6,4},{7,5},{8,10},{9,11},{10,... | collective-permute-start | bytes 1179656 | tf_op jit(solution)/shard_map/ppermute | solution.py:760
  136.0 30.3 %all-to-all-start.3 = ((bf16[64,8,1280]{2,1,0:T(8,128)(2,1)}), bf16[64,8,1280]{2,1,0:T(8,128)(2,1)S(1)}, u32[]{:S(2)}, u32[]{:S(2)}) async-start(bf16[64,8,1280]{2,1,0:T(8,128)(2,1)} %bitcast.13), calls=%async_computation.3 | async-start | bytes 2621440 | tf_op jit(solution)/shard_map/all_to_all | solution.py:702
  149.5 11.9 %copy-start.14 = (bf16[192,512]{1,0:T(8,128)(2,1)S(1)}, bf16[192,512]{1,0:T(8,128)(2,1)}, u32[]{:S(2)}) copy-start(bf16[192,512]{1,0:T(8,128)(2,1)} %values_h.1) | copy-start | bytes 589828
  149.5 11.9 %copy-start.18 = (bf16[192,256]{1,0:T(8,128)(2,1)S(1)}, bf16[192,256]{1,0:T(8,128)(2,1)}, u32[]{:S(2)}) copy-start(bf16[192,256]{1,0:T(8,128)(2,1)} %out_map.3) | copy-start | bytes 294916
  149.5 11.9 %copy-start.24 = (bf16[192,512]{1,0:T(8,128)(2,1)S(1)}, bf16[192,512]{1,0:T(8,128)(2,1)}, u32[]{:S(2)}) copy-start(bf16[192,512]{1,0:T(8,128)(2,1)} %copy-done.23) | copy-start | bytes 589828
  149.5 11.9 %copy-start.27 = (f32[192,8]{1,0:T(8,128)S(1)}, f32[192,8]{1,0:T(8,128)}, u32[]{:S(2)}) copy-start(f32[192,8]{1,0:T(8,128)} %copy-done.26) | copy-start | bytes 18436
  (11 other events, 18.0 us)
